TPU v7x, 512 devices: a whole 4x4x16 slice. The times are simulated.
512 devices in a mesh: sp: 128 (over z, x, core), tp: 4 (over y).
Axes of the slice: x: 4, y: 4, z: 16, core: 2. Of those that a mesh axis runs over, the one named last changes fastest.
Arguments:
- stream: bfloat16 [16384, 2048], P('sp', 'tp')
- norm_gain: float32 [2048], P('tp'), may hold values from 0.1 to 1.9
- w_value: bfloat16 [2048, 512], P(None, 'tp'), may hold values from -0.125 to 0.125
- w_mix: bfloat16 [2048, 512], P(None, 'tp'), may hold values from -0.125 to 0.125
- w_gate: bfloat16 [2048, 512], P(None, 'tp'), may hold values from -0.125 to 0.125
- w_state: bfloat16 [2048, 512], P(None, 'tp'), may hold values from -0.125 to 0.125
- conv_taps: float32 [3, 512], P(None, 'tp'), may hold values from -3 to 3
- skip_gain: float32 [512], P('tp'), may hold values from -3 to 3
- decay_rate: float32 [2, 32, 64], P(None, 'tp'), as said below
- turn_rate: float32 [2, 32, 64], P(None, 'tp'), may hold values from 0.25 to 1.5
- input_real: float32 [2, 32, 64, 16], P(None, 'tp')
- input_imag: float32 [2, 32, 64, 16], P(None, 'tp')
- read_real: float32 [2, 32, 16, 64], P(None, 'tp'), may hold values from -0.75 to 0.75
- read_imag: float32 [2, 32, 16, 64], P(None, 'tp'), may hold values from -0.75 to 0.75
- initial_state: float32 [2, 2, 32, 64], P(None, None, 'tp'), may hold values from -5 to 5
- intervals: float32 [16384], P('sp'), as said below
- proj_conv: bfloat16 [512, 2048], P('tp'), may hold values from -0.1875 to 0.1875
- proj_state: bfloat16 [512, 2048], P('tp'), may hold values from -0.1875 to 0.1875
Outputs:
- mixed: bfloat16 [16384, 2048], P('sp', 'tp')
Inputs may be any that keep to these rules, and one draw needn't show every extreme that they name: `decay_rate`: Positive. `intervals`: Positive.
All inputs are finite; a program needn't handle non-finite values.
Results may differ from a plain program's by a relative error of at most 0.024.
Values may be sent and summed in bfloat16 or wider, within the bound.
No kernel may reach another device: no remote copies, remote signals or barrier semaphores. Data moves between devices by JAX's collectives and lax.ppermute only.
A program may use at most 64 MiB of HBM per device.

v0:
```python
import jax
import jax.numpy as jnp
from jax import lax
from jax.sharding import Mesh
from jax.sharding import PartitionSpec as P

D = 2048
SP = ("sp_0", "sp_1", "sp_2")


EPSILON = 1e-06
HIGH = lax.Precision.HIGHEST


def from_everyone(shard, axis):
    size = lax.axis_size(axis)
    return lax.all_to_all(
        jnp.broadcast_to(shard[None], (size, *shard.shape)), axis, 0, 0, tiled=True
    )


def over_copies(shard, axis):
    return from_everyone(shard, axis).sum(axis=0)


def laid_out(parts, dim):
    parts = jnp.moveaxis(parts, 0, dim)
    dims = parts.shape
    return parts.reshape(*dims[:dim], dims[dim] * dims[dim + 1], *dims[dim + 2 :])


def gather_directly(shard, axis, dim):
    parts = from_everyone(shard, axis)
    return laid_out(parts, dim)


def padded_2(shard, sides, width):
    for axis, dim in sides:
        size, length = (lax.axis_size(axis), shard.shape[dim])
        up = [(i, (i + 1) % size) for i in range(size - 1)]
        down = [(j, i) for i, j in up]
        last = lax.slice_in_dim(shard, length - width, length, axis=dim)
        first = lax.slice_in_dim(shard, 0, width, axis=dim)
        before = lax.ppermute(last, axis, up)
        after = lax.ppermute(first, axis, down)
        shard = jnp.concatenate([before, shard, after], axis=dim)
    return shard


def neutral_like(shard, identity):
    return jax.tree.map(
        lambda a, e: jnp.broadcast_to(jnp.asarray(e, a.dtype), a.shape), shard, identity
    )


def all_in_one(shard, axis):
    leaves = jax.tree.leaves(shard)
    sequence = sorted(range(len(leaves)), key=lambda k: -leaves[k].size)
    width = (1, *leaves[sequence[0]].shape)[-1]
    lines = [
        jnp.pad(leaves[k].reshape(-1), (0, -leaves[k].size % width)).reshape(-1, width)
        for k in sequence
    ]
    both, at, found = (lax.all_gather(jnp.concatenate(lines), axis), 0, {})
    for k, line in zip(sequence, lines):
        section = both[:, at : at + len(line)].reshape(len(both), -1)
        found[k] = section[:, : leaves[k].size].reshape(-1, *leaves[k].shape)
        at += len(line)
    numbers = iter(range(len(leaves)))
    return jax.tree.map(lambda _: found[next(numbers)], shard)


def entering(shard, axes, combine, identity, reverse):
    before = start = neutral_like(shard, identity)
    subtotal = shard
    for axis in reversed(axes):
        size, place = (lax.axis_size(axis), lax.axis_index(axis))
        pieces = all_in_one(subtotal, axis)
        inside, subtotal = (start, start)
        for k in reversed(range(size)) if reverse else range(size):
            passed = k > place if reverse else k < place
            subtotal = combine(subtotal, jax.tree.map(lambda part: part[k], pieces))
            inside = jax.tree.map(lambda new, old: jnp.where(passed, new, old), subtotal, inside)
        before = combine(inside, before)
    return before


def cut_along(shard, dim, size):
    dims = shard.shape
    parts = shard.reshape(*dims[:dim], size, dims[dim] // size, *dims[dim + 1 :])
    return jnp.moveaxis(parts, dim, 0)


def summed_on_arrival(shard, axis, dim):
    parts = cut_along(shard, dim, lax.axis_size(axis))
    arrived = lax.all_to_all(parts, axis, split_axis=0, concat_axis=0, tiled=True)
    return arrived.astype(jnp.float32).sum(axis=0)


def step_factors(decay_rate, turn_rate, interval):
    damping = -decay_rate * interval
    angle = turn_rate * interval
    magnitude = jnp.exp(damping)
    factor_re = magnitude * jnp.cos(angle)
    factor_im = magnitude * jnp.sin(angle)
    half_sine = jnp.sin(0.5 * angle)
    lift_re = jnp.expm1(damping) * jnp.cos(angle) - 2.0 * half_sine * half_sine
    denominator = decay_rate * decay_rate + turn_rate * turn_rate
    gain_real = (turn_rate * factor_im - decay_rate * lift_re) / denominator
    gain_im = -(decay_rate * factor_im + turn_rate * lift_re) / denominator
    return (factor_re, factor_im, gain_real, gain_im)


def advance(elapsed, real_part, imaginary_piece, decay_rate, turn_rate):
    magnitude = jnp.exp(-decay_rate * elapsed)
    angle = turn_rate * elapsed
    cosine = magnitude * jnp.cos(angle)
    sine = magnitude * jnp.sin(angle)
    return (
        cosine * real_part - sine * imaginary_piece,
        sine * real_part + cosine * imaginary_piece,
    )


def chain_rule(decay_rate, turn_rate):

    def compose_edges(earlier, later):
        moved_re, moved_im = advance(later[0], earlier[1], earlier[2], decay_rate, turn_rate)
        return (earlier[0] + later[0], moved_re + later[1], moved_im + later[2])

    return compose_edges


def compose_steps(earlier, later):
    product_re = earlier[0] * later[0] - earlier[1] * later[1]
    product_im = earlier[0] * later[1] + earlier[1] * later[0]
    carried_re = later[0] * earlier[2] - later[1] * earlier[3] + later[2]
    carried_im = later[0] * earlier[3] + later[1] * earlier[2] + later[3]
    return (product_re, product_im, carried_re, carried_im)


def spread_input(matrix, identity_map):
    groups, states, group_width = matrix.shape
    wide = jnp.einsum("gph,gk->ghkp", matrix, identity_map, precision=HIGH)
    return wide.reshape(groups * group_width, groups * states)


def spread_read(matrix, identity_map):
    groups, group_width, states = matrix.shape
    wide = jnp.einsum("ghp,gk->gpkh", matrix, identity_map, precision=HIGH)
    return wide.reshape(groups * states, groups * group_width)


def per_device(
    stream,
    norm_gain,
    w_value,
    w_mix,
    w_gate,
    w_state,
    conv_taps,
    skip_gain,
    decay_rate,
    turn_rate,
    input_real,
    input_imag,
    read_real,
    read_imag,
    initial_state,
    intervals,
    proj_conv,
    proj_state,
):
    row_count = stream.shape[0]
    weights = jnp.concatenate([w_value, w_mix, w_gate, w_state], axis=1)
    widened = stream.astype(jnp.float32)
    squares = over_copies(jnp.sum(widened * widened, axis=1), "tp")
    inv_rms = lax.rsqrt(squares / D + EPSILON)
    normed = (widened * inv_rms[:, None] * norm_gain).astype(jnp.bfloat16)
    projected = jnp.dot(
        gather_directly(normed, "tp", 1), weights, preferred_element_type=jnp.float32
    )
    channels = w_value.shape[1]
    conv_value = projected[:, :channels].astype(jnp.bfloat16)
    conv_mix = projected[:, channels : 2 * channels].astype(jnp.bfloat16)
    conv_gate = projected[:, 2 * channels : 3 * channels].astype(jnp.bfloat16)
    state_input = projected[:, 3 * channels :].astype(jnp.bfloat16)
    source = (conv_mix.astype(jnp.float32) * conv_value.astype(jnp.float32)).astype(jnp.bfloat16)
    padded = padded_2(source, ((SP, 0),), 1).astype(jnp.float32)
    filtered = conv_taps[0] * padded[:-2] + conv_taps[1] * padded[1:-1] + conv_taps[2] * padded[2:]
    conv_out = (conv_gate.astype(jnp.float32) * filtered).astype(jnp.bfloat16)
    state_float = state_input.astype(jnp.float32)
    identity_map = jnp.eye(decay_rate.shape[1], dtype=jnp.float32)
    position = lax.axis_index(SP)
    final_index = lax.axis_size(SP) - 1
    elapsed = jnp.sum(intervals)
    responses = state_float * skip_gain
    runs = []
    edges = []
    for direction in range(2):
        backward = direction == 1
        rate_vec = decay_rate[direction].reshape(-1)
        turn_vec = turn_rate[direction].reshape(-1)
        factor_re, factor_im, gain_real, gain_im = step_factors(
            rate_vec, turn_vec, intervals[:, None]
        )
        driven_re = jnp.dot(
            state_float, spread_input(input_real[direction], identity_map), precision=HIGH
        )
        driven_im = jnp.dot(
            state_float, spread_input(input_imag[direction], identity_map), precision=HIGH
        )
        push_re = gain_real * driven_re - gain_im * driven_im
        push_im = gain_real * driven_im + gain_im * driven_re
        local_run = lax.associative_scan(
            compose_steps, (factor_re, factor_im, push_re, push_im), reverse=backward, axis=0
        )
        start_re = initial_state[direction, 0].reshape(-1)
        start_im = initial_state[direction, 1].reshape(-1)
        chain_end = position == (final_index if backward else 0)
        entered_re, entered_im = advance(elapsed, start_re, start_im, rate_vec, turn_vec)
        edge_row = 0 if backward else row_count - 1
        edge_re = local_run[2][edge_row] + jnp.where(chain_end, entered_re, 0.0)
        edge_im = local_run[3][edge_row] + jnp.where(chain_end, entered_im, 0.0)
        runs.append((rate_vec, turn_vec, local_run, start_re, start_im, chain_end))
        edges.append((edge_re, edge_im))
    blank = jnp.zeros_like(edges[0][0])
    forward_in = entering(
        (elapsed, edges[0][0], edges[0][1]),
        SP,
        chain_rule(runs[0][0], runs[0][1]),
        (jnp.zeros((), jnp.float32), blank, blank),
        False,
    )
    backward_in = entering(
        (elapsed, edges[1][0], edges[1][1]),
        SP,
        chain_rule(runs[1][0], runs[1][1]),
        (jnp.zeros((), jnp.float32), blank, blank),
        True,
    )
    arrivals = [(forward_in[1], forward_in[2]), (backward_in[1], backward_in[2])]
    for direction in range(2):
        rate_vec, turn_vec, local_run, start_re, start_im, chain_end = runs[direction]
        incoming_re = arrivals[direction][0] + jnp.where(chain_end, start_re, 0.0)
        incoming_im = arrivals[direction][1] + jnp.where(chain_end, start_im, 0.0)
        state_re = local_run[2] + local_run[0] * incoming_re - local_run[1] * incoming_im
        state_im = local_run[3] + local_run[0] * incoming_im + local_run[1] * incoming_re
        responses = responses + jnp.dot(
            state_re, spread_read(read_real[direction], identity_map), precision=HIGH
        )
        responses = responses - jnp.dot(
            state_im, spread_read(read_imag[direction], identity_map), precision=HIGH
        )
    state_out = jax.nn.gelu(responses).astype(jnp.bfloat16)
    branches = jnp.concatenate([conv_out, state_out], axis=1)
    projection = jnp.concatenate([proj_conv, proj_state], axis=0)
    partial_terms = jnp.dot(branches, projection, preferred_element_type=jnp.float32)
    result = summed_on_arrival(partial_terms.astype(jnp.bfloat16), "tp", 1)
    return result.astype(jnp.bfloat16)


def solution(mesh):
    finer = Mesh(mesh.devices.reshape(16, 4, 2, mesh.shape["tp"]), ("sp_0", "sp_1", "sp_2", "tp"))
    return jax.shard_map(
        per_device,
        mesh=finer,
        in_specs=(
            P(SP, "tp"),
            P("tp"),
            P(None, "tp"),
            P(None, "tp"),
            P(None, "tp"),
            P(None, "tp"),
            P(None, "tp"),
            P("tp"),
            P(None, "tp", None),
            P(None, "tp", None),
            P(None, "tp", None, None),
            P(None, "tp", None, None),
            P(None, "tp", None, None),
            P(None, "tp", None, None),
            P(None, None, "tp", None),
            P(SP),
            P("tp", None),
            P("tp", None),
        ),
        out_specs=P(SP, "tp"),
        check_vma=False,
    )
```

profile of v0, /device:TPU:32, one launch (start us, length us, event | category | flops | bytes accessed | tf_op | source)
XLA Modules:
  0.0 263.2 jit_solution(3959704297367488250)
XLA Ops:
  0.0 1.0 fusion.20
  1.6 4.5 %all-to-all-start = ((f32[4,1,128]{2,1,0:T(1,128)}), f32[4,1,128]{2,1,0:T(1,128)S(1)}, u32[]{:S(2)}, u32[]{:S(2)}) async-start(f32[4,1,128]{2,1,0:T(1,128)} %broadcast_in_dim.19), calls=%async_computation | async-start | bytes 4096 | tf_op jit(solution)/shard_map/all_to_all | solution.py:17
  6.1 1.3 reduce_sum.41
  7.4 1.2 pad.415
  8.6 1.3 sine_multiply_fusion.4
  11.4 0.9 slice_bitcast_fusion.1
  13.5 1.3 multiply_bitcast_fusion.3
  20.0 1.9 reshape.3187
  21.9 1.9 reshape.3175
  23.9 0.9 reshape.3174
  24.8 0.9 reshape.3197
  25.8 0.9 reshape.3196
  26.9 0.7 copy-done.8
  27.8 0.9 broadcast_in_dim.20
  28.7 4.9 %all-to-all-start.1 = ((bf16[4,128,512]{1,2,0:T(8,128)(2,1)}), bf16[4,128,512]{1,2,0:T(8,128)(2,1)S(1)}, u32[]{:S(2)}, u32[]{:S(2)}) async-start(bf16[4,128,512]{1,2,0:T(8,128)(2,1)} %broadcast_in_dim.20), calls=%async_computation.1 | async-start | bytes 1048576 | tf_op jit(solution)/shard_map/all_to_all | solution.py:17
  34.2 8.4 %all-to-all-done.1 = bf16[4,128,512]{1,2,0:T(8,128)(2,1)S(1)} async-done(((bf16[4,128,512]{1,2,0:T(8,128)(2,1)}), bf16[4,128,512]{1,2,0:T(8,128)(2,1)S(1)}, u32[]{:S(2)}, u32[]{:S(2)}) %all-to-all-start.1) | async-done | bytes 524320 | tf_op jit(solution)/shard_map/all_to_all | solution.py:17
  42.6 1.5 fusion.8
  45.1 2.2 multiply_add_fusion
  55.8 0.8 multiply_subtract_fusion.2
  57.7 1.9 all-gather.9
  62.1 1.3 fusion.104
  63.8 12.5 %all-gather.10 = f32[4,3,512]{2,1,0:T(4,128)S(1)} all-gather(f32[1,3,512]{2,1,0:T(4,128)S(1)} %maximum_bitcast_fusion.2), channel_id=6, replica_groups=mesh['sp_0'=16,'sp_1'=4,'sp_2'=2,'tp'=4] {'sp_1'}, dimensions={0}, use_global_device_ids=true | all-gather | bytes 30720 | tf_op jit(solution)/shard_map/all_gather | solution.py:64
  77.4 2.2 multiply_add_fusion.1
  86.3 3.7 %cosine_multiply_fusion.1 = (f32[1,8,64]{2,1,0:T(8,128)}, f32[1,8,64]{2,1,0:T(8,128)S(1)}, f32[1,8,64]{2,1,0:T(8,128)S(1)}, f32[1,8,64]{2,1,0:T(8,128)}, f32[1,8...) fusion(f32[]{:T(128)} %bitcast.117, f32[2,8,64]{2,1,0:T(8,128)S(1)} %copy-done.17, ...), kind=kLoop, calls=%fused_computation.342 | loop fusion | flops 11776 | bytes 22548 | tf_op jit(solution)/shard_map/mul | solution.py:117
  94.9 0.8 multiply_subtract_fusion.4
  96.0 0.7 copy-done.7
  96.9 1.8 all-gather.6
  101.1 2.5 sine_multiply_fusion.1
  104.0 11.9 %all-gather.7 = f32[4,3,512]{2,1,0:T(4,128)S(1)} all-gather(f32[1,3,512]{2,1,0:T(4,128)S(1)} %maximum_bitcast_fusion), channel_id=3, replica_groups=mesh['sp_0'=16,'sp_1'=4,'sp_2'=2,'tp'=4] {'sp_1'}, dimensions={0}, use_global_device_ids=true | all-gather | bytes 30720 | tf_op jit(solution)/shard_map/all_gather | solution.py:64
  118.4 1.3 cosine_multiply_fusion.6
  119.8 3.2 %cosine_multiply_fusion = (f32[1,8,64]{2,1,0:T(8,128)S(1)}, f32[1,8,64]{2,1,0:T(8,128)S(1)}, f32[1,8,64]{2,1,0:T(8,128)S(1)}, f32[1,8,64]{2,1,0:T(8,128)S(1)}, f...) fusion(f32[]{:T(128)} %bitcast.116, f32[2,8,64]{2,1,0:T(8,128)S(1)} %copy-done.17, ...), kind=kLoop, calls=%fused_computation.340 | loop fusion | flops 11776 | bytes 22548 | tf_op jit(solution)/shard_map/mul | solution.py:117
  125.0 34.0 %all-gather.8 = f32[16,3,512]{2,1,0:T(4,128)S(1)} all-gather(f32[1,3,512]{2,1,0:T(4,128)S(1)} %maximum_bitcast_fusion.1), channel_id=4, replica_groups=mesh['sp_0'=16,'sp_1'=4,'sp_2'=2,'tp'=4] {'sp_0'}, dimensions={0}, use_global_device_ids=true | all-gather | bytes 104448 | tf_op jit(solution)/shard_map/all_gather | solution.py:64
  162.9 28.8 %all-gather.11 = f32[16,3,512]{2,1,0:T(4,128)S(1)} all-gather(f32[1,3,512]{2,1,0:T(4,128)S(1)} %maximum_bitcast_fusion.3), channel_id=7, replica_groups=mesh['sp_0'=16,'sp_1'=4,'sp_2'=2,'tp'=4] {'sp_0'}, dimensions={0}, use_global_device_ids=true | all-gather | bytes 104448 | tf_op jit(solution)/shard_map/all_gather | solution.py:64
  193.7 1.3 fusion.113
  194.9 1.9 collective-permute-start
  196.9 6.1 %collective-permute-start.1 = (bf16[1,128]{1,0:T(2,128)(2,1)}, bf16[1,128]{1,0:T(2,128)(2,1)}, u32[]{:S(2)}, u32[]{:S(2)}) collective-permute-start(bf16[1,128]{1,0:T(2,128)(2,1)} %get-tuple-element.186), channel_id=1, source_target_pairs={{4,0},{8,4},{12,8},{16,12},{20,16},{24,20},{28,24},{32,28},{36,32}... | collective-permute-start | bytes 776 | tf_op jit(solution)/shard_map/ppermute | solution.py:45
  203.0 1.4 rev.16
  205.9 0.8 copy-done.4
  208.1 0.8 copy-done.6
  210.2 0.8 copy.91
  211.6 0.8 copy.90
  213.0 15.1 %add_add_fusion.44 = (f32[512]{0:T(512)S(1)}, f32[512]{0:T(512)S(1)}, f32[512]{0:T(512)S(1)}, f32[512]{0:T(512)S(1)}, f32[512]{0:T(512)S(1)}) fusion(f32[512]{0:T(512)} %select_n.1270, f32[512]{0:T(512)S(1)} %copy-done.30, f32[]{:T(128)S(6)} %add.2791, f32[]{:T(128)S(6)} %select_n.1201, pred[]{:T(512)S(6)} %gt.71, f32[512]{0:T(512)S(1)} %bitcast.369, ...), kind=kLoop, calls=%fused_computation.565 | loop fusion | flops 167424 | bytes 106614 | tf_op jit(solution)/shard_map/add | solution.py:245
  228.1 2.0 add_add_fusion.43
  230.1 1.1 convolution_add_fusion.1
  232.4 14.7 %add_add_fusion.23 = (f32[512]{0:T(512)S(1)}, f32[512]{0:T(512)S(1)}, f32[512]{0:T(512)S(1)}, f32[512]{0:T(512)S(1)}, f32[512]{0:T(512)S(1)}) fusion(f32[512]{0:T(512)S(1)} %copy-done.47, f32[512]{0:T(512)S(1)} %copy-done.26, f32[]{:T(128)S(6)} %add.2979, f32[]{:T(128)S(6)} %select_n.1281, pred[]{:T(512)S(6)} %lt.71, f32[512]{0:T(512)S(1)} %bitcast.361, ...), kind=kLoop, calls=%fused_computation.435 | loop fusion | flops 167424 | bytes 106614 | tf_op jit(solution)/shard_map/add | solution.py:245
  247.1 2.0 add_add_fusion.22
  252.0 10.5 %all_to_all.16 = bf16[4,128,512]{2,1,0:T(8,128)(2,1)S(1)} all-to-all(bf16[4,128,512]{2,1,0:T(8,128)(2,1)S(1)} %bitcast.354), channel_id=1, replica_groups=mesh['sp_0'=16,'sp_1'=4,'sp_2'=2,'tp'=4] {'tp'}, dimensions={0} | all-to-all | bytes 1048576 | tf_op jit(solution)/shard_map/all_to_all | solution.py:96
  262.5 0.7 reduce_sum.42
  (747 shorter events, 45.3 us)
Async XLA Ops:
  0.0 12.4 %copy-start.22 = (f32[2,8,16,64]{3,2,1,0:T(8,128)S(1)}, f32[2,8,16,64]{3,2,1,0:T(8,128)}, u32[]{:S(2)}) copy-start(f32[2,8,16,64]{3,2,1,0:T(8,128)} %param.31) | copy-start | bytes 196612
  1.6 25.2 %all-to-all-start = ((f32[4,1,128]{2,1,0:T(1,128)}), f32[4,1,128]{2,1,0:T(1,128)S(1)}, u32[]{:S(2)}, u32[]{:S(2)}) async-start(f32[4,1,128]{2,1,0:T(1,128)} %broadcast_in_dim.19), calls=%async_computation | async-start | bytes 4096 | tf_op jit(solution)/shard_map/all_to_all | solution.py:17
  10.7 34.3 %copy-start.25 = (f32[512]{0:T(512)}, f32[512]{0:T(512)S(1)}, u32[]{:S(2)}) copy-start(f32[512]{0:T(512)S(1)} %mul.6742) | copy-start | bytes 6148
  10.8 34.3 %copy-start.27 = (f32[512]{0:T(512)}, f32[512]{0:T(512)S(1)}, u32[]{:S(2)}) copy-start(f32[512]{0:T(512)S(1)} %reshape_squeeze.23) | copy-start | bytes 6148
  11.4 1.1 copy-start.23
  11.4 1.1 copy-start.24
  27.8 14.7 %copy-start.97 = (bf16[2048,128]{1,0:T(8,128)(2,1)S(1)}, bf16[2048,128]{1,0:T(8,128)(2,1)}, u32[]{:S(2)}) copy-start(bf16[2048,128]{1,0:T(8,128)(2,1)} %param.21) | copy-start | bytes 1572868
  28.7 4.9 %copy-start.94 = (f32[3,128]{1,0:T(4,128)S(1)}, f32[3,128]{1,0:T(4,128)}, u32[]{:S(2)}) copy-start(f32[3,128]{1,0:T(4,128)} %param.24) | copy-start | bytes 4612
  28.7 13.9 %copy-start.95 = (bf16[2048,128]{1,0:T(8,128)(2,1)S(1)}, bf16[2048,128]{1,0:T(8,128)(2,1)}, u32[]{:S(2)}) copy-start(bf16[2048,128]{1,0:T(8,128)(2,1)} %param.23) | copy-start | bytes 1572868
  28.7 13.9 %copy-start.96 = (bf16[2048,128]{1,0:T(8,128)(2,1)S(1)}, bf16[2048,128]{1,0:T(8,128)(2,1)}, u32[]{:S(2)}) copy-start(bf16[2048,128]{1,0:T(8,128)(2,1)} %param.22) | copy-start | bytes 1572868
  28.7 13.8 %all-to-all-start.1 = ((bf16[4,128,512]{1,2,0:T(8,128)(2,1)}), bf16[4,128,512]{1,2,0:T(8,128)(2,1)S(1)}, u32[]{:S(2)}, u32[]{:S(2)}) async-start(bf16[4,128,512]{1,2,0:T(8,128)(2,1)} %broadcast_in_dim.20), calls=%async_computation.1 | async-start | bytes 1048576 | tf_op jit(solution)/shard_map/all_to_all | solution.py:17
  44.1 33.3 %copy-start.13 = (bf16[128,512]{1,0:T(8,128)(2,1)}, bf16[128,512]{1,0:T(8,128)(2,1)S(1)}, u32[]{:S(2)}) copy-start(bf16[128,512]{1,0:T(8,128)(2,1)S(1)} %fusion.8) | copy-start | bytes 393220
  44.1 1.0 copy-start.16
  44.1 1.0 copy-start.100
  57.0 5.2 %copy-start.17 = (f32[2,8,64]{2,1,0:T(8,128)S(1)}, f32[2,8,64]{2,1,0:T(8,128)}, u32[]{:S(2)}) copy-start(f32[2,8,64]{2,1,0:T(8,128)} %param.26) | copy-start | bytes 12292
  57.0 5.2 %copy-start.18 = (f32[2,8,64]{2,1,0:T(8,128)S(1)}, f32[2,8,64]{2,1,0:T(8,128)}, u32[]{:S(2)}) copy-start(f32[2,8,64]{2,1,0:T(8,128)} %param.27) | copy-start | bytes 12292
  57.0 19.9 %copy-start = (f32[128,512]{1,0:T(8,128)S(1)}, f32[128,512]{1,0:T(8,128)}, u32[]{:S(2)}) copy-start(f32[128,512]{1,0:T(8,128)} %reshape.3175) | copy-start | bytes 786436
  57.6 19.8 %copy-start.15 = (f32[128,512]{1,0:T(8,128)S(1)}, f32[128,512]{1,0:T(8,128)}, u32[]{:S(2)}) copy-start(f32[128,512]{1,0:T(8,128)} %reshape.3174) | copy-start | bytes 786436
  57.6 19.8 %copy-start.101 = (f32[128]{0:T(128)S(1)}, f32[128]{0:T(128)}, u32[]{:S(2)}) copy-start(f32[128]{0:T(128)} %param.33) | copy-start | bytes 1540
  76.3 3.4 %copy-start.19 = (f32[4,3,512]{2,1,0:T(4,128)}, f32[4,3,512]{2,1,0:T(4,128)S(1)}, u32[]{:S(2)}) copy-start(f32[4,3,512]{2,1,0:T(4,128)S(1)} %all-gather.10) | copy-start | bytes 73732
  77.3 2.4 copy-start.29
  77.4 2.3 copy-start.31
  95.9 1.0 copy-start.40
  96.8 65.4 %copy-start.46 = (f32[1,8,64]{2,1,0:T(8,128)S(1)}, f32[1,8,64]{2,1,0:T(8,128)}, u32[]{:S(2)}) copy-start(f32[1,8,64]{2,1,0:T(8,128)} %get-tuple-element.259) | copy-start | bytes 6148
  96.8 65.4 %copy-start.45 = (f32[1,8,64]{2,1,0:T(8,128)S(1)}, f32[1,8,64]{2,1,0:T(8,128)}, u32[]{:S(2)}) copy-start(f32[1,8,64]{2,1,0:T(8,128)} %get-tuple-element.264) | copy-start | bytes 6148
  96.8 65.5 %copy-start.44 = (f32[1,8,64]{2,1,0:T(8,128)S(1)}, f32[1,8,64]{2,1,0:T(8,128)}, u32[]{:S(2)}) copy-start(f32[1,8,64]{2,1,0:T(8,128)} %get-tuple-element.262) | copy-start | bytes 6148
  96.8 65.6 %copy-start.43 = (f32[1,8,64]{2,1,0:T(8,128)S(1)}, f32[1,8,64]{2,1,0:T(8,128)}, u32[]{:S(2)}) copy-start(f32[1,8,64]{2,1,0:T(8,128)} %get-tuple-element.263) | copy-start | bytes 6148
  96.9 65.6 %copy-start.42 = (f32[1,8,64]{2,1,0:T(8,128)S(1)}, f32[1,8,64]{2,1,0:T(8,128)}, u32[]{:S(2)}) copy-start(f32[1,8,64]{2,1,0:T(8,128)} %get-tuple-element.265) | copy-start | bytes 6148
  96.9 65.9 %copy-start.20 = (f32[4,3,512]{2,1,0:T(4,128)S(1)}, f32[4,3,512]{2,1,0:T(4,128)}, u32[]{:S(2)}) copy-start(f32[4,3,512]{2,1,0:T(4,128)} %copy-done.19) | copy-start | bytes 73732
  194.9 55.6 %collective-permute-start = (bf16[1,128]{1,0:T(2,128)(2,1)}, bf16[1,128]{1,0:T(2,128)(2,1)}, u32[]{:S(2)}, u32[]{:S(2)}) collective-permute-start(bf16[1,128]{1,0:T(2,128)(2,1)} %get-tuple-element.185), channel_id=1, source_target_pairs={{0,4},{4,8},{8,12},{12,16},{16,20},{20,24},{24,28},{28,32},{32,36}... | collective-permute-start | bytes 776 | tf_op jit(solution)/shard_map/ppermute | solution.py:44
  196.8 8.9 %copy-start.10 = (f32[63,512]{1,0:T(8,128)S(1)}, f32[63,512]{1,0:T(8,128)}, u32[]{:S(2)}) copy-start(f32[63,512]{1,0:T(8,128)} %get-tuple-element.24) | copy-start | bytes 387076
  196.9 8.9 %copy-start.76 = (f32[1,512]{1,0:T(1,128)S(1)}, f32[1,512]{1,0:T(1,128)}, u32[]{:S(2)}) copy-start(f32[1,512]{1,0:T(1,128)} %slice.2398) | copy-start | bytes 6148
  196.9 53.7 %collective-permute-start.1 = (bf16[1,128]{1,0:T(2,128)(2,1)}, bf16[1,128]{1,0:T(2,128)(2,1)}, u32[]{:S(2)}, u32[]{:S(2)}) collective-permute-start(bf16[1,128]{1,0:T(2,128)(2,1)} %get-tuple-element.186), channel_id=1, source_target_pairs={{4,0},{8,4},{12,8},{16,12},{20,16},{24,20},{28,24},{32,28},{36,32}... | collective-permute-start | bytes 776 | tf_op jit(solution)/shard_map/ppermute | solution.py:45
  204.4 1.5 copy-start.9
  204.4 1.5 copy-start.75
  208.8 4.2 %copy-start.30 = (f32[512]{0:T(512)S(1)}, f32[512]{0:T(512)}, u32[]{:S(2)}) copy-start(f32[512]{0:T(512)} %copy-done.29) | copy-start | bytes 6148
  208.8 4.2 %copy-start.32 = (f32[512]{0:T(512)S(1)}, f32[512]{0:T(512)}, u32[]{:S(2)}) copy-start(f32[512]{0:T(512)} %copy-done.31) | copy-start | bytes 6148
  208.8 4.2 %copy-start.37 = (f32[1,1,512]{2,1,0:T(1,128)S(1)}, f32[1,1,512]{2,1,0:T(1,128)}, u32[]{:S(2)}) copy-start(f32[1,1,512]{2,1,0:T(1,128)} %get-tuple-element.307) | copy-start | bytes 6148
  208.8 4.2 %copy-start.38 = (f32[1,1,512]{2,1,0:T(1,128)S(1)}, f32[1,1,512]{2,1,0:T(1,128)}, u32[]{:S(2)}) copy-start(f32[1,1,512]{2,1,0:T(1,128)} %get-tuple-element.308) | copy-start | bytes 6148
  208.9 21.2 %copy-start.14 = (bf16[128,512]{1,0:T(8,128)(2,1)S(1)}, bf16[128,512]{1,0:T(8,128)(2,1)}, u32[]{:S(2)}) copy-start(bf16[128,512]{1,0:T(8,128)(2,1)} %copy-done.13) | copy-start | bytes 393220
  231.6 17.6 %copy-start.3 = (f32[128,512]{1,0:T(8,128)S(1)}, f32[128,512]{1,0:T(8,128)}, u32[]{:S(2)}) copy-start(f32[128,512]{1,0:T(8,128)} %rev.16) | copy-start | bytes 786436
  232.0 17.1 %copy-start.2 = (f32[512,128]{0,1:T(8,128)S(1)}, f32[512,128]{0,1:T(8,128)}, u32[]{:S(2)}) copy-start(f32[512,128]{0,1:T(8,128)} %reshape.3196) | copy-start | bytes 786436
  249.2 1.0 copy-start.1
  250.1 1.4 copy-start.91
  250.1 1.4 copy-start.92
  250.1 1.4 copy-start.93
  250.1 1.5 copy-start.98
  250.1 1.5 copy-start.99
  (58 other events, 48.0 us)
where the time goes:
time: 265 us; the launch traced here: 263 us
  blocking collectives  101 us (38%)
  other arithmetic  60 us (23%)
  local copies, waits for them, and re-layouts  52.8 us (20%)
  starting transfers between devices  17.4 us (7%)
  between operations  14 us (5%)
  matrix products  9.18 us (3%)
  waiting for transfers between devices  8.38 us (3%)
    all_gather x6, blocking collectives, all_in_one(): both, at, found = (lax.all_gather(jnp.concatenate(lines), axis), 0, {})  90.9 us
    add x2, other arithmetic, per_device(): incoming_re = arrivals[direction][0] + jnp.where(chain_end, start_re, 0.0)  29.8 us
    all_to_all x1, blocking collectives, summed_on_arrival(): lax.all_to_all(parts, axis, split_axis=0, concat_axis=0, tiled=True)  10.5 us
    all_to_all x2, starting transfers between devices, from_everyone(): lax.all_to_all(jnp.broadcast_to(shard[None], (size, *shard.shape)), axis,...  9.39 us
    slice x194, local copies, waits for them, and re-layouts, per_device(): lax.associative_scan(compose_steps, (factor_re, factor_im, push_re, push_...  9.26 us
    slice x14, local copies, waits for them, and re-layouts, entering(): subtotal = combine(subtotal, jax.tree.map(lambda part: part[k], pieces))  8.65 us
    all_to_all x2, waiting for transfers between devices, from_everyone(): lax.all_to_all(jnp.broadcast_to(shard[None], (size, *shard.shape)), axis,...  8.37 us
    mul x3, other arithmetic, advance(): cosine = magnitude * jnp.cos(angle)  8.3 us
  transfers between devices with their start and end apart: 4, of which 1 were waited for; matrix products, arithmetic and copies ran while one was open for 23% of the time, Pallas kernels for 0%

commit v1 on v0

v1 whole, which is shorter than its diff:
```python
import jax
import jax.numpy as jnp
from jax import lax
from jax.experimental import pallas as pl
from jax.experimental.pallas import tpu as pltpu
from jax.sharding import Mesh
from jax.sharding import PartitionSpec as P

D = 2048
SP = ("sp_0", "sp_1", "sp_2")
EPSILON = 1e-06
F32 = jnp.float32
BF16 = jnp.bfloat16
CHUNKS = 8


def sin_cos(angle):
    turns = jnp.floor(angle * 0.6366197723675814 + 0.5)
    rest = ((angle - turns * 1.5703125) - turns * 4.837512969970703125e-4) - turns * 7.54978995489188216e-8
    rest = jnp.clip(rest, -0.8, 0.8)
    square = rest * rest
    sine = rest + rest * square * (
        -1.6666654611e-1 + square * (8.3321608736e-3 - 1.9515295891e-4 * square)
    )
    cosine = 1.0 - 0.5 * square + square * square * (
        4.166664568298827e-2 + square * (-1.388731625493765e-3 + 2.443315711809948e-5 * square)
    )
    quadrant = turns.astype(jnp.int32)
    odd = (quadrant & 1) == 1
    s = jnp.where(odd, cosine, sine)
    c = jnp.where(odd, sine, cosine)
    s = jnp.where((quadrant & 2) == 2, -s, s)
    c = jnp.where(((quadrant + 1) & 2) == 2, -c, c)
    return s, c


def exp_less_one(x):
    series = x * (1.0 + x * (1 / 2 + x * (1 / 6 + x * (1 / 24 + x * (1 / 120 + x * (1 / 720 + x * (1 / 5040 + x * (1 / 40320))))))))
    return jnp.where(x > -0.5, series, jnp.exp(x) - 1.0)


def moved(elapsed, decay, turn):
    magnitude = jnp.exp(-decay * elapsed)
    s, c = sin_cos(turn * elapsed)
    return magnitude * c, magnitude * s


def cmul(ar, ai, br, bi):
    return ar * br - ai * bi, ar * bi + ai * br


def iota(shape, dim):
    return lax.broadcasted_iota(jnp.int32, shape, dim)


def dot(a, b, dims=((1,), (0,))):
    return lax.dot_general(a, b, (dims, ((), ())), preferred_element_type=F32)


def halves(x):
    high = x.astype(BF16)
    return high, (x - high.astype(F32)).astype(BF16)


def scan_chunks(fr, fi, lr, li, backward):
    rows = iota(fr.shape, 0)
    for k in (1, 2, 4):
        shift = CHUNKS - k if backward else k
        outside = rows >= CHUNKS - k if backward else rows < k
        sfr = jnp.where(outside, 1.0, pltpu.roll(fr, shift, 0))
        sfi = jnp.where(outside, 0.0, pltpu.roll(fi, shift, 0))
        if lr is not None:
            slr = jnp.where(outside, 0.0, pltpu.roll(lr, shift, 0))
            sli = jnp.where(outside, 0.0, pltpu.roll(li, shift, 0))
            ar, ai = cmul(fr, fi, slr, sli)
            lr, li = lr + ar, li + ai
        fr, fi = cmul(fr, fi, sfr, sfi)
    return fr, fi, lr, li


def one_later(x, backward, fill):
    rows = iota(x.shape, 0)
    if backward:
        return jnp.where(rows == CHUNKS - 1, fill, pltpu.roll(x, CHUNKS - 1, 0))
    return jnp.where(rows == 0, fill, pltpu.roll(x, 1, 0))


def pack_kernel(stream, gain, out):
    n = stream.shape[0]
    per = n // CHUNKS
    row, col = iota((n, n), 0), iota((n, n), 1)
    order = jnp.where(col == (row % CHUNKS) * per + row // CHUNKS, 1.0, 0.0).astype(BF16)
    x = dot(order, stream[...]).astype(BF16)
    g = gain[...]
    high = g.astype(BF16)
    left = g - high.astype(F32)
    mid = left.astype(BF16)
    low = (left - mid.astype(F32)).astype(BF16)
    row = iota((16, g.shape[1]), 0)
    tail = jnp.where(row == 0, high.astype(F32), jnp.where(row == 1, mid.astype(F32), jnp.where(row == 2, low.astype(F32), 0.0)))
    tail = tail.astype(BF16)
    for k in range(out.shape[0]):
        out[k, 0:n, :] = x
        out[k, n : n + 16, :] = tail


def prepare_kernel(intervals, decay, turn, in_re, in_im, rd_re, rd_im, fr_o, fi_o, gr_o, gi_o, pr_o, pi_o, br_o, bi_o, in_hi, in_lo, rd_hi, rd_lo, total):
    n = intervals.shape[1]
    per = n // CHUNKS
    row, col = iota((n, n), 0), iota((n, n), 1)
    steps = jnp.sum(jnp.where(col == (row % CHUNKS) * per + row // CHUNKS, intervals[...], 0.0), axis=1, keepdims=True)
    total[...] = jnp.broadcast_to(jnp.sum(intervals[...], axis=1, keepdims=True), total.shape)
    width = decay.shape[1]
    half = width // 2
    for tile in range(width // 128):
        lanes = slice(tile * 128, tile * 128 + 128)
        rate, turning = decay[:, lanes], turn[:, lanes]
        damping = -rate * steps
        s, c = sin_cos(0.5 * (turning * steps))
        magnitude = jnp.exp(damping)
        twice = 2.0 * s * s
        cosine = 1.0 - twice
        fr = magnitude * cosine
        fi = magnitude * (2.0 * s * c)
        lift = exp_less_one(damping) * cosine - twice
        inverse = 1.0 / (rate * rate + turning * turning)
        fr_o[:, lanes] = fr
        fi_o[:, lanes] = fi
        gr_o[:, lanes] = (turning * fi - rate * lift) * inverse
        gi_o[:, lanes] = -(rate * fi + turning * lift) * inverse
        backward = tile * 128 >= half
        cr = ci = None
        for i in reversed(range(per)) if backward else range(per):
            at = slice(i * CHUNKS, i * CHUNKS + CHUNKS)
            r, m = fr[at], fi[at]
            cr, ci = (r, m) if cr is None else cmul(r, m, cr, ci)
            pr_o[at, lanes] = cr
            pi_o[at, lanes] = ci
        br, bi, _, _ = scan_chunks(cr, ci, None, None, backward)
        br_o[:, lanes] = one_later(br, backward, 1.0)
        bi_o[:, lanes] = one_later(bi, backward, 0.0)
    channels = rd_re.shape[0] // 2
    groups = half // rd_re.shape[1]
    wide = channels // groups
    states = rd_re.shape[1]
    spread = jnp.where(iota((wide, channels), 1) % wide == iota((wide, channels), 0), 1.0, 0.0).astype(BF16)
    mine = iota((channels, width), 0) // wide == (iota((channels, width), 1) % half) // states
    for at, ref in enumerate((in_re, in_im)):
        for piece, out in zip(halves(ref[...]), (in_hi, in_lo)):
            full = dot(spread, piece, ((0,), (1,)))
            out[:, at * width : (at + 1) * width] = jnp.where(mine, full, 0.0).astype(BF16)
    spread = jnp.where(iota((states, half), 1) % states == iota((states, half), 0), 1.0, 0.0).astype(BF16)
    mine = iota((half, channels), 0) // states == iota((half, channels), 1) // wide
    for at, ref in enumerate((rd_re, rd_im)):
        for d in range(2):
            both = ref[d * channels : (d + 1) * channels, :]
            both = -both if at == 1 else both
            for piece, out in zip(halves(both), (rd_hi, rd_lo)):
                full = dot(spread, piece, ((0,), (1,)))
                place = at * width + d * half
                out[place : place + half, :] = jnp.where(mine, full, 0.0).astype(BF16)


def local_kernel(rows, w_value, w_mix, w_gate, w_state, fr, fi, gr, gi, pr, pi, in_hi, in_lo, total, hr_o, hi_o, cr_o, ci_o, source_o, gate_o, input_o, message):
    parts, n, share = rows.shape[0], rows.shape[1] - 16, rows.shape[2]
    per = n // CHUNKS
    squares = 0.0
    for k in range(parts):
        x = rows[k, 0:n, :].astype(F32)
        squares = squares + jnp.sum(x * x, axis=1, keepdims=True)
    inv_rms = lax.rsqrt(squares / D + EPSILON)
    value = mix = gate = state = 0.0
    for k in range(parts):
        tail = rows[k, n : n + 16, :].astype(F32)
        gain = (tail[0:1] + tail[1:2]) + tail[2:3]
        normed = ((rows[k, 0:n, :].astype(F32) * inv_rms) * gain).astype(BF16)
        at = slice(k * share, k * share + share)
        value = value + dot(normed, w_value[at, :])
        mix = mix + dot(normed, w_mix[at, :])
        gate = gate + dot(normed, w_gate[at, :])
        state = state + dot(normed, w_state[at, :])
    source = (mix.astype(BF16).astype(F32) * value.astype(BF16).astype(F32)).astype(BF16).astype(F32)
    source_o[...] = source
    gate_o[...] = gate.astype(BF16).astype(F32)
    state = state.astype(BF16)
    input_o[...] = state.astype(F32)
    width = fr.shape[1]
    half = width // 2
    edges = []
    for tile in range(width // 128):
        lanes = slice(tile * 128, tile * 128 + 128)
        other = slice(width + tile * 128, width + tile * 128 + 128)
        driven_re = dot(state, in_hi[:, lanes]) + dot(state, in_lo[:, lanes])
        driven_im = dot(state, in_hi[:, other]) + dot(state, in_lo[:, other])
        push_re, push_im = cmul(gr[:, lanes], gi[:, lanes], driven_re, driven_im)
        backward = tile * 128 >= half
        hr = hi = None
        for i in reversed(range(per)) if backward else range(per):
            at = slice(i * CHUNKS, i * CHUNKS + CHUNKS)
            if hr is None:
                hr, hi = push_re[at], push_im[at]
            else:
                ar, ai = cmul(fr[at, lanes], fi[at, lanes], hr, hi)
                hr, hi = ar + push_re[at], ai + push_im[at]
            hr_o[at, lanes] = hr
            hi_o[at, lanes] = hi
        end = slice(0, CHUNKS) if backward else slice(n - CHUNKS, n)
        _, _, lr, li = scan_chunks(pr[end, lanes], pi[end, lanes], hr, hi, backward)
        cr_o[:, lanes] = one_later(lr, backward, 0.0)
        ci_o[:, lanes] = one_later(li, backward, 0.0)
        edge = 0 if backward else CHUNKS - 1
        edges.append((lr[edge : edge + 1], li[edge : edge + 1]))
    for k in range(message.shape[0]):
        for tile, (r, m) in enumerate(edges):
            message[k, tile : tile + 1, :] = r
            message[k, 8 + tile : 9 + tile, :] = m
        message[k, 16:17, :] = total[0:1, :]
        message[k, 17:18, :] = source[0:1]
        message[k, 18:19, :] = source[n - 1 : n]
        message[k, 19:24, :] = jnp.zeros((5, 128), F32)


def plane_kernel(place, got, decay, turn, inner, message):
    size = got.shape[0]
    here, plane = place[0], place[1]
    rate, turning = decay[...], turn[...]
    forward = iota((8, 128), 0) < 4
    hr = hi = spent = jnp.zeros((8, 128), F32)
    ir = ii = before = hr
    for k in range(size):
        m = size - 1 - k
        mine = (forward & (here == k)) | (jnp.logical_not(forward) & (here == m))
        ir = jnp.where(mine, hr, ir)
        ii = jnp.where(mine, hi, ii)
        before = jnp.where(mine, spent, before)
        elapsed = jnp.where(forward, got[k, 16:17, :], got[m, 16:17, :])
        ar, ai = moved(elapsed, rate, turning)
        ar, ai = cmul(ar, ai, hr, hi)
        hr = ar + jnp.where(forward, got[k, 0:8, :], got[m, 0:8, :])
        hi = ai + jnp.where(forward, got[k, 8:16, :], got[m, 8:16, :])
        spent = spent + elapsed
    wr, wi = moved(before, rate, turning)
    inner[0:8, :] = ir
    inner[8:16, :] = ii
    inner[16:24, :] = wr
    inner[24:32, :] = wi
    previous = following = jnp.zeros((1, 128), F32)
    for k in range(size):
        previous = jnp.where(here - 1 == k, got[k, 18:19, :], previous)
        following = jnp.where(here + 1 == k, got[k, 17:18, :], following)
    inner[32:40, :] = jnp.broadcast_to(previous, (8, 128))
    inner[40:48, :] = jnp.broadcast_to(following, (8, 128))
    swapped = pltpu.roll(hi, 4, 0)
    later = jnp.where(forward, hr, swapped)
    earlier = jnp.where(forward, swapped, hr)
    row = iota((8, 128), 0)
    note_later = jnp.where(row == 0, spent, jnp.where(row == 1, got[size - 1, 18:19, :], 0.0))
    note_earlier = jnp.where(row == 0, spent, jnp.where(row == 1, got[0, 17:18, :], 0.0))
    for k in range(message.shape[0]):
        message[k, 0:8, :] = jnp.where(plane < k, later, earlier)
        message[k, 8:16, :] = jnp.where(plane < k, note_later, note_earlier)


def finish_kernel(place, got, inner, decay, turn, init_re, init_im, hr_i, hi_i, cr_i, ci_i, pr, pi, br, bi, rd_hi, rd_lo, source, gate, state, taps, skip, proj_conv, proj_state, out):
    size = got.shape[0]
    here, plane, last = place[0], place[1], place[2]
    rate, turning = decay[...], turn[...]
    forward = iota((8, 128), 0) < 4
    hr, hi = init_re[...], init_im[...]
    for k in range(size):
        m = size - 1 - k
        active = (forward & (plane > k)) | (jnp.logical_not(forward) & (plane < m))
        elapsed = jnp.where(forward, got[k, 8:9, :], got[m, 8:9, :])
        ar, ai = moved(elapsed, rate, turning)
        ar, ai = cmul(ar, ai, hr, hi)
        a, b = got[k, 0:8, :], got[m, 0:8, :]
        hr = jnp.where(active, ar + jnp.where(forward, a, b), hr)
        hi = jnp.where(active, ai + pltpu.roll(jnp.where(forward, b, a), 4, 0), hi)
    ar, ai = cmul(inner[16:24, :], inner[24:32, :], hr, hi)
    inc_re = ar + inner[0:8, :]
    inc_im = ai + inner[8:16, :]
    n, width = hr_i.shape
    per = n // CHUNKS
    response = state[...] * skip[...]
    for tile in range(width // 128):
        lanes = slice(tile * 128, tile * 128 + 128)
        er, ei = cmul(br[:, lanes], bi[:, lanes], inc_re[tile : tile + 1], inc_im[tile : tile + 1])
        er = er + cr_i[:, lanes]
        ei = ei + ci_i[:, lanes]
        er = jnp.concatenate([er] * per, axis=0)
        ei = jnp.concatenate([ei] * per, axis=0)
        ar, ai = cmul(pr[:, lanes], pi[:, lanes], er, ei)
        full = jnp.concatenate([ar + hr_i[:, lanes], ai + hi_i[:, lanes]], axis=1)
        high, low = halves(full)
        other = slice(width + tile * 128, width + tile * 128 + 128)
        r_hi = jnp.concatenate([rd_hi[lanes, :], rd_hi[other, :]], axis=0)
        r_lo = jnp.concatenate([rd_lo[lanes, :], rd_lo[other, :]], axis=0)
        response = response + ((dot(low, r_hi) + dot(high, r_lo)) + dot(high, r_hi))
    state_out = jax.nn.gelu(response).astype(BF16)
    previous, following = inner[32:33, :], inner[40:41, :]
    for k in range(size):
        previous = jnp.where((here == 0) & (plane - 1 == k), got[k, 9:10, :], previous)
        following = jnp.where((here == last) & (plane + 1 == k), got[k, 9:10, :], following)
    x = source[...]
    row = iota((CHUNKS, x.shape[1]), 0)
    head = jnp.where(row == 0, previous, pltpu.roll(x[n - CHUNKS :], 1, 0))
    foot = jnp.where(row == CHUNKS - 1, following, pltpu.roll(x[:CHUNKS], CHUNKS - 1, 0))
    before = jnp.concatenate([head, x[: n - CHUNKS]], axis=0)
    after = jnp.concatenate([x[CHUNKS:], foot], axis=0)
    filtered = taps[0:1, :] * before + taps[1:2, :] * x + taps[2:3, :] * after
    conv_out = (gate[...] * filtered).astype(BF16)
    row, col = iota((n, n), 0), iota((n, n), 1)
    order = jnp.where(row == (col % CHUNKS) * per + col // CHUNKS, 1.0, 0.0).astype(BF16)
    conv_out = dot(order, conv_out).astype(BF16)
    state_out = dot(order, state_out).astype(BF16)
    share = out.shape[2]
    for k in range(out.shape[0]):
        at = slice(k * share, k * share + share)
        out[k] = (dot(conv_out, proj_conv[:, at]) + dot(state_out, proj_state[:, at])).astype(BF16)


def exchange(x, axis):
    return lax.all_to_all(x, axis, split_axis=0, concat_axis=0, tiled=True)


VMEM = pl.BlockSpec(memory_space=pltpu.VMEM)
SMEM = pl.BlockSpec(memory_space=pltpu.SMEM)


def call(kernel, shapes, *args, scalars=0, flops=10**7, name=None):
    return pl.pallas_call(
        kernel,
        out_shape=[jax.ShapeDtypeStruct(s, d) for s, d in shapes],
        in_specs=[SMEM] * scalars + [VMEM] * (len(args) - scalars),
        out_specs=[VMEM] * len(shapes),
        compiler_params=pltpu.CompilerParams(vmem_limit_bytes=24 * 2**20),
        cost_estimate=pl.CostEstimate(flops=flops, bytes_accessed=10**6, transcendentals=0),
        name=name,
    )(*args)


def per_device(
    stream,
    norm_gain,
    w_value,
    w_mix,
    w_gate,
    w_state,
    conv_taps,
    skip_gain,
    decay_rate,
    turn_rate,
    input_real,
    input_imag,
    read_real,
    read_imag,
    initial_state,
    intervals,
    proj_conv,
    proj_state,
):
    n, share = stream.shape
    parts = lax.axis_size("tp")
    inner_axes = SP[1:]
    inside = lax.axis_size(inner_axes)
    planes = lax.axis_size(SP[0])
    channels = w_value.shape[1]
    width = decay_rate.size
    here = lax.axis_index(inner_axes)
    plane = lax.axis_index(SP[0])
    place = jnp.stack([here, plane, jnp.full_like(here, inside - 1)]).astype(jnp.int32)

    (packed,) = call(pack_kernel, [((parts, n + 16, share), BF16)], stream, norm_gain.reshape(1, -1), name="pack")
    rows = exchange(packed, "tp")

    states = (n, width)
    table = call(
        prepare_kernel,
        [(states, F32)] * 6
        + [((CHUNKS, width), F32)] * 2
        + [((channels, 2 * width), BF16)] * 2
        + [((2 * width, channels), BF16)] * 2
        + [((8, 128), F32)],
        intervals.reshape(1, n),
        decay_rate.reshape(1, width),
        turn_rate.reshape(1, width),
        input_real.reshape(width, -1),
        input_imag.reshape(width, -1),
        read_real.reshape(2 * channels, -1),
        read_imag.reshape(2 * channels, -1),
        flops=3 * 10**9,
        name="prepare",
    )
    fr, fi, gr, gi, pr, pi, br, bi, in_hi, in_lo, rd_hi, rd_lo, total = table

    hr, hi, cr, ci, source, gate, state, message = call(
        local_kernel,
        [(states, F32)] * 2
        + [((CHUNKS, width), F32)] * 2
        + [((n, channels), F32)] * 3
        + [((inside, 24, 128), F32)],
        rows, w_value, w_mix, w_gate, w_state, fr, fi, gr, gi, pr, pi, in_hi, in_lo, total,
        name="local",
    )
    decay = decay_rate.reshape(8, 128)
    turn = turn_rate.reshape(8, 128)
    inner, message = call(
        plane_kernel,
        [((48, 128), F32), ((planes, 16, 128), F32)],
        place, exchange(message, inner_axes), decay, turn,
        scalars=1,
        name="plane",
    )
    got = exchange(message, SP[0])
    (partial,) = call(
        finish_kernel,
        [((parts, n, share), BF16)],
        place, got, inner, decay, turn,
        initial_state[:, 0].reshape(8, 128), initial_state[:, 1].reshape(8, 128),
        hr, hi, cr, ci, pr, pi, br, bi, rd_hi, rd_lo, source, gate, state,
        conv_taps, skip_gain.reshape(1, -1), proj_conv, proj_state,
        scalars=1,
        name="finish",
    )
    arrived = exchange(partial, "tp")
    return arrived.astype(F32).sum(axis=0).astype(BF16)


def solution(mesh):
    finer = Mesh(mesh.devices.reshape(16, 4, 2, mesh.shape["tp"]), ("sp_0", "sp_1", "sp_2", "tp"))
    return jax.shard_map(
        per_device,
        mesh=finer,
        in_specs=(
            P(SP, "tp"),
            P("tp"),
            P(None, "tp"),
            P(None, "tp"),
            P(None, "tp"),
            P(None, "tp"),
            P(None, "tp"),
            P("tp"),
            P(None, "tp", None),
            P(None, "tp", None),
            P(None, "tp", None, None),
            P(None, "tp", None, None),
            P(None, "tp", None, None),
            P(None, "tp", None, None),
            P(None, None, "tp", None),
            P(SP),
            P("tp", None),
            P("tp", None),
        ),
        out_specs=P(SP, "tp"),
        check_vma=False,
    )
```

time: 265 us -> 96.7 us (0.36)
  blocking collectives: 101 us -> 12.7 us
  other arithmetic: 60 us -> 0.82 us
  local copies, waits for them, and re-layouts: 52.8 us -> 29.6 us
  between operations: 14 us -> 0.09 us
  waiting for transfers between devices: 8.38 us -> 19.5 us
  matrix products: 9.18 us -> 0 us
  Pallas kernels: 0 us -> 8.44 us
  starting transfers between devices: 17.4 us -> 24.4 us
    all_gather x6 -> x0, blocking collectives: 90.9 us -> none  [all_in_one(): both, at, found = (lax.all_gather(jnp.concatenate(lines), axis), 0, {})]
    add x101 -> x0, other arithmetic: 39.5 us -> none  [the longest x2 29.8 us: per_device(): incoming_re = arrivals[direction][0] + jnp.where(chain_end, start_re, 0.0)]
    unnamed x210 -> x82, local copies, waits for them, and re-layouts: 7.65 us -> 29.1 us
    slice x215 -> x1, local copies, waits for them, and re-layouts: 20.5 us -> 0.01 us  [per_device(): initial_state[:, 1].reshape(8, 128)]
    all_to_all x2 -> x3, starting transfers between devices: 9.39 us -> 24.4 us  [exchange(): return lax.all_to_all(x, axis, split_axis=0, concat_axis=0, tiled=True)]
    mul x5 -> x0, other arithmetic: 12.2 us -> none  [the longest x3 8.3 us: advance(): cosine = magnitude * jnp.cos(angle)]
    all_to_all x2 -> x3, waiting for transfers between devices: 8.37 us -> 19.5 us  [exchange(): return lax.all_to_all(x, axis, split_axis=0, concat_axis=0, tiled=True)]
    dot_general x10 -> x0, matrix products: 9.18 us -> none  [the longest x2 4.46 us: per_device(): jnp.dot(state_float, spread_input(input_real[direction], identity_map), p...]
  transfers between devices with their start and end apart: 4 -> 3, of which waited for: 1 -> 2; matrix products, arithmetic and copies ran while one was open for 23% -> 3% of each run, Pallas kernels for 0% -> 2%
where the time goes in v1:
time: 96.7 us; the launch traced here: 95.5 us
  local copies, waits for them, and re-layouts  29.6 us (31%)
  starting transfers between devices  24.4 us (25%)
  waiting for transfers between devices  19.5 us (20%)
  blocking collectives  12.7 us (13%)
  Pallas kernels  8.44 us (9%)
    unnamed x82, local copies, waits for them, and re-layouts  29.1 us
    all_to_all x3, starting transfers between devices, exchange(): return lax.all_to_all(x, axis, split_axis=0, concat_axis=0, tiled=True)  24.4 us
    all_to_all x3, waiting for transfers between devices, exchange(): return lax.all_to_all(x, axis, split_axis=0, concat_axis=0, tiled=True)  19.5 us
    all_to_all x1, blocking collectives, exchange(): return lax.all_to_all(x, axis, split_axis=0, concat_axis=0, tiled=True)  12.7 us
    pallas_call x5, Pallas kernels, call(): pl.pallas_call(kernel, out_shape=[jax.ShapeDtypeStruct(s, d) for s, d in...  8.44 us
  transfers between devices with their start and end apart: 3, of which 2 were waited for; matrix products, arithmetic and copies ran while one was open for 3% of the time, Pallas kernels for 2%

profile of v1, /device:TPU:32, one launch (start us, length us, event | category | flops | bytes accessed | tf_op | source)
XLA Modules:
  0.0 95.5 jit_solution(2398099634475405434)
XLA Ops:
  0.0 0.9 copy-done.28
  0.9 0.7 copy-done.29
  1.6 1.0 %pack.1 = bf16[4,144,512]{2,1,0:T(8,128)(2,1)} custom-call(bf16[128,512]{1,0:T(8,128)(2,1)S(1)} %copy-done.28, f32[1,512]{1,0:T(1,128)S(1)} %bitcast.15), custom_call_target="tpu_custom_call" | custom-call | flops 10000000 | bytes 1000000 | tf_op jit(solution)/shard_map/pack/pallas_call | solution.py:331
  2.6 4.6 %all-to-all-start = ((bf16[4,144,512]{2,1,0:T(8,128)(2,1)}), bf16[4,144,512]{2,1,0:T(8,128)(2,1)S(1)}, u32[]{:S(2)}, u32[]{:S(2)}) async-start(bf16[4,144,512]{2,1,0:T(8,128)(2,1)} %pack.1), calls=%async_computation | async-start | bytes 1179648 | tf_op jit(solution)/shard_map/all_to_all | solution.py:323
  7.2 0.1 reshape.35.decay
  7.3 0.6 copy-done.38
  8.0 0.1 reshape.36.turn
  8.1 1.0 %copy.19 = f32[2,8,64,16]{3,2,1,0:T(8,128)} copy(f32[2,8,64,16]{2,3,1,0:T(8,128)S(1)} %copy-done.35) | data formatting | bytes 131072 | tf_op args[10]
  9.1 1.0 %copy.20 = f32[2,8,64,16]{3,2,1,0:T(8,128)} copy(f32[2,8,64,16]{2,3,1,0:T(8,128)S(1)} %copy-done.36) | data formatting | bytes 131072 | tf_op args[11]
  10.2 0.7 copy-done.34
  10.8 1.0 %copy-done.16 = f32[2,8,64,16]{3,2,1,0:T(8,128)S(1)} copy-done((f32[2,8,64,16]{3,2,1,0:T(8,128)S(1)}, f32[2,8,64,16]{3,2,1,0:T(8,128)}, u32[]{:S(2)}) %copy-start.16) | copy-done | bytes 65560
  11.9 1.0 %copy-done.17 = f32[2,8,64,16]{3,2,1,0:T(8,128)S(1)} copy-done((f32[2,8,64,16]{3,2,1,0:T(8,128)S(1)}, f32[2,8,64,16]{3,2,1,0:T(8,128)}, u32[]{:S(2)}) %copy-start.17) | copy-done | bytes 65560
  12.9 0.9 copy-done.33
  13.8 2.3 %prepare.1 = (f32[128,1024]{1,0:T(8,128)S(1)}, f32[128,1024]{1,0:T(8,128)S(1)}, f32[128,1024]{1,0:T(8,128)S(1)}, f32[128,1024]{1,0:T(8,128)S(1)}, f32[128,1024]{...) custom-call(f32[1,128]{1,0:T(1,128)S(1)} %bitcast.19, ...), custom_call_target="tpu_custom_call" | custom-call | flops 3000000000 | bytes 1000000 | tf_op jit(solution)/shard_map/prepare/pallas_call | solution.py:331
  16.1 0.8 copy-done.4
  16.9 0.8 copy-done.6
  17.7 0.8 copy-done.8
  18.5 0.8 copy-done.10
  19.3 0.8 copy-done.12
  20.1 0.8 copy-done.14
  20.9 0.8 copy-done.20
  21.7 0.8 copy-done.22
  22.6 1.0 %copy-done.3 = bf16[2048,128]{1,0:T(8,128)(2,1)S(1)} copy-done((bf16[2048,128]{1,0:T(8,128)(2,1)S(1)}, bf16[2048,128]{1,0:T(8,128)(2,1)}, u32[]{:S(2)}) %copy-start.3) | copy-done | bytes 524312
  23.6 1.0 %copy-done.5 = f32[128,1024]{1,0:T(8,128)S(1)} copy-done((f32[128,1024]{1,0:T(8,128)S(1)}, f32[128,1024]{1,0:T(8,128)}, u32[]{:S(2)}) %copy-start.5) | copy-done | bytes 524312
  24.6 1.0 %copy-done.7 = f32[128,1024]{1,0:T(8,128)S(1)} copy-done((f32[128,1024]{1,0:T(8,128)S(1)}, f32[128,1024]{1,0:T(8,128)}, u32[]{:S(2)}) %copy-start.7) | copy-done | bytes 524312
  25.7 1.0 %copy-done.9 = f32[128,1024]{1,0:T(8,128)S(1)} copy-done((f32[128,1024]{1,0:T(8,128)S(1)}, f32[128,1024]{1,0:T(8,128)}, u32[]{:S(2)}) %copy-start.9) | copy-done | bytes 524312
  26.7 1.0 %copy-done.11 = f32[128,1024]{1,0:T(8,128)S(1)} copy-done((f32[128,1024]{1,0:T(8,128)S(1)}, f32[128,1024]{1,0:T(8,128)}, u32[]{:S(2)}) %copy-start.11) | copy-done | bytes 524312
  27.8 1.0 %copy-done.13 = bf16[128,2048]{1,0:T(8,128)(2,1)S(1)} copy-done((bf16[128,2048]{1,0:T(8,128)(2,1)S(1)}, bf16[128,2048]{1,0:T(8,128)(2,1)}, u32[]{:S(2)}) %copy-start.13) | copy-done | bytes 524312
  28.8 1.0 %copy-done.15 = bf16[128,2048]{1,0:T(8,128)(2,1)S(1)} copy-done((bf16[128,2048]{1,0:T(8,128)(2,1)S(1)}, bf16[128,2048]{1,0:T(8,128)(2,1)}, u32[]{:S(2)}) %copy-start.15) | copy-done | bytes 524312
  29.8 2.1 %local.1 = (f32[128,1024]{1,0:T(8,128)S(1)}, f32[128,1024]{1,0:T(8,128)S(1)}, f32[8,1024]{1,0:T(8,128)S(1)}, f32[8,1024]{1,0:T(8,128)S(1)}, f32[128,128]{1,0:T(8...) custom-call(bf16[4,144,512]{2,1,0:T(8,128)(2,1)S(1)} %all-to-all-done.rows, ...), custom_call_target="tpu_custom_call" | custom-call | flops 10000000 | bytes 1000000 | tf_op jit(solution)/shard_map/local/pallas_call | solution.py:331
  31.9 0.8 copy-done.24
  32.7 0.8 copy-done.26
  33.5 4.4 %all-to-all-start.1 = ((f32[8,24,128]{2,1,0:T(8,128)}), f32[8,24,128]{2,1,0:T(8,128)S(1)}, u32[]{:S(2)}, u32[]{:S(2)}) async-start(f32[8,24,128]{2,1,0:T(8,128)} %get-tuple-element.37), calls=%async_computation.1 | async-start | bytes 196608 | tf_op jit(solution)/shard_map/all_to_all | solution.py:323
  38.0 0.1 pad_add_fusion.place
  38.1 5.7 %all-to-all-done.1.got = f32[8,24,128]{2,1,0:T(8,128)S(1)} async-done(((f32[8,24,128]{2,1,0:T(8,128)}), f32[8,24,128]{2,1,0:T(8,128)S(1)}, u32[]{:S(2)}, u32[]{:S(2)}) %all-to-all-start.1) | async-done | bytes 98336 | tf_op jit(solution)/shard_map/all_to_all | solution.py:323
  43.8 1.3 %plane.1 = (f32[48,128]{1,0:T(8,128)S(1)}, f32[16,16,128]{2,1,0:T(8,128)}) custom-call(s32[3]{0:T(128)S(1)} %pad_add_fusion.place, f32[8,24,128]{2,1,0:T(8,128)S(1)} %all-to-all-done.1.got, f32[8,128]{1,0:T(8,128)S(1)} %reshape.41.decay, f32[8,128]{1,0:T(8,128)S(1)} %reshape.42.turn), custom_call_target="tpu_custom_call" | custom-call | flops 10000000 | bytes 1000000 | tf_op jit(solution)/shard_map/plane/pallas_call | solution.py:331
  45.1 15.3 %all-to-all-start.2 = ((f32[16,16,128]{2,1,0:T(8,128)}), f32[16,16,128]{2,1,0:T(8,128)S(1)}, u32[]{:S(2)}, u32[]{:S(2)}) async-start(f32[16,16,128]{2,1,0:T(8,128)} %get-tuple-element.38), calls=%async_computation.2 | async-start | bytes 262144 | tf_op jit(solution)/shard_map/all_to_all | solution.py:323
  60.4 0.1 reshape_squeeze.6.init_re
  60.6 13.8 %all-to-all-done.2.got = f32[16,16,128]{2,1,0:T(8,128)S(1)} async-done(((f32[16,16,128]{2,1,0:T(8,128)}), f32[16,16,128]{2,1,0:T(8,128)S(1)}, u32[]{:S(2)}, u32[]{:S(2)}) %all-to-all-start.2) | async-done | bytes 131104 | tf_op jit(solution)/shard_map/all_to_all | solution.py:323
  74.3 0.7 copy-done.30
  75.0 1.0 %copy-done.19 = bf16[128,2048]{1,0:T(8,128)(2,1)S(1)} copy-done((bf16[128,2048]{1,0:T(8,128)(2,1)S(1)}, bf16[128,2048]{1,0:T(8,128)(2,1)}, u32[]{:S(2)}) %copy-start.19) | copy-done | bytes 524312
  76.1 1.0 %copy-done.21 = bf16[2048,128]{1,0:T(8,128)(2,1)S(1)} copy-done((bf16[2048,128]{1,0:T(8,128)(2,1)S(1)}, bf16[2048,128]{1,0:T(8,128)(2,1)}, u32[]{:S(2)}) %copy-start.21) | copy-done | bytes 524312
  77.1 1.0 %copy-done.23 = bf16[2048,128]{1,0:T(8,128)(2,1)S(1)} copy-done((bf16[2048,128]{1,0:T(8,128)(2,1)S(1)}, bf16[2048,128]{1,0:T(8,128)(2,1)}, u32[]{:S(2)}) %copy-start.23) | copy-done | bytes 524312
  78.1 1.0 %copy-done.25 = f32[128,1024]{1,0:T(8,128)S(1)} copy-done((f32[128,1024]{1,0:T(8,128)S(1)}, f32[128,1024]{1,0:T(8,128)}, u32[]{:S(2)}) %copy-start.25) | copy-done | bytes 524312
  79.2 1.0 %copy-done.27 = f32[128,1024]{1,0:T(8,128)S(1)} copy-done((f32[128,1024]{1,0:T(8,128)S(1)}, f32[128,1024]{1,0:T(8,128)}, u32[]{:S(2)}) %copy-start.27) | copy-done | bytes 524312
  80.2 1.8 %finish.1 = bf16[4,128,512]{2,1,0:T(8,128)(2,1)S(1)} custom-call(s32[3]{0:T(128)S(1)} %pad_add_fusion.place, f32[16,16,128]{2,1,0:T(8,128)S(1)} %all-to-all-done.2.got, f32[48,128]{1,0:T(8,128)S(1)} %get-tuple-element.39.inner, f32[8,128]{1,0:T(8,128)S(1)} %reshape.41.decay, f32[8,128]{1,0:T(8,128)S(1)} %reshape.42.turn, ...), custom_call_target="tpu_custom_call" | custom-call | flops 10000000 | bytes 1000000 | tf_op jit(solution)/shard_map/finish/pallas_call | solution.py:331
  82.0 12.7 %all_to_all.20 = bf16[4,128,512]{2,1,0:T(8,128)(2,1)S(1)} all-to-all(bf16[4,128,512]{2,1,0:T(8,128)(2,1)S(1)} %finish.1), channel_id=1, replica_groups=mesh['sp_0'=16,'sp_1'=4,'sp_2'=2,'tp'=4] {'tp'}, dimensions={0} | all-to-all | bytes 1048576 | tf_op jit(solution)/shard_map/all_to_all | solution.py:323
  94.7 0.7 reduce_sum.12
  (55 shorter events, 0.3 us)
Async XLA Ops:
  0.0 0.9 copy-start.28
  0.9 0.7 copy-start.29
  2.6 4.6 %copy-start.37 = (f32[2,8,64]{2,1,0:T(8,128)S(1)}, f32[2,8,64]{2,1,0:T(8,128)}, u32[]{:S(2)}) copy-start(f32[2,8,64]{2,1,0:T(8,128)} %param.26) | copy-start | bytes 12292
  2.6 5.5 %copy-start.35 = (f32[2,8,64,16]{2,3,1,0:T(8,128)S(1)}, f32[2,8,64,16]{2,3,1,0:T(8,128)}, u32[]{:S(2)}) copy-start(f32[2,8,64,16]{2,3,1,0:T(8,128)} %param.28) | copy-start | bytes 196612
  2.6 19.9 %all-to-all-start = ((bf16[4,144,512]{2,1,0:T(8,128)(2,1)}), bf16[4,144,512]{2,1,0:T(8,128)(2,1)S(1)}, u32[]{:S(2)}, u32[]{:S(2)}) async-start(bf16[4,144,512]{2,1,0:T(8,128)(2,1)} %pack.1), calls=%async_computation | async-start | bytes 1179648 | tf_op jit(solution)/shard_map/all_to_all | solution.py:323
  7.3 0.7 copy-start.38
  8.1 1.0 %copy-start.36 = (f32[2,8,64,16]{2,3,1,0:T(8,128)S(1)}, f32[2,8,64,16]{2,3,1,0:T(8,128)}, u32[]{:S(2)}) copy-start(f32[2,8,64,16]{2,3,1,0:T(8,128)} %param.29) | copy-start | bytes 196612
  9.1 1.0 %copy-start.32 = (f32[2,8,16,64]{3,2,1,0:T(8,128)S(1)}, f32[2,8,16,64]{3,2,1,0:T(8,128)}, u32[]{:S(2)}) copy-start(f32[2,8,16,64]{3,2,1,0:T(8,128)} %param.30) | copy-start | bytes 196612
  10.2 0.7 copy-start.34
  10.8 1.0 %copy-start.16 = (f32[2,8,64,16]{3,2,1,0:T(8,128)S(1)}, f32[2,8,64,16]{3,2,1,0:T(8,128)}, u32[]{:S(2)}) copy-start(f32[2,8,64,16]{3,2,1,0:T(8,128)} %copy.19) | copy-start | bytes 196612
  11.9 1.0 %copy-start.17 = (f32[2,8,64,16]{3,2,1,0:T(8,128)S(1)}, f32[2,8,64,16]{3,2,1,0:T(8,128)}, u32[]{:S(2)}) copy-start(f32[2,8,64,16]{3,2,1,0:T(8,128)} %copy.20) | copy-start | bytes 196612
  12.9 0.9 copy-start.33
  13.8 8.7 %copy-start = (bf16[2048,128]{1,0:T(8,128)(2,1)S(1)}, bf16[2048,128]{1,0:T(8,128)(2,1)}, u32[]{:S(2)}) copy-start(bf16[2048,128]{1,0:T(8,128)(2,1)} %w_value.1) | copy-start | bytes 1572868
  13.8 8.7 %copy-start.1 = (bf16[2048,128]{1,0:T(8,128)(2,1)S(1)}, bf16[2048,128]{1,0:T(8,128)(2,1)}, u32[]{:S(2)}) copy-start(bf16[2048,128]{1,0:T(8,128)(2,1)} %w_mix.1) | copy-start | bytes 1572868
  13.8 8.7 %copy-start.2 = (bf16[2048,128]{1,0:T(8,128)(2,1)S(1)}, bf16[2048,128]{1,0:T(8,128)(2,1)}, u32[]{:S(2)}) copy-start(bf16[2048,128]{1,0:T(8,128)(2,1)} %w_gate.1) | copy-start | bytes 1572868
  16.1 0.8 copy-start.4
  16.9 0.8 copy-start.6
  17.7 0.8 copy-start.8
  18.5 0.8 copy-start.10
  19.3 0.8 copy-start.12
  20.1 0.8 copy-start.14
  20.9 0.8 copy-start.20
  21.7 0.8 copy-start.22
  22.6 1.0 %copy-start.3 = (bf16[2048,128]{1,0:T(8,128)(2,1)S(1)}, bf16[2048,128]{1,0:T(8,128)(2,1)}, u32[]{:S(2)}) copy-start(bf16[2048,128]{1,0:T(8,128)(2,1)} %w_state.1) | copy-start | bytes 1572868
  23.6 1.0 %copy-start.5 = (f32[128,1024]{1,0:T(8,128)S(1)}, f32[128,1024]{1,0:T(8,128)}, u32[]{:S(2)}) copy-start(f32[128,1024]{1,0:T(8,128)} %copy-done.4) | copy-start | bytes 1572868
  24.6 1.0 %copy-start.7 = (f32[128,1024]{1,0:T(8,128)S(1)}, f32[128,1024]{1,0:T(8,128)}, u32[]{:S(2)}) copy-start(f32[128,1024]{1,0:T(8,128)} %copy-done.6) | copy-start | bytes 1572868
  25.7 1.0 %copy-start.9 = (f32[128,1024]{1,0:T(8,128)S(1)}, f32[128,1024]{1,0:T(8,128)}, u32[]{:S(2)}) copy-start(f32[128,1024]{1,0:T(8,128)} %copy-done.8) | copy-start | bytes 1572868
  26.7 1.0 %copy-start.11 = (f32[128,1024]{1,0:T(8,128)S(1)}, f32[128,1024]{1,0:T(8,128)}, u32[]{:S(2)}) copy-start(f32[128,1024]{1,0:T(8,128)} %copy-done.10) | copy-start | bytes 1572868
  27.8 1.0 %copy-start.13 = (bf16[128,2048]{1,0:T(8,128)(2,1)S(1)}, bf16[128,2048]{1,0:T(8,128)(2,1)}, u32[]{:S(2)}) copy-start(bf16[128,2048]{1,0:T(8,128)(2,1)} %copy-done.12) | copy-start | bytes 1572868
  28.8 1.0 %copy-start.15 = (bf16[128,2048]{1,0:T(8,128)(2,1)S(1)}, bf16[128,2048]{1,0:T(8,128)(2,1)}, u32[]{:S(2)}) copy-start(bf16[128,2048]{1,0:T(8,128)(2,1)} %copy-done.14) | copy-start | bytes 1572868
  31.9 0.8 copy-start.24
  32.7 0.8 copy-start.26
  33.5 40.8 %copy-start.18 = (bf16[128,2048]{1,0:T(8,128)(2,1)S(1)}, bf16[128,2048]{1,0:T(8,128)(2,1)}, u32[]{:S(2)}) copy-start(bf16[128,2048]{1,0:T(8,128)(2,1)} %proj_conv.1) | copy-start | bytes 1572868
  33.5 10.2 %all-to-all-start.1 = ((f32[8,24,128]{2,1,0:T(8,128)}), f32[8,24,128]{2,1,0:T(8,128)S(1)}, u32[]{:S(2)}, u32[]{:S(2)}) async-start(f32[8,24,128]{2,1,0:T(8,128)} %get-tuple-element.37), calls=%async_computation.1 | async-start | bytes 196608 | tf_op jit(solution)/shard_map/all_to_all | solution.py:323
  45.1 15.3 %copy-start.39 = (f32[2,2,8,64]{3,2,1,0:T(8,128)S(1)}, f32[2,2,8,64]{3,2,1,0:T(8,128)}, u32[]{:S(2)}) copy-start(f32[2,2,8,64]{3,2,1,0:T(8,128)} %param.32) | copy-start | bytes 24580
  45.1 29.3 %all-to-all-start.2 = ((f32[16,16,128]{2,1,0:T(8,128)}), f32[16,16,128]{2,1,0:T(8,128)S(1)}, u32[]{:S(2)}, u32[]{:S(2)}) async-start(f32[16,16,128]{2,1,0:T(8,128)} %get-tuple-element.38), calls=%async_computation.2 | async-start | bytes 262144 | tf_op jit(solution)/shard_map/all_to_all | solution.py:323
  74.3 0.7 copy-start.30
  74.3 0.7 copy-start.31
  75.0 1.0 %copy-start.19 = (bf16[128,2048]{1,0:T(8,128)(2,1)S(1)}, bf16[128,2048]{1,0:T(8,128)(2,1)}, u32[]{:S(2)}) copy-start(bf16[128,2048]{1,0:T(8,128)(2,1)} %proj_state.1) | copy-start | bytes 1572868
  76.1 1.0 %copy-start.21 = (bf16[2048,128]{1,0:T(8,128)(2,1)S(1)}, bf16[2048,128]{1,0:T(8,128)(2,1)}, u32[]{:S(2)}) copy-start(bf16[2048,128]{1,0:T(8,128)(2,1)} %copy-done.20) | copy-start | bytes 1572868
  77.1 1.0 %copy-start.23 = (bf16[2048,128]{1,0:T(8,128)(2,1)S(1)}, bf16[2048,128]{1,0:T(8,128)(2,1)}, u32[]{:S(2)}) copy-start(bf16[2048,128]{1,0:T(8,128)(2,1)} %copy-done.22) | copy-start | bytes 1572868
  78.1 1.0 %copy-start.25 = (f32[128,1024]{1,0:T(8,128)S(1)}, f32[128,1024]{1,0:T(8,128)}, u32[]{:S(2)}) copy-start(f32[128,1024]{1,0:T(8,128)} %copy-done.24) | copy-start | bytes 1572868
  79.2 1.0 %copy-start.27 = (f32[128,1024]{1,0:T(8,128)S(1)}, f32[128,1024]{1,0:T(8,128)}, u32[]{:S(2)}) copy-start(f32[128,1024]{1,0:T(8,128)} %copy-done.26) | copy-start | bytes 1572868

commit v2 on v1

v2 whole, which is shorter than its diff:
```python
import jax
import jax.numpy as jnp
from jax import lax
from jax.experimental import pallas as pl
from jax.experimental.pallas import tpu as pltpu
from jax.sharding import Mesh
from jax.sharding import PartitionSpec as P

D = 2048
SP = ("sp_0", "sp_1", "sp_2")
EPSILON = 1e-06
F32 = jnp.float32
BF16 = jnp.bfloat16
CHUNKS = 8


def sin_cos(angle):
    turns = jnp.floor(angle * 0.6366197723675814 + 0.5)
    rest = ((angle - turns * 1.5703125) - turns * 4.837512969970703125e-4) - turns * 7.54978995489188216e-8
    rest = jnp.clip(rest, -0.8, 0.8)
    square = rest * rest
    sine = rest + rest * square * (
        -1.6666654611e-1 + square * (8.3321608736e-3 - 1.9515295891e-4 * square)
    )
    cosine = 1.0 - 0.5 * square + square * square * (
        4.166664568298827e-2 + square * (-1.388731625493765e-3 + 2.443315711809948e-5 * square)
    )
    quadrant = turns.astype(jnp.int32)
    odd = (quadrant & 1) == 1
    s = jnp.where(odd, cosine, sine)
    c = jnp.where(odd, sine, cosine)
    s = jnp.where((quadrant & 2) == 2, -s, s)
    c = jnp.where(((quadrant + 1) & 2) == 2, -c, c)
    return s, c


def exp_less_one(x):
    series = x * (1.0 + x * (1 / 2 + x * (1 / 6 + x * (1 / 24 + x * (1 / 120 + x * (1 / 720 + x * (1 / 5040 + x * (1 / 40320))))))))
    return jnp.where(x > -0.5, series, jnp.exp(x) - 1.0)


def moved(elapsed, decay, turn):
    magnitude = jnp.exp(-decay * elapsed)
    s, c = sin_cos(turn * elapsed)
    return magnitude * c, magnitude * s


def cmul(ar, ai, br, bi):
    return ar * br - ai * bi, ar * bi + ai * br


def iota(shape, dim):
    return lax.broadcasted_iota(jnp.int32, shape, dim)


def dot(a, b, dims=((1,), (0,))):
    return lax.dot_general(a, b, (dims, ((), ())), preferred_element_type=F32)


def halves(x):
    high = x.astype(BF16)
    return high, (x - high.astype(F32)).astype(BF16)


def scan_chunks(fr, fi, lr, li, backward):
    rows = iota(fr.shape, 0)
    for k in (1, 2, 4):
        shift = CHUNKS - k if backward else k
        outside = rows >= CHUNKS - k if backward else rows < k
        sfr = jnp.where(outside, 1.0, pltpu.roll(fr, shift, 0))
        sfi = jnp.where(outside, 0.0, pltpu.roll(fi, shift, 0))
        if lr is not None:
            slr = jnp.where(outside, 0.0, pltpu.roll(lr, shift, 0))
            sli = jnp.where(outside, 0.0, pltpu.roll(li, shift, 0))
            ar, ai = cmul(fr, fi, slr, sli)
            lr, li = lr + ar, li + ai
        fr, fi = cmul(fr, fi, sfr, sfi)
    return fr, fi, lr, li


def one_later(x, backward, fill):
    rows = iota(x.shape, 0)
    if backward:
        return jnp.where(rows == CHUNKS - 1, fill, pltpu.roll(x, CHUNKS - 1, 0))
    return jnp.where(rows == 0, fill, pltpu.roll(x, 1, 0))


def pack_kernel(place, stream, gain, out, gain_here, sems):
    n = stream.shape[0]
    copies = [pltpu.make_async_copy(stream, out.at[k, pl.ds(0, n)], sems.at[k]) for k in range(out.shape[0])]
    gain_copy = pltpu.make_async_copy(gain, gain_here, sems.at[out.shape[0]])
    gain_copy.start()
    for copy in copies:
        copy.start()
    gain_copy.wait()
    g = gain_here[...]
    high = g.astype(BF16)
    left = g - high.astype(F32)
    mid = left.astype(BF16)
    low = (left - mid.astype(F32)).astype(BF16)
    row = iota((16, g.shape[1]), 0)
    tail = jnp.where(row == 0, high.astype(F32), jnp.where(row == 1, mid.astype(F32), jnp.where(row == 2, low.astype(F32), 0.0)))
    tail = tail.astype(BF16)
    for k in range(out.shape[0]):
        out[k, n : n + 16, :] = tail
    for copy in copies:
        copy.wait()


def row_of(ref, d, q):
    return jnp.concatenate([ref[d, 2 * q : 2 * q + 1, :], ref[d, 2 * q + 1 : 2 * q + 2, :]], axis=1)


def doubled(x):
    return jnp.concatenate([x, x], axis=1)


def local_kernel(rows, w_value, w_mix, w_gate, w_state, intervals, decay, turn, in_re, in_im, init, hr_o, hi_o, cr_o, ci_o, pr_o, pi_o, br_o, bi_o, source_o, gate_o, input_o, consts, message):
    parts, n, share = rows.shape[0], rows.shape[1] - 16, rows.shape[2]
    per = n // CHUNKS
    channels = w_value.shape[1]
    row, col = iota((n, n), 0), iota((n, n), 1)
    ordered = col == (row % CHUNKS) * per + row // CHUNKS
    steps = jnp.sum(jnp.where(ordered, intervals[...], 0.0), axis=1, keepdims=True)
    total = jnp.sum(intervals[...], axis=1, keepdims=True)
    order = jnp.where(ordered, 1.0, 0.0).astype(BF16)

    squares = 0.0
    for k in range(parts):
        x = rows[k, 0:n, :].astype(F32)
        squares = squares + jnp.sum(x * x, axis=1, keepdims=True)
    inv_rms = lax.rsqrt(squares / D + EPSILON)
    first = second = 0.0
    for k in range(parts):
        tail = rows[k, n : n + 16, :].astype(F32)
        gain = (tail[0:1] + tail[1:2]) + tail[2:3]
        normed = ((rows[k, 0:n, :].astype(F32) * inv_rms) * gain).astype(BF16)
        at = slice(k * share, k * share + share)
        first = first + dot(normed, jnp.concatenate([w_value[at, :], w_mix[at, :]], axis=1))
        second = second + dot(normed, jnp.concatenate([w_gate[at, :], w_state[at, :]], axis=1))
    first = dot(order, first.astype(BF16))
    second = dot(order, second.astype(BF16))
    source = (first[:, :channels] * first[:, channels:]).astype(BF16).astype(F32)
    source_o[...] = source
    gate_o[...] = second[:, :channels]
    input_o[...] = second[:, channels:]
    state = second[:, channels:].astype(BF16)
    state = jnp.concatenate([state, state], axis=1)

    groups, states = decay.shape[1], decay.shape[2]
    wide = channels // groups
    pairs = groups // 2
    edges = []
    for d in range(2):
        backward = d == 1
        rates, turns = decay[d], turn[d]
        inverse = 1.0 / (rates * rates + turns * turns)
        inv_re = jnp.broadcast_to((-rates * inverse)[:, None, :], (groups, wide, states)).reshape(channels, states)
        inv_im = jnp.broadcast_to((-turns * inverse)[:, None, :], (groups, wide, states)).reshape(channels, states)
        at = slice(d * channels, d * channels + channels)
        scaled_re, scaled_im = cmul(in_re[at, :], in_im[at, :], inv_re, inv_im)
        scaled_re, scaled_im = doubled(scaled_re), doubled(scaled_im)
        for q in range(pairs):
            tile = d * pairs + q
            lanes = slice(tile * 128, tile * 128 + 128)
            rate, turning = row_of(decay, d, q), row_of(turn, d, q)
            consts[tile : tile + 1, :] = rate
            consts[8 + tile : 9 + tile, :] = turning
            consts[16 + tile : 17 + tile, :] = jnp.concatenate([init[d, 0, 2 * q : 2 * q + 1, :], init[d, 0, 2 * q + 1 : 2 * q + 2, :]], axis=1)
            consts[24 + tile : 25 + tile, :] = jnp.concatenate([init[d, 1, 2 * q : 2 * q + 1, :], init[d, 1, 2 * q + 1 : 2 * q + 2, :]], axis=1)
            mine = iota((channels, 128), 0) // wide == 2 * q + iota((channels, 128), 1) // states
            re_hi, re_lo = halves(jnp.where(mine, scaled_re, 0.0))
            im_hi, im_lo = halves(jnp.where(mine, scaled_im, 0.0))
            matrix = jnp.concatenate([jnp.concatenate([re_hi, re_lo], axis=0), jnp.concatenate([im_hi, im_lo], axis=0)], axis=1)
            driven = dot(state, matrix)
            damping = -rate * steps
            s, c = sin_cos((0.5 * turning) * steps)
            magnitude = jnp.exp(damping)
            twice = 2.0 * s * s
            cosine = 1.0 - twice
            fr = magnitude * cosine
            fi = magnitude * (2.0 * s * c)
            lift = exp_less_one(damping) * cosine - twice
            push_re, push_im = cmul(lift, fi, driven[:, :128], driven[:, 128:])
            cr = ci = hr = hi = None
            for i in reversed(range(per)) if backward else range(per):
                at = slice(i * CHUNKS, i * CHUNKS + CHUNKS)
                r, m = fr[at], fi[at]
                if cr is None:
                    cr, ci, hr, hi = r, m, push_re[at], push_im[at]
                else:
                    cr, ci = cmul(r, m, cr, ci)
                    ar, ai = cmul(r, m, hr, hi)
                    hr, hi = ar + push_re[at], ai + push_im[at]
                pr_o[at, lanes] = cr
                pi_o[at, lanes] = ci
                hr_o[at, lanes] = hr
                hi_o[at, lanes] = hi
            br, bi, lr, li = scan_chunks(cr, ci, hr, hi, backward)
            br_o[:, lanes] = one_later(br, backward, 1.0)
            bi_o[:, lanes] = one_later(bi, backward, 0.0)
            cr_o[:, lanes] = one_later(lr, backward, 0.0)
            ci_o[:, lanes] = one_later(li, backward, 0.0)
            edge = 0 if backward else CHUNKS - 1
            edges.append((lr[edge : edge + 1], li[edge : edge + 1]))
    for k in range(message.shape[0]):
        for tile, (r, m) in enumerate(edges):
            message[k, tile : tile + 1, :] = r
            message[k, 8 + tile : 9 + tile, :] = m
        message[k, 16:17, :] = jnp.broadcast_to(total, (1, 128))
        message[k, 17:18, :] = source[0:1]
        message[k, 18:19, :] = source[n - 1 : n]
        message[k, 19:24, :] = jnp.zeros((5, 128), F32)


def plane_kernel(place, got, consts, inner, message):
    size = got.shape[0]
    here, plane = place[0], place[1]
    rate, turning = consts[0:8, :], consts[8:16, :]
    forward = iota((8, 128), 0) < 4
    hr = hi = spent = jnp.zeros((8, 128), F32)
    ir = ii = before = hr
    for k in range(size):
        m = size - 1 - k
        mine = (forward & (here == k)) | (jnp.logical_not(forward) & (here == m))
        ir = jnp.where(mine, hr, ir)
        ii = jnp.where(mine, hi, ii)
        before = jnp.where(mine, spent, before)
        elapsed = jnp.where(forward, got[k, 16:17, :], got[m, 16:17, :])
        ar, ai = moved(elapsed, rate, turning)
        ar, ai = cmul(ar, ai, hr, hi)
        hr = ar + jnp.where(forward, got[k, 0:8, :], got[m, 0:8, :])
        hi = ai + jnp.where(forward, got[k, 8:16, :], got[m, 8:16, :])
        spent = spent + elapsed
    wr, wi = moved(before, rate, turning)
    inner[0:8, :] = ir
    inner[8:16, :] = ii
    inner[16:24, :] = wr
    inner[24:32, :] = wi
    previous = following = jnp.zeros((1, 128), F32)
    for k in range(size):
        previous = jnp.where(here - 1 == k, got[k, 18:19, :], previous)
        following = jnp.where(here + 1 == k, got[k, 17:18, :], following)
    inner[32:40, :] = jnp.broadcast_to(previous, (8, 128))
    inner[40:48, :] = jnp.broadcast_to(following, (8, 128))
    swapped = pltpu.roll(hi, 4, 0)
    later = jnp.where(forward, hr, swapped)
    earlier = jnp.where(forward, swapped, hr)
    row = iota((8, 128), 0)
    note_later = jnp.where(row == 0, spent, jnp.where(row == 1, got[size - 1, 18:19, :], 0.0))
    note_earlier = jnp.where(row == 0, spent, jnp.where(row == 1, got[0, 17:18, :], 0.0))
    for k in range(message.shape[0]):
        message[k, 0:8, :] = jnp.where(plane < k, later, earlier)
        message[k, 8:16, :] = jnp.where(plane < k, note_later, note_earlier)


def finish_kernel(place, got, inner, consts, hr_i, hi_i, cr_i, ci_i, pr, pi, br, bi, rd_re, rd_im, source, gate, state, taps, skip, proj_conv, proj_state, out):
    size = got.shape[0]
    here, plane, last = place[0], place[1], place[2]
    rate, turning = consts[0:8, :], consts[8:16, :]
    forward = iota((8, 128), 0) < 4
    hr, hi = consts[16:24, :], consts[24:32, :]
    for k in range(size):
        m = size - 1 - k
        active = (forward & (plane > k)) | (jnp.logical_not(forward) & (plane < m))
        elapsed = jnp.where(forward, got[k, 8:9, :], got[m, 8:9, :])
        ar, ai = moved(elapsed, rate, turning)
        ar, ai = cmul(ar, ai, hr, hi)
        a, b = got[k, 0:8, :], got[m, 0:8, :]
        hr = jnp.where(active, ar + jnp.where(forward, a, b), hr)
        hi = jnp.where(active, ai + pltpu.roll(jnp.where(forward, b, a), 4, 0), hi)
    ar, ai = cmul(inner[16:24, :], inner[24:32, :], hr, hi)
    inc_re = ar + inner[0:8, :]
    inc_im = ai + inner[8:16, :]
    n, width = hr_i.shape
    per = n // CHUNKS
    channels = rd_re.shape[0] // 2
    states = rd_re.shape[1]
    pairs = width // 256
    block = channels // pairs
    wide = block // 2
    responses = []
    for q in range(pairs):
        mine = iota((block, 128), 0) // wide == iota((block, 128), 1) // states
        full, matrix = [], []
        for d in range(2):
            tile = d * pairs + q
            lanes = slice(tile * 128, tile * 128 + 128)
            er, ei = cmul(br[:, lanes], bi[:, lanes], inc_re[tile : tile + 1], inc_im[tile : tile + 1])
            er = jnp.concatenate([er + cr_i[:, lanes]] * per, axis=0)
            ei = jnp.concatenate([ei + ci_i[:, lanes]] * per, axis=0)
            ar, ai = cmul(pr[:, lanes], pi[:, lanes], er, ei)
            full += [ar + hr_i[:, lanes], ai + hi_i[:, lanes]]
            at = slice(d * channels + q * block, d * channels + (q + 1) * block)
            matrix += [jnp.where(mine, doubled(rd_re[at, :]), 0.0), jnp.where(mine, -doubled(rd_im[at, :]), 0.0)]
        high, low = halves(jnp.concatenate(full, axis=1))
        r_hi, r_lo = halves(jnp.concatenate(matrix, axis=1))
        across = ((1,), (1,))
        responses.append((dot(low, r_hi, across) + dot(high, r_lo, across)) + dot(high, r_hi, across))
    response = state[...] * skip[...] + jnp.concatenate(responses, axis=1)
    state_out = jax.nn.gelu(response).astype(BF16)
    previous, following = inner[32:33, :], inner[40:41, :]
    for k in range(size):
        previous = jnp.where((here == 0) & (plane - 1 == k), got[k, 9:10, :], previous)
        following = jnp.where((here == last) & (plane + 1 == k), got[k, 9:10, :], following)
    x = source[...]
    row = iota((CHUNKS, x.shape[1]), 0)
    head = jnp.where(row == 0, previous, pltpu.roll(x[n - CHUNKS :], 1, 0))
    foot = jnp.where(row == CHUNKS - 1, following, pltpu.roll(x[:CHUNKS], CHUNKS - 1, 0))
    before = jnp.concatenate([head, x[: n - CHUNKS]], axis=0)
    after = jnp.concatenate([x[CHUNKS:], foot], axis=0)
    filtered = taps[0:1, :] * before + taps[1:2, :] * x + taps[2:3, :] * after
    conv_out = (gate[...] * filtered).astype(BF16)
    row, col = iota((n, n), 0), iota((n, n), 1)
    order = jnp.where(row == (col % CHUNKS) * per + col // CHUNKS, 1.0, 0.0).astype(BF16)
    conv_out = dot(order, conv_out).astype(BF16)
    state_out = dot(order, state_out).astype(BF16)
    share = out.shape[2]
    for k in range(out.shape[0]):
        at = slice(k * share, k * share + share)
        out[k] = (dot(conv_out, proj_conv[:, at]) + dot(state_out, proj_state[:, at])).astype(BF16)


def exchange(x, axis):
    return lax.all_to_all(x, axis, split_axis=0, concat_axis=0, tiled=True)


VMEM = pl.BlockSpec(memory_space=pltpu.VMEM)
HBM = pl.BlockSpec(memory_space=pltpu.HBM)
SMEM = pl.BlockSpec(memory_space=pltpu.SMEM)


def call(kernel, shapes, *args, specs=(), name=None):
    return pl.pallas_call(
        kernel,
        out_shape=[jax.ShapeDtypeStruct(s, d) for s, d in shapes],
        in_specs=[dict(specs).get(k, VMEM) for k in range(len(args))],
        out_specs=[VMEM] * len(shapes),
        compiler_params=pltpu.CompilerParams(vmem_limit_bytes=24 * 2**20),
        name=name,
    )(*args)


def per_device(
    stream,
    norm_gain,
    w_value,
    w_mix,
    w_gate,
    w_state,
    conv_taps,
    skip_gain,
    decay_rate,
    turn_rate,
    input_real,
    input_imag,
    read_real,
    read_imag,
    initial_state,
    intervals,
    proj_conv,
    proj_state,
):
    n, share = stream.shape
    parts = lax.axis_size("tp")
    inner_axes = SP[1:]
    inside = lax.axis_size(inner_axes)
    planes = lax.axis_size(SP[0])
    channels = w_value.shape[1]
    width = decay_rate.size
    here = lax.axis_index(inner_axes)
    plane = lax.axis_index(SP[0])
    place = jnp.stack([here, plane, jnp.full_like(here, inside - 1)]).astype(jnp.int32)

    packed = pl.pallas_call(
        pack_kernel,
        out_shape=jax.ShapeDtypeStruct((parts, n + 16, share), BF16),
        in_specs=[SMEM, HBM, HBM],
        out_specs=VMEM,
        scratch_shapes=[pltpu.VMEM((1, share), F32), pltpu.SemaphoreType.DMA((parts + 1,))],
        compiler_params=pltpu.CompilerParams(vmem_limit_bytes=4 * 2**20),
        cost_estimate=pl.CostEstimate(flops=10**9, bytes_accessed=3 * 10**7, transcendentals=0),
        name="pack",
    )(place, stream, norm_gain.reshape(1, -1))
    rows = exchange(packed, "tp")

    states = ((n, width), F32)
    chunks = ((CHUNKS, width), F32)
    mixed = ((n, channels), F32)
    hr, hi, cr, ci, pr, pi, br, bi, source, gate, state, consts, message = call(
        local_kernel,
        [states, states, chunks, chunks, states, states, chunks, chunks, mixed, mixed, mixed]
        + [((32, 128), F32), ((inside, 24, 128), F32)],
        rows, w_value, w_mix, w_gate, w_state, intervals.reshape(1, n), decay_rate, turn_rate,
        jnp.swapaxes(input_real, 2, 3).reshape(2 * channels, -1),
        jnp.swapaxes(input_imag, 2, 3).reshape(2 * channels, -1),
        initial_state,
        name="local",
    )
    inner, message = call(
        plane_kernel,
        [((48, 128), F32), ((planes, 16, 128), F32)],
        place, exchange(message, inner_axes), consts,
        specs={0: SMEM},
        name="plane",
    )
    got = exchange(message, SP[0])
    (partial,) = call(
        finish_kernel,
        [((parts, n, share), BF16)],
        place, got, inner, consts, hr, hi, cr, ci, pr, pi, br, bi,
        read_real.reshape(2 * channels, -1), read_imag.reshape(2 * channels, -1), source, gate, state,
        conv_taps, skip_gain.reshape(1, -1), proj_conv, proj_state,
        specs={0: SMEM},
        name="finish",
    )
    arrived = exchange(partial, "tp")
    return arrived.astype(F32).sum(axis=0).astype(BF16)


def solution(mesh):
    finer = Mesh(mesh.devices.reshape(16, 4, 2, mesh.shape["tp"]), ("sp_0", "sp_1", "sp_2", "tp"))
    return jax.shard_map(
        per_device,
        mesh=finer,
        in_specs=(
            P(SP, "tp"),
            P("tp"),
            P(None, "tp"),
            P(None, "tp"),
            P(None, "tp"),
            P(None, "tp"),
            P(None, "tp"),
            P("tp"),
            P(None, "tp", None),
            P(None, "tp", None),
            P(None, "tp", None, None),
            P(None, "tp", None, None),
            P(None, "tp", None, None),
            P(None, "tp", None, None),
            P(None, None, "tp", None),
            P(SP),
            P("tp", None),
            P("tp", None),
        ),
        out_specs=P(SP, "tp"),
        check_vma=False,
    )
```

time: 96.7 us -> 74.5 us (0.77)
  blocking collectives: 12.7 us -> 64 us
  local copies, waits for them, and re-layouts: 29.6 us -> 2.81 us
  starting transfers between devices: 24.4 us -> 0 us
  waiting for transfers between devices: 19.5 us -> 0 us
  Pallas kernels: 8.44 us -> 6.35 us
    all_to_all x1 -> x4, blocking collectives: 12.7 us -> 64 us  [exchange(): return lax.all_to_all(x, axis, split_axis=0, concat_axis=0, tiled=True)]
    unnamed x82 -> x36, local copies, waits for them, and re-layouts: 29.1 us -> 2.81 us
    all_to_all x3 -> x0, starting transfers between devices: 24.4 us -> none  [exchange(): return lax.all_to_all(x, axis, split_axis=0, concat_axis=0, tiled=True)]
    all_to_all x3 -> x0, waiting for transfers between devices: 19.5 us -> none  [exchange(): return lax.all_to_all(x, axis, split_axis=0, concat_axis=0, tiled=True)]
    pallas_call x5 -> x3, Pallas kernels: 8.44 us -> 5.06 us  [call(): pl.pallas_call(kernel, out_shape=[jax.ShapeDtypeStruct(s, d) for s, d in...]
    pallas_call x0 -> x1, Pallas kernels: none -> 1.3 us  [per_device(): pl.pallas_call(pack_kernel, out_shape=jax.ShapeDtypeStruct((parts, n + 16...]
  transfers between devices with their start and end apart: 3 -> 0, of which waited for: 2 -> 0; matrix products, arithmetic and copies ran while one was open for 3% -> 0% of each run, Pallas kernels for 2% -> 0%
where the time goes in v2:
time: 74.5 us; the launch traced here: 74.2 us
  blocking collectives  64 us (86%)
  Pallas kernels  6.35 us (9%)
  local copies, waits for them, and re-layouts  2.81 us (4%)
  other arithmetic  0.82 us (1%)
    all_to_all x4, blocking collectives, exchange(): return lax.all_to_all(x, axis, split_axis=0, concat_axis=0, tiled=True)  64 us
    pallas_call x3, Pallas kernels, call(): pl.pallas_call(kernel, out_shape=[jax.ShapeDtypeStruct(s, d) for s, d in...  5.06 us
    unnamed x36, local copies, waits for them, and re-layouts  2.81 us

profile of v2, /device:TPU:32, one launch (start us, length us, event | category | flops | bytes accessed | tf_op | source)
XLA Modules:
  0.0 74.2 jit_solution(17944694421623669652)
XLA Ops:
  0.0 0.0 copy-start.17
  0.0 0.1 pad_add_fusion.place
  0.1 0.6 copy-done.17
  0.7 0.0 copy-start.16
  0.7 0.9 %copy-done.16 = bf16[128,512]{1,0:T(8,128)(2,1)S(1)} copy-done((bf16[128,512]{1,0:T(8,128)(2,1)S(1)}, bf16[128,512]{1,0:T(8,128)(2,1)}, u32[]{:S(2)}) %copy-start.16) | copy-done | bytes 131096
  1.6 0.0 copy-start.2
  1.6 0.0 copy-start.3
  1.6 0.0 copy-start.7
  1.6 0.0 copy-start.10
  1.6 0.0 copy-start.11
  1.6 0.0 copy-start.12
  1.6 1.3 %pack.1 = bf16[4,144,512]{2,1,0:T(8,128)(2,1)S(1)} custom-call(s32[3]{0:T(128)S(1)} %pad_add_fusion.place, bf16[128,512]{1,0:T(8,128)(2,1)S(1)} %copy-done.16, f32[1,512]{1,0:T(1,128)S(1)} %bitcast.19), custom_call_target="tpu_custom_call" | custom-call | flops 1000000000 | bytes 30000000 | tf_op jit(solution)/shard_map/pack/pallas_call | solution.py:375
  2.9 0.0 copy-start
  2.9 0.0 copy-start.1
  3.0 0.0 copy-start.6
  3.0 14.6 %all_to_all.20.rows = bf16[4,144,512]{2,1,0:T(8,128)(2,1)S(1)} all-to-all(bf16[4,144,512]{2,1,0:T(8,128)(2,1)S(1)} %pack.1), channel_id=1, replica_groups=mesh['sp_0'=16,'sp_1'=4,'sp_2'=2,'tp'=4] {'tp'}, dimensions={0} | all-to-all | bytes 1179648 | tf_op jit(solution)/shard_map/all_to_all | solution.py:325
  17.5 0.0 copy-start.14
  17.5 0.0 copy-done.2
  17.5 0.0 copy-done.3
  17.5 0.0 copy-done.7
  17.6 0.0 copy-done.10
  17.6 0.0 copy-done.11
  17.6 0.0 copy-done.12
  17.6 0.0 copy-done
  17.6 0.0 copy-done.1
  17.6 0.0 copy-done.6
  17.6 0.6 copy-done.14
  18.2 0.0 copy-start.5
  18.2 0.0 copy-start.8
  18.2 0.0 copy-start.9
  18.2 2.5 %local.1 = (f32[128,1024]{1,0:T(8,128)S(1)}, f32[128,1024]{1,0:T(8,128)S(1)}, f32[8,1024]{1,0:T(8,128)S(1)}, f32[8,1024]{1,0:T(8,128)S(1)}, f32[128,1024]{1,0:T(...) custom-call(bf16[4,144,512]{2,1,0:T(8,128)(2,1)S(1)} %all_to_all.20., ...), custom_call_target="tpu_custom_call" | custom-call | tf_op jit(solution)/shard_map/local/pallas_call | solution.py:334
  20.7 0.0 copy-start.4
  20.7 10.0 %all_to_all.21.got = f32[8,24,128]{2,1,0:T(8,128)S(1)} all-to-all(f32[8,24,128]{2,1,0:T(8,128)S(1)} %get-tuple-element.20), channel_id=1, replica_groups=mesh['sp_0'=16,'sp_1'=4,'sp_2'=2,'tp'=4] {'sp_1','sp_2'}, dimensions={0} | all-to-all | bytes 196608 | tf_op jit(solution)/shard_map/all_to_all | solution.py:325
  30.8 0.6 plane.1
  31.4 28.9 %all_to_all.22.got = f32[16,16,128]{2,1,0:T(8,128)S(1)} all-to-all(f32[16,16,128]{2,1,0:T(8,128)S(1)} %get-tuple-element.22), channel_id=1, replica_groups=mesh['sp_0'=16,'sp_1'=4,'sp_2'=2,'tp'=4] {'sp_0'}, dimensions={0} | all-to-all | bytes 262144 | tf_op jit(solution)/shard_map/all_to_all | solution.py:325
  60.4 0.0 copy-start.13
  60.4 0.0 copy-start.15
  60.4 0.0 copy-done.5
  60.4 0.0 copy-done.8
  60.4 0.0 copy-done.9
  60.4 0.0 copy-done.4
  60.4 0.6 copy-done.13
  61.0 0.0 copy-done.15
  61.0 1.9 %finish.1 = bf16[4,128,512]{2,1,0:T(8,128)(2,1)S(1)} custom-call(s32[3]{0:T(128)S(1)} %pad_add_fusion.place, f32[16,16,128]{2,1,0:T(8,128)S(1)} %all_to_all.22.got, f32[48,128]{1,0:T(8,128)S(1)} %get-tuple-element.23.inner, f32[32,128]{1,0:T(8,128)S(1)} %get-tuple-element.21.consts, f32[128,1024]{1,0:T(8,128)S(1)} %get-tuple-element.24.hr_i, ...), custom_call_target="tpu_custom_call" | custom-call | tf_op jit(solution)/shard_map/finish/pallas_call | solution.py:334
  62.9 10.5 %all_to_all.23 = bf16[4,128,512]{2,1,0:T(8,128)(2,1)S(1)} all-to-all(bf16[4,128,512]{2,1,0:T(8,128)(2,1)S(1)} %finish.1), channel_id=1, replica_groups=mesh['sp_0'=16,'sp_1'=4,'sp_2'=2,'tp'=4] {'tp'}, dimensions={0} | all-to-all | bytes 1048576 | tf_op jit(solution)/shard_map/all_to_all | solution.py:325
  73.4 0.7 %reduce_sum.12 = bf16[128,512]{1,0:T(8,128)(2,1)} reduce(bf16[4,128,512]{2,1,0:T(8,128)(2,1)S(1)} %all_to_all.23, bf16[]{:T(256)} %constant.22.clone.1), dimensions={0}, to_apply=%region_0.0 | reduce | flops 196608 | bytes 655362 | tf_op jit(solution)/shard_map/reduce_sum | solution.py:418
Async XLA Ops:
  0.0 0.7 copy-start.17
  0.7 0.9 %copy-start.16 = (bf16[128,512]{1,0:T(8,128)(2,1)S(1)}, bf16[128,512]{1,0:T(8,128)(2,1)}, u32[]{:S(2)}) copy-start(bf16[128,512]{1,0:T(8,128)(2,1)} %stream.1) | copy-start | bytes 393220
  1.6 16.0 %copy-start.2 = (bf16[2048,128]{1,0:T(8,128)(2,1)S(1)}, bf16[2048,128]{1,0:T(8,128)(2,1)}, u32[]{:S(2)}) copy-start(bf16[2048,128]{1,0:T(8,128)(2,1)} %w_gate.1) | copy-start | bytes 1572868
  1.6 16.0 %copy-start.3 = (bf16[2048,128]{1,0:T(8,128)(2,1)S(1)}, bf16[2048,128]{1,0:T(8,128)(2,1)}, u32[]{:S(2)}) copy-start(bf16[2048,128]{1,0:T(8,128)(2,1)} %w_state.1) | copy-start | bytes 1572868
  1.6 16.0 %copy-start.7 = (f32[2,8,64,16]{2,3,1,0:T(8,128)S(1)}, f32[2,8,64,16]{2,3,1,0:T(8,128)}, u32[]{:S(2)}) copy-start(f32[2,8,64,16]{2,3,1,0:T(8,128)} %param.29) | copy-start | bytes 196612
  1.6 16.0 %copy-start.10 = (f32[2,2,8,64]{3,2,1,0:T(8,128)S(1)}, f32[2,2,8,64]{3,2,1,0:T(8,128)}, u32[]{:S(2)}) copy-start(f32[2,2,8,64]{3,2,1,0:T(8,128)} %init.1) | copy-start | bytes 24580
  1.6 16.0 %copy-start.11 = (f32[2,8,64]{2,1,0:T(8,128)S(1)}, f32[2,8,64]{2,1,0:T(8,128)}, u32[]{:S(2)}) copy-start(f32[2,8,64]{2,1,0:T(8,128)} %decay.1) | copy-start | bytes 12292
  1.6 16.0 %copy-start.12 = (f32[2,8,64]{2,1,0:T(8,128)S(1)}, f32[2,8,64]{2,1,0:T(8,128)}, u32[]{:S(2)}) copy-start(f32[2,8,64]{2,1,0:T(8,128)} %turn.1) | copy-start | bytes 12292
  2.9 14.7 %copy-start = (bf16[2048,128]{1,0:T(8,128)(2,1)S(1)}, bf16[2048,128]{1,0:T(8,128)(2,1)}, u32[]{:S(2)}) copy-start(bf16[2048,128]{1,0:T(8,128)(2,1)} %w_value.1) | copy-start | bytes 1572868
  2.9 14.7 %copy-start.1 = (bf16[2048,128]{1,0:T(8,128)(2,1)S(1)}, bf16[2048,128]{1,0:T(8,128)(2,1)}, u32[]{:S(2)}) copy-start(bf16[2048,128]{1,0:T(8,128)(2,1)} %w_mix.1) | copy-start | bytes 1572868
  3.0 14.7 %copy-start.6 = (f32[2,8,64,16]{2,3,1,0:T(8,128)S(1)}, f32[2,8,64,16]{2,3,1,0:T(8,128)}, u32[]{:S(2)}) copy-start(f32[2,8,64,16]{2,3,1,0:T(8,128)} %param.28) | copy-start | bytes 196612
  17.5 0.7 copy-start.14
  18.2 42.2 %copy-start.5 = (bf16[128,2048]{1,0:T(8,128)(2,1)S(1)}, bf16[128,2048]{1,0:T(8,128)(2,1)}, u32[]{:S(2)}) copy-start(bf16[128,2048]{1,0:T(8,128)(2,1)} %proj_state.1) | copy-start | bytes 1572868
  18.2 42.2 %copy-start.8 = (f32[2,8,16,64]{3,2,1,0:T(8,128)S(1)}, f32[2,8,16,64]{3,2,1,0:T(8,128)}, u32[]{:S(2)}) copy-start(f32[2,8,16,64]{3,2,1,0:T(8,128)} %param.30) | copy-start | bytes 196612
  18.2 42.2 %copy-start.9 = (f32[2,8,16,64]{3,2,1,0:T(8,128)S(1)}, f32[2,8,16,64]{3,2,1,0:T(8,128)}, u32[]{:S(2)}) copy-start(f32[2,8,16,64]{3,2,1,0:T(8,128)} %param.31) | copy-start | bytes 196612
  20.7 39.7 %copy-start.4 = (bf16[128,2048]{1,0:T(8,128)(2,1)S(1)}, bf16[128,2048]{1,0:T(8,128)(2,1)}, u32[]{:S(2)}) copy-start(bf16[128,2048]{1,0:T(8,128)(2,1)} %proj_conv.1) | copy-start | bytes 1572868
  60.4 0.7 copy-start.13
  60.4 0.7 copy-start.15

commit v3 on v2

--- a/solution.py
+++ b/solution.py
@@ -85,24 +85,23 @@
     return jnp.where(rows == 0, fill, pltpu.roll(x, 1, 0))
 
 
-def pack_kernel(place, stream, gain, out, gain_here, sems):
-    n = stream.shape[0]
+def pack_kernel(stream, gain, intervals, taps, skip, out, notes, sems):
+    n, share = stream.shape
     copies = [pltpu.make_async_copy(stream, out.at[k, pl.ds(0, n)], sems.at[k]) for k in range(out.shape[0])]
-    gain_copy = pltpu.make_async_copy(gain, gain_here, sems.at[out.shape[0]])
-    gain_copy.start()
     for copy in copies:
         copy.start()
-    gain_copy.wait()
-    g = gain_here[...]
-    high = g.astype(BF16)
-    left = g - high.astype(F32)
-    mid = left.astype(BF16)
-    low = (left - mid.astype(F32)).astype(BF16)
-    row = iota((16, g.shape[1]), 0)
-    tail = jnp.where(row == 0, high.astype(F32), jnp.where(row == 1, mid.astype(F32), jnp.where(row == 2, low.astype(F32), 0.0)))
-    tail = tail.astype(BF16)
+    row = iota((8, share), 0)
+    tail = jnp.zeros((8, share), F32)
+    for at, x in enumerate((gain[...], jnp.concatenate([intervals[...]] * (share // n), axis=1))):
+        high = x.astype(BF16).astype(F32)
+        mid = (x - high).astype(BF16).astype(F32)
+        for p, piece in enumerate((high, mid, x - high - mid)):
+            tail = jnp.where(row == 3 * at + p, piece, tail)
     for k in range(out.shape[0]):
-        out[k, n : n + 16, :] = tail
+        out[k, n : n + 8, :] = tail.astype(BF16)
+    notes[0:3, :] = taps[...]
+    notes[3:4, :] = skip[...]
+    notes[4:8, :] = jnp.zeros((4, notes.shape[1]), F32)
     for copy in copies:
         copy.wait()
 
@@ -115,14 +114,16 @@
     return jnp.concatenate([x, x], axis=1)
 
 
-def local_kernel(rows, w_value, w_mix, w_gate, w_state, intervals, decay, turn, in_re, in_im, init, hr_o, hi_o, cr_o, ci_o, pr_o, pi_o, br_o, bi_o, source_o, gate_o, input_o, consts, message):
-    parts, n, share = rows.shape[0], rows.shape[1] - 16, rows.shape[2]
+def local_kernel(rows, w_value, w_mix, w_gate, w_state, decay, turn, in_re, in_im, init, notes, hr_o, hi_o, cr_o, ci_o, pr_o, pi_o, br_o, bi_o, source_o, gate_o, input_o, consts, message):
+    parts, n, share = rows.shape[0], rows.shape[1] - 8, rows.shape[2]
     per = n // CHUNKS
     channels = w_value.shape[1]
     row, col = iota((n, n), 0), iota((n, n), 1)
     ordered = col == (row % CHUNKS) * per + row // CHUNKS
-    steps = jnp.sum(jnp.where(ordered, intervals[...], 0.0), axis=1, keepdims=True)
-    total = jnp.sum(intervals[...], axis=1, keepdims=True)
+    tail = rows[0, n : n + 8, 0:n].astype(F32)
+    intervals = (tail[3:4] + tail[4:5]) + tail[5:6]
+    steps = jnp.sum(jnp.where(ordered, intervals, 0.0), axis=1, keepdims=True)
+    total = jnp.sum(intervals, axis=1, keepdims=True)
     order = jnp.where(ordered, 1.0, 0.0).astype(BF16)
 
     squares = 0.0
@@ -132,7 +133,7 @@
     inv_rms = lax.rsqrt(squares / D + EPSILON)
     first = second = 0.0
     for k in range(parts):
-        tail = rows[k, n : n + 16, :].astype(F32)
+        tail = rows[k, n : n + 8, :].astype(F32)
         gain = (tail[0:1] + tail[1:2]) + tail[2:3]
         normed = ((rows[k, 0:n, :].astype(F32) * inv_rms) * gain).astype(BF16)
         at = slice(k * share, k * share + share)
@@ -150,6 +151,7 @@
     groups, states = decay.shape[1], decay.shape[2]
     wide = channels // groups
     pairs = groups // 2
+    consts[32:40, :] = notes[...]
     edges = []
     for d in range(2):
         backward = d == 1
@@ -213,9 +215,9 @@
         message[k, 19:24, :] = jnp.zeros((5, 128), F32)
 
 
-def plane_kernel(place, got, consts, inner, message):
+def plane_kernel(got, consts, inner, message):
     size = got.shape[0]
-    here, plane = place[0], place[1]
+    here, plane = lax.axis_index(SP[1:]), lax.axis_index(SP[0])
     rate, turning = consts[0:8, :], consts[8:16, :]
     forward = iota((8, 128), 0) < 4
     hr = hi = spent = jnp.zeros((8, 128), F32)
@@ -247,26 +249,33 @@
     later = jnp.where(forward, hr, swapped)
     earlier = jnp.where(forward, swapped, hr)
     row = iota((8, 128), 0)
-    note_later = jnp.where(row == 0, spent, jnp.where(row == 1, got[size - 1, 18:19, :], 0.0))
-    note_earlier = jnp.where(row == 0, spent, jnp.where(row == 1, got[0, 17:18, :], 0.0))
+    high = spent.astype(BF16).astype(F32)
+    mid = (spent - high).astype(BF16).astype(F32)
+    note = jnp.where(row == 0, high, jnp.where(row == 1, mid, jnp.where(row == 2, spent - high - mid, 0.0)))
+    note_later = jnp.where(row == 3, got[size - 1, 18:19, :], note)
+    note_earlier = jnp.where(row == 3, got[0, 17:18, :], note)
+    later = jnp.concatenate([later, note_later], axis=0)
+    earlier = jnp.concatenate([earlier, note_earlier], axis=0)
     for k in range(message.shape[0]):
-        message[k, 0:8, :] = jnp.where(plane < k, later, earlier)
-        message[k, 8:16, :] = jnp.where(plane < k, note_later, note_earlier)
-
-
-def finish_kernel(place, got, inner, consts, hr_i, hi_i, cr_i, ci_i, pr, pi, br, bi, rd_re, rd_im, source, gate, state, taps, skip, proj_conv, proj_state, out):
+        message[k] = jnp.where(plane < k, later, earlier).astype(BF16)
+
+
+def finish_kernel(got, inner, consts, hr_i, hi_i, cr_i, ci_i, pr, pi, br, bi, rd_re, rd_im, source, gate, state, proj_conv, proj_state, out):
     size = got.shape[0]
-    here, plane, last = place[0], place[1], place[2]
+    here, plane = lax.axis_index(SP[1:]), lax.axis_index(SP[0])
+    last = lax.axis_size(SP[1:]) - 1
     rate, turning = consts[0:8, :], consts[8:16, :]
     forward = iota((8, 128), 0) < 4
     hr, hi = consts[16:24, :], consts[24:32, :]
+    arrived = [got[k].astype(F32) for k in range(size)]
+    times = [(x[8:9] + x[9:10]) + x[10:11] for x in arrived]
     for k in range(size):
         m = size - 1 - k
         active = (forward & (plane > k)) | (jnp.logical_not(forward) & (plane < m))
-        elapsed = jnp.where(forward, got[k, 8:9, :], got[m, 8:9, :])
+        elapsed = jnp.where(forward, times[k], times[m])
         ar, ai = moved(elapsed, rate, turning)
         ar, ai = cmul(ar, ai, hr, hi)
-        a, b = got[k, 0:8, :], got[m, 0:8, :]
+        a, b = arrived[k][0:8], arrived[m][0:8]
         hr = jnp.where(active, ar + jnp.where(forward, a, b), hr)
         hi = jnp.where(active, ai + pltpu.roll(jnp.where(forward, b, a), 4, 0), hi)
     ar, ai = cmul(inner[16:24, :], inner[24:32, :], hr, hi)
@@ -297,19 +306,19 @@
         r_hi, r_lo = halves(jnp.concatenate(matrix, axis=1))
         across = ((1,), (1,))
         responses.append((dot(low, r_hi, across) + dot(high, r_lo, across)) + dot(high, r_hi, across))
-    response = state[...] * skip[...] + jnp.concatenate(responses, axis=1)
+    response = state[...] * consts[35:36, :] + jnp.concatenate(responses, axis=1)
     state_out = jax.nn.gelu(response).astype(BF16)
     previous, following = inner[32:33, :], inner[40:41, :]
     for k in range(size):
-        previous = jnp.where((here == 0) & (plane - 1 == k), got[k, 9:10, :], previous)
-        following = jnp.where((here == last) & (plane + 1 == k), got[k, 9:10, :], following)
+        previous = jnp.where((here == 0) & (plane - 1 == k), arrived[k][11:12], previous)
+        following = jnp.where((here == last) & (plane + 1 == k), arrived[k][11:12], following)
     x = source[...]
     row = iota((CHUNKS, x.shape[1]), 0)
     head = jnp.where(row == 0, previous, pltpu.roll(x[n - CHUNKS :], 1, 0))
     foot = jnp.where(row == CHUNKS - 1, following, pltpu.roll(x[:CHUNKS], CHUNKS - 1, 0))
     before = jnp.concatenate([head, x[: n - CHUNKS]], axis=0)
     after = jnp.concatenate([x[CHUNKS:], foot], axis=0)
-    filtered = taps[0:1, :] * before + taps[1:2, :] * x + taps[2:3, :] * after
+    filtered = consts[32:33, :] * before + consts[33:34, :] * x + consts[34:35, :] * after
     conv_out = (gate[...] * filtered).astype(BF16)
     row, col = iota((n, n), 0), iota((n, n), 1)
     order = jnp.where(row == (col % CHUNKS) * per + col // CHUNKS, 1.0, 0.0).astype(BF16)
@@ -326,15 +335,13 @@
 
 
 VMEM = pl.BlockSpec(memory_space=pltpu.VMEM)
-HBM = pl.BlockSpec(memory_space=pltpu.HBM)
-SMEM = pl.BlockSpec(memory_space=pltpu.SMEM)
-
-
-def call(kernel, shapes, *args, specs=(), name=None):
+
+
+def call(kernel, shapes, *args, name=None):
     return pl.pallas_call(
         kernel,
         out_shape=[jax.ShapeDtypeStruct(s, d) for s, d in shapes],
-        in_specs=[dict(specs).get(k, VMEM) for k in range(len(args))],
+        in_specs=[VMEM] * len(args),
         out_specs=[VMEM] * len(shapes),
         compiler_params=pltpu.CompilerParams(vmem_limit_bytes=24 * 2**20),
         name=name,
@@ -368,20 +375,16 @@
     planes = lax.axis_size(SP[0])
     channels = w_value.shape[1]
     width = decay_rate.size
-    here = lax.axis_index(inner_axes)
-    plane = lax.axis_index(SP[0])
-    place = jnp.stack([here, plane, jnp.full_like(here, inside - 1)]).astype(jnp.int32)
-
-    packed = pl.pallas_call(
+    packed, notes = pl.pallas_call(
         pack_kernel,
-        out_shape=jax.ShapeDtypeStruct((parts, n + 16, share), BF16),
-        in_specs=[SMEM, HBM, HBM],
-        out_specs=VMEM,
-        scratch_shapes=[pltpu.VMEM((1, share), F32), pltpu.SemaphoreType.DMA((parts + 1,))],
+        out_shape=[jax.ShapeDtypeStruct((parts, n + 8, share), BF16), jax.ShapeDtypeStruct((8, channels), F32)],
+        in_specs=[VMEM] * 5,
+        out_specs=[VMEM] * 2,
+        scratch_shapes=[pltpu.SemaphoreType.DMA((parts,))],
         compiler_params=pltpu.CompilerParams(vmem_limit_bytes=4 * 2**20),
-        cost_estimate=pl.CostEstimate(flops=10**9, bytes_accessed=3 * 10**7, transcendentals=0),
+        cost_estimate=pl.CostEstimate(flops=10**9, bytes_accessed=3 * 10**8, transcendentals=0),
         name="pack",
-    )(place, stream, norm_gain.reshape(1, -1))
+    )(stream, norm_gain.reshape(1, -1), intervals.reshape(1, n), conv_taps, skip_gain.reshape(1, -1))
     rows = exchange(packed, "tp")
 
     states = ((n, width), F32)
@@ -390,28 +393,26 @@
     hr, hi, cr, ci, pr, pi, br, bi, source, gate, state, consts, message = call(
         local_kernel,
         [states, states, chunks, chunks, states, states, chunks, chunks, mixed, mixed, mixed]
-        + [((32, 128), F32), ((inside, 24, 128), F32)],
-        rows, w_value, w_mix, w_gate, w_state, intervals.reshape(1, n), decay_rate, turn_rate,
+        + [((40, channels), F32), ((inside, 24, 128), F32)],
+        rows, w_value, w_mix, w_gate, w_state, decay_rate, turn_rate,
         jnp.swapaxes(input_real, 2, 3).reshape(2 * channels, -1),
         jnp.swapaxes(input_imag, 2, 3).reshape(2 * channels, -1),
-        initial_state,
+        initial_state, notes,
         name="local",
     )
     inner, message = call(
         plane_kernel,
-        [((48, 128), F32), ((planes, 16, 128), F32)],
-        place, exchange(message, inner_axes), consts,
-        specs={0: SMEM},
+        [((48, 128), F32), ((planes, 16, 128), BF16)],
+        exchange(message, inner_axes), consts,
         name="plane",
     )
     got = exchange(message, SP[0])
     (partial,) = call(
         finish_kernel,
         [((parts, n, share), BF16)],
-        place, got, inner, consts, hr, hi, cr, ci, pr, pi, br, bi,
+        got, inner, consts, hr, hi, cr, ci, pr, pi, br, bi,
         read_real.reshape(2 * channels, -1), read_imag.reshape(2 * channels, -1), source, gate, state,
-        conv_taps, skip_gain.reshape(1, -1), proj_conv, proj_state,
-        specs={0: SMEM},
+        proj_conv, proj_state,
         name="finish",
     )
     arrived = exchange(partial, "tp")

time: 74.5 us -> 69.3 us (0.930)
  blocking collectives: 64 us -> 61.7 us
  Pallas kernels: 6.35 us -> 4.81 us
  local copies, waits for them, and re-layouts: 2.81 us -> 1.66 us
    all_to_all x4, blocking collectives: 64 us -> 61.7 us  [exchange(): return lax.all_to_all(x, axis, split_axis=0, concat_axis=0, tiled=True)]
    unnamed x36, local copies, waits for them, and re-layouts: 2.81 us -> 1.66 us
    pallas_call x3, Pallas kernels: 5.06 us -> 4.07 us  [call(): pl.pallas_call(kernel, out_shape=[jax.ShapeDtypeStruct(s, d) for s, d in...]
where the time goes in v3:
time: 69.3 us; the launch traced here: 69 us
  blocking collectives  61.7 us (89%)
  Pallas kernels  4.81 us (7%)
  local copies, waits for them, and re-layouts  1.66 us (2%)
  other arithmetic  0.75 us (1%)
    all_to_all x4, blocking collectives, exchange(): return lax.all_to_all(x, axis, split_axis=0, concat_axis=0, tiled=True)  61.7 us
    pallas_call x3, Pallas kernels, call(): pl.pallas_call(kernel, out_shape=[jax.ShapeDtypeStruct(s, d) for s, d in...  4.07 us
    unnamed x36, local copies, waits for them, and re-layouts  1.66 us

profile of v3, /device:TPU:32, one launch (start us, length us, event | category | flops | bytes accessed | tf_op | source)
XLA Modules:
  0.0 69.0 jit_solution(4326230601619615875)
XLA Ops:
  0.0 0.0 copy-start.15
  0.0 0.0 copy-start.14
  0.0 0.0 copy-start.16
  0.0 0.0 copy-start.17
  0.0 0.7 copy-done.15
  0.7 0.0 copy-done.14
  0.7 0.0 copy-done.16
  0.7 0.0 copy-done.17
  0.7 0.0 copy-start.13
  0.7 0.9 %copy-done.13 = bf16[128,512]{1,0:T(8,128)(2,1)S(1)} copy-done((bf16[128,512]{1,0:T(8,128)(2,1)S(1)}, bf16[128,512]{1,0:T(8,128)(2,1)}, u32[]{:S(2)}) %copy-start.13) | copy-done | bytes 131096
  1.6 0.0 copy-start.4
  1.6 0.0 copy-start.5
  1.6 0.0 copy-start.6
  1.6 0.0 copy-start.7
  1.6 0.7 %pack.1 = (bf16[4,136,512]{2,1,0:T(8,128)(2,1)S(1)}, f32[8,128]{1,0:T(8,128)S(1)}) custom-call(bf16[128,512]{1,0:T(8,128)(2,1)S(1)} %copy-done.13, f32[1,512]{1,0:T(1,128)S(1)} %bitcast.15, f32[1,128]{1,0:T(1,128)S(1)} %bitcast.16, f32[3,128]{1,0:T(4,128)S(1)} %copy-done.15, f32[1,128]{1,0:T(1,128)S(1)} %bitcast.17), custom_call_target="tpu_custom_call" | custom-call | flops 1000000000 | bytes 300000000 | tf_op jit(solution)/shard_map/pack/pallas_call | solution.py:378
  2.4 0.0 copy-start.2
  2.4 0.0 copy-start.3
  2.4 0.0 copy-start.10
  2.4 0.0 copy-start.11
  2.4 0.0 copy-start.12
  2.4 14.2 %all_to_all.20.rows = bf16[4,136,512]{2,1,0:T(8,128)(2,1)S(1)} all-to-all(bf16[4,136,512]{2,1,0:T(8,128)(2,1)S(1)} %get-tuple-element.22), channel_id=1, replica_groups=mesh['sp_0'=16,'sp_1'=4,'sp_2'=2,'tp'=4] {'tp'}, dimensions={0} | all-to-all | bytes 1114112 | tf_op jit(solution)/shard_map/all_to_all | solution.py:334
  16.7 0.0 copy-done.4
  16.7 0.0 copy-done.5
  16.7 0.0 copy-done.6
  16.7 0.0 copy-done.7
  16.7 0.0 copy-done.2
  16.7 0.0 copy-done.3
  16.7 0.0 copy-done.10
  16.7 0.0 copy-done.11
  16.7 0.0 copy-done.12
  16.7 0.0 copy-start
  16.7 0.0 copy-start.1
  16.8 2.5 %local.1 = (f32[128,1024]{1,0:T(8,128)S(1)}, f32[128,1024]{1,0:T(8,128)S(1)}, f32[8,1024]{1,0:T(8,128)S(1)}, f32[8,1024]{1,0:T(8,128)S(1)}, f32[128,1024]{1,0:T(...) custom-call(bf16[4,136,512]{2,1,0:T(8,128)(2,1)S(1)} %all_to_all.20., ...), custom_call_target="tpu_custom_call" | custom-call | tf_op jit(solution)/shard_map/local/pallas_call | solution.py:341
  19.3 9.9 %all_to_all.21.got = f32[8,24,128]{2,1,0:T(8,128)S(1)} all-to-all(f32[8,24,128]{2,1,0:T(8,128)S(1)} %get-tuple-element.24), channel_id=1, replica_groups=mesh['sp_0'=16,'sp_1'=4,'sp_2'=2,'tp'=4] {'sp_1','sp_2'}, dimensions={0} | all-to-all | bytes 196608 | tf_op jit(solution)/shard_map/all_to_all | solution.py:334
  29.2 0.0 copy-start.8
  29.2 0.0 copy-start.9
  29.2 0.1 plane.1
  29.3 26.8 %all_to_all.22.got = bf16[16,16,128]{2,1,0:T(8,128)(2,1)S(1)} all-to-all(bf16[16,16,128]{2,1,0:T(8,128)(2,1)S(1)} %get-tuple-element.26), channel_id=1, replica_groups=mesh['sp_0'=16,'sp_1'=4,'sp_2'=2,'tp'=4] {'sp_0'}, dimensions={0} | all-to-all | bytes 131072 | tf_op jit(solution)/shard_map/all_to_all | solution.py:334
  56.1 0.0 copy-done
  56.1 0.0 copy-done.1
  56.1 0.0 copy-done.8
  56.1 0.0 copy-done.9
  56.1 1.4 %finish.1 = bf16[4,128,512]{2,1,0:T(8,128)(2,1)S(1)} custom-call(bf16[16,16,128]{2,1,0:T(8,128)(2,1)S(1)} %all_to_all.22.got, f32[48,128]{1,0:T(8,128)S(1)} %get-tuple-element.27.inner, f32[40,128]{1,0:T(8,128)S(1)} %get-tuple-element.25.consts, f32[128,1024]{1,0:T(8,128)S(1)} %get-tuple-element.28.hr_i, f32[128,1024]{1,0:T(8,128)S(1)} %get-tuple-element.29.hi_i, ...), custom_call_target="tpu_custom_call" | custom-call | tf_op jit(solution)/shard_map/finish/pallas_call | solution.py:341
  57.5 10.8 %all_to_all.23 = bf16[4,128,512]{2,1,0:T(8,128)(2,1)S(1)} all-to-all(bf16[4,128,512]{2,1,0:T(8,128)(2,1)S(1)} %finish.1), channel_id=1, replica_groups=mesh['sp_0'=16,'sp_1'=4,'sp_2'=2,'tp'=4] {'tp'}, dimensions={0} | all-to-all | bytes 1048576 | tf_op jit(solution)/shard_map/all_to_all | solution.py:334
  68.3 0.7 %reduce_sum.12 = bf16[128,512]{1,0:T(8,128)(2,1)} reduce(bf16[4,128,512]{2,1,0:T(8,128)(2,1)S(1)} %all_to_all.23, bf16[]{:T(256)} %constant.2.clone.1), dimensions={0}, to_apply=%region_0.0 | reduce | flops 196608 | bytes 655362 | tf_op jit(solution)/shard_map/reduce_sum | solution.py:419
Async XLA Ops:
  0.0 0.7 copy-start.15
  0.0 0.7 %copy-start.14 = (f32[512]{0:T(512)S(1)}, f32[512]{0:T(512)}, u32[]{:S(2)}) copy-start(f32[512]{0:T(512)} %param.19) | copy-start | bytes 6148
  0.0 0.7 %copy-start.16 = (f32[128]{0:T(128)S(1)}, f32[128]{0:T(128)}, u32[]{:S(2)}) copy-start(f32[128]{0:T(128)} %param.33) | copy-start | bytes 1540
  0.0 0.7 %copy-start.17 = (f32[128]{0:T(128)S(1)}, f32[128]{0:T(128)}, u32[]{:S(2)}) copy-start(f32[128]{0:T(128)} %param.25) | copy-start | bytes 1540
  0.7 0.9 %copy-start.13 = (bf16[128,512]{1,0:T(8,128)(2,1)S(1)}, bf16[128,512]{1,0:T(8,128)(2,1)}, u32[]{:S(2)}) copy-start(bf16[128,512]{1,0:T(8,128)(2,1)} %stream.1) | copy-start | bytes 393220
  1.6 15.0 %copy-start.4 = (bf16[2048,128]{1,0:T(8,128)(2,1)S(1)}, bf16[2048,128]{1,0:T(8,128)(2,1)}, u32[]{:S(2)}) copy-start(bf16[2048,128]{1,0:T(8,128)(2,1)} %w_gate.1) | copy-start | bytes 1572868
  1.6 15.1 %copy-start.5 = (bf16[2048,128]{1,0:T(8,128)(2,1)S(1)}, bf16[2048,128]{1,0:T(8,128)(2,1)}, u32[]{:S(2)}) copy-start(bf16[2048,128]{1,0:T(8,128)(2,1)} %w_state.1) | copy-start | bytes 1572868
  1.6 15.1 %copy-start.6 = (f32[2,8,64,16]{2,3,1,0:T(8,128)S(1)}, f32[2,8,64,16]{2,3,1,0:T(8,128)}, u32[]{:S(2)}) copy-start(f32[2,8,64,16]{2,3,1,0:T(8,128)} %param.28) | copy-start | bytes 196612
  1.6 15.1 %copy-start.7 = (f32[2,8,64,16]{2,3,1,0:T(8,128)S(1)}, f32[2,8,64,16]{2,3,1,0:T(8,128)}, u32[]{:S(2)}) copy-start(f32[2,8,64,16]{2,3,1,0:T(8,128)} %param.29) | copy-start | bytes 196612
  2.4 14.3 %copy-start.2 = (bf16[2048,128]{1,0:T(8,128)(2,1)S(1)}, bf16[2048,128]{1,0:T(8,128)(2,1)}, u32[]{:S(2)}) copy-start(bf16[2048,128]{1,0:T(8,128)(2,1)} %w_value.1) | copy-start | bytes 1572868
  2.4 14.3 %copy-start.3 = (bf16[2048,128]{1,0:T(8,128)(2,1)S(1)}, bf16[2048,128]{1,0:T(8,128)(2,1)}, u32[]{:S(2)}) copy-start(bf16[2048,128]{1,0:T(8,128)(2,1)} %w_mix.1) | copy-start | bytes 1572868
  2.4 14.3 %copy-start.10 = (f32[2,2,8,64]{3,2,1,0:T(8,128)S(1)}, f32[2,2,8,64]{3,2,1,0:T(8,128)}, u32[]{:S(2)}) copy-start(f32[2,2,8,64]{3,2,1,0:T(8,128)} %init.1) | copy-start | bytes 24580
  2.4 14.3 %copy-start.11 = (f32[2,8,64]{2,1,0:T(8,128)S(1)}, f32[2,8,64]{2,1,0:T(8,128)}, u32[]{:S(2)}) copy-start(f32[2,8,64]{2,1,0:T(8,128)} %decay.1) | copy-start | bytes 12292
  2.4 14.3 %copy-start.12 = (f32[2,8,64]{2,1,0:T(8,128)S(1)}, f32[2,8,64]{2,1,0:T(8,128)}, u32[]{:S(2)}) copy-start(f32[2,8,64]{2,1,0:T(8,128)} %turn.1) | copy-start | bytes 12292
  16.7 39.3 %copy-start = (bf16[128,2048]{1,0:T(8,128)(2,1)S(1)}, bf16[128,2048]{1,0:T(8,128)(2,1)}, u32[]{:S(2)}) copy-start(bf16[128,2048]{1,0:T(8,128)(2,1)} %proj_conv.1) | copy-start | bytes 1572868
  16.7 39.3 %copy-start.1 = (bf16[128,2048]{1,0:T(8,128)(2,1)S(1)}, bf16[128,2048]{1,0:T(8,128)(2,1)}, u32[]{:S(2)}) copy-start(bf16[128,2048]{1,0:T(8,128)(2,1)} %proj_state.1) | copy-start | bytes 1572868
  29.2 26.9 %copy-start.8 = (f32[2,8,16,64]{3,2,1,0:T(8,128)S(1)}, f32[2,8,16,64]{3,2,1,0:T(8,128)}, u32[]{:S(2)}) copy-start(f32[2,8,16,64]{3,2,1,0:T(8,128)} %param.30) | copy-start | bytes 196612
  29.2 26.9 %copy-start.9 = (f32[2,8,16,64]{3,2,1,0:T(8,128)S(1)}, f32[2,8,16,64]{3,2,1,0:T(8,128)}, u32[]{:S(2)}) copy-start(f32[2,8,16,64]{3,2,1,0:T(8,128)} %param.31) | copy-start | bytes 196612

commit v4 on v3

--- a/solution.py
+++ b/solution.py
@@ -14,35 +14,41 @@
 CHUNKS = 8
 
 
-def sin_cos(angle):
-    turns = jnp.floor(angle * 0.6366197723675814 + 0.5)
-    rest = ((angle - turns * 1.5703125) - turns * 4.837512969970703125e-4) - turns * 7.54978995489188216e-8
-    rest = jnp.clip(rest, -0.8, 0.8)
+def turned(half_turn, elapsed):
+    half = half_turn * elapsed
+    turns = jnp.round(half * 0.3183098861837907)
+    rest = jnp.clip((half - turns * 3.140625) - turns * 9.67653589793e-4, -1.6, 1.6)
     square = rest * rest
-    sine = rest + rest * square * (
-        -1.6666654611e-1 + square * (8.3321608736e-3 - 1.9515295891e-4 * square)
-    )
-    cosine = 1.0 - 0.5 * square + square * square * (
-        4.166664568298827e-2 + square * (-1.388731625493765e-3 + 2.443315711809948e-5 * square)
-    )
-    quadrant = turns.astype(jnp.int32)
-    odd = (quadrant & 1) == 1
-    s = jnp.where(odd, cosine, sine)
-    c = jnp.where(odd, sine, cosine)
-    s = jnp.where((quadrant & 2) == 2, -s, s)
-    c = jnp.where(((quadrant + 1) & 2) == 2, -c, c)
-    return s, c
-
-
-def exp_less_one(x):
-    series = x * (1.0 + x * (1 / 2 + x * (1 / 6 + x * (1 / 24 + x * (1 / 120 + x * (1 / 720 + x * (1 / 5040 + x * (1 / 40320))))))))
-    return jnp.where(x > -0.5, series, jnp.exp(x) - 1.0)
-
-
-def moved(elapsed, decay, turn):
-    magnitude = jnp.exp(-decay * elapsed)
-    s, c = sin_cos(turn * elapsed)
-    return magnitude * c, magnitude * s
+    sine = rest + rest * (square * (-0.16666659712791443 + square * (0.008333086036145687 + square * (-0.0001981096138479188 + square * 2.6085685931320768e-06))))
+    cosine = 1.0 + square * (-0.4999993145465851 + square * (0.04166397079825401 + square * (-0.0013855763245373964 + square * 2.3190419597085565e-05)))
+    double = sine + sine
+    fall = double * sine
+    return double * cosine, 1.0 - fall, fall
+
+
+def turned_briefly(rate, elapsed):
+    turns = rate * elapsed
+    rest = turns - jnp.round(turns)
+    square = rest * rest
+    sine = rest * (4.442883014678955 + square * (-7.308244228363037 + square * (3.606335163116455 + square * (-0.846008837223053 + square * 0.10963883250951767))))
+    cosine = 1.4142135381698608 + square * (-6.978850841522217 + square * (5.7394561767578125 + square * (-1.8835265636444092 + square * 0.3106144070625305)))
+    fall = sine * sine
+    return sine * cosine, 1.0 - fall, fall
+
+
+def damped(half_rate, elapsed):
+    x = half_rate * elapsed
+    root = jnp.exp(-x)
+    magnitude = root * root
+    square = x * x
+    series = root * (x * (-2.0 - square * (1 / 3 + square * (1 / 60))))
+    return magnitude, jnp.where(x < 0.25, series, magnitude - 1.0)
+
+
+def moved(elapsed, rate, half_turn):
+    magnitude = jnp.exp(-rate * elapsed)
+    sine, cosine, _ = turned(half_turn, elapsed)
+    return magnitude * cosine, magnitude * sine
 
 
 def cmul(ar, ai, br, bi):
@@ -85,11 +91,12 @@
     return jnp.where(rows == 0, fill, pltpu.roll(x, 1, 0))
 
 
-def pack_kernel(stream, gain, intervals, taps, skip, out, notes, sems):
+def lead_kernel(out):
+    out[...] = jnp.zeros(out.shape, F32)
+
+
+def pack_kernel(stream, gain, intervals, taps, skip, blank, out, notes):
     n, share = stream.shape
-    copies = [pltpu.make_async_copy(stream, out.at[k, pl.ds(0, n)], sems.at[k]) for k in range(out.shape[0])]
-    for copy in copies:
-        copy.start()
     row = iota((8, share), 0)
     tail = jnp.zeros((8, share), F32)
     for at, x in enumerate((gain[...], jnp.concatenate([intervals[...]] * (share // n), axis=1))):
@@ -97,13 +104,13 @@
         mid = (x - high).astype(BF16).astype(F32)
         for p, piece in enumerate((high, mid, x - high - mid)):
             tail = jnp.where(row == 3 * at + p, piece, tail)
+    tail = tail.astype(BF16)
     for k in range(out.shape[0]):
-        out[k, n : n + 8, :] = tail.astype(BF16)
+        out[k, 0:n, :] = stream[...]
+        out[k, n : n + 8, :] = tail
+    notes[...] = blank[...]
     notes[0:3, :] = taps[...]
     notes[3:4, :] = skip[...]
-    notes[4:8, :] = jnp.zeros((4, notes.shape[1]), F32)
-    for copy in copies:
-        copy.wait()
 
 
 def row_of(ref, d, q):
@@ -114,17 +121,50 @@
     return jnp.concatenate([x, x], axis=1)
 
 
-def local_kernel(rows, w_value, w_mix, w_gate, w_state, decay, turn, in_re, in_im, init, notes, hr_o, hi_o, cr_o, ci_o, pr_o, pi_o, br_o, bi_o, source_o, gate_o, input_o, consts, message):
+def local_kernel(rows, w_value, w_mix, w_gate, w_state, decay, turn, in_re, in_im, init, notes, ur_o, ui_o, cr_o, ci_o, fr_o, fi_o, br_o, bi_o, source_o, gate_o, input_o, consts, message, lift_s, er_s, ei_s):
     parts, n, share = rows.shape[0], rows.shape[1] - 8, rows.shape[2]
     per = n // CHUNKS
     channels = w_value.shape[1]
+    groups, states = decay.shape[1], decay.shape[2]
+    wide = channels // groups
+    pairs = groups // 2
+    tiles = 2 * pairs
     row, col = iota((n, n), 0), iota((n, n), 1)
     ordered = col == (row % CHUNKS) * per + row // CHUNKS
     tail = rows[0, n : n + 8, 0:n].astype(F32)
     intervals = (tail[3:4] + tail[4:5]) + tail[5:6]
     steps = jnp.sum(jnp.where(ordered, intervals, 0.0), axis=1, keepdims=True)
     total = jnp.sum(intervals, axis=1, keepdims=True)
+    elapsed = sum(steps[i * CHUNKS : i * CHUNKS + CHUNKS] for i in range(per))
     order = jnp.where(ordered, 1.0, 0.0).astype(BF16)
+    consts[32:40, :] = notes[...]
+
+    def lanes_of(tile):
+        return slice(tile * 128, tile * 128 + 128)
+
+    def chunk_rows(tile):
+        return [slice(i * CHUNKS, i * CHUNKS + CHUNKS) for i in (reversed(range(per)) if tile >= pairs else range(per))]
+
+    def tabulate(tile):
+        d, q = tile // pairs, tile % pairs
+        lanes = lanes_of(tile)
+        rate, half_turn = row_of(decay, d, q), 0.5 * row_of(turn, d, q)
+        consts[tile : tile + 1, :] = rate
+        consts[8 + tile : 9 + tile, :] = half_turn
+        for part in range(2):
+            pair = [init[d, part, 2 * q + k : 2 * q + k + 1, :] for k in range(2)]
+            consts[16 + 8 * part + tile : 17 + 8 * part + tile, :] = jnp.concatenate(pair, axis=1)
+        sine, cosine, fall = turned_briefly(half_turn * 0.3183098861837907, steps)
+        magnitude, less_one = damped(0.5 * rate, steps)
+        fr_o[:, lanes] = magnitude * cosine
+        fi_o[:, lanes] = magnitude * sine
+        lift_s[:, lanes] = less_one * cosine - fall
+        er, ei = moved(elapsed, rate, half_turn)
+        er_s[:, lanes] = er
+        ei_s[:, lanes] = ei
+        br, bi, _, _ = scan_chunks(er, ei, None, None, tile >= pairs)
+        br_o[:, lanes] = one_later(br, tile >= pairs, 1.0)
+        bi_o[:, lanes] = one_later(bi, tile >= pairs, 0.0)
 
     squares = 0.0
     for k in range(parts):
@@ -139,6 +179,8 @@
         at = slice(k * share, k * share + share)
         first = first + dot(normed, jnp.concatenate([w_value[at, :], w_mix[at, :]], axis=1))
         second = second + dot(normed, jnp.concatenate([w_gate[at, :], w_state[at, :]], axis=1))
+        for tile in range(k * tiles // parts, (k + 1) * tiles // parts):
+            tabulate(tile)
     first = dot(order, first.astype(BF16))
     second = dot(order, second.astype(BF16))
     source = (first[:, :channels] * first[:, channels:]).astype(BF16).astype(F32)
@@ -146,12 +188,8 @@
     gate_o[...] = second[:, :channels]
     input_o[...] = second[:, channels:]
     state = second[:, channels:].astype(BF16)
-    state = jnp.concatenate([state, state], axis=1)
-
-    groups, states = decay.shape[1], decay.shape[2]
-    wide = channels // groups
-    pairs = groups // 2
-    consts[32:40, :] = notes[...]
+
+    block = 2 * wide
     edges = []
     for d in range(2):
         backward = d == 1
@@ -161,46 +199,26 @@
         inv_im = jnp.broadcast_to((-turns * inverse)[:, None, :], (groups, wide, states)).reshape(channels, states)
         at = slice(d * channels, d * channels + channels)
         scaled_re, scaled_im = cmul(in_re[at, :], in_im[at, :], inv_re, inv_im)
-        scaled_re, scaled_im = doubled(scaled_re), doubled(scaled_im)
+        scaled = (doubled(scaled_re), doubled(scaled_im))
+        mine = iota((block, 128), 0) // wide == iota((block, 128), 1) // states
         for q in range(pairs):
             tile = d * pairs + q
-            lanes = slice(tile * 128, tile * 128 + 128)
-            rate, turning = row_of(decay, d, q), row_of(turn, d, q)
-            consts[tile : tile + 1, :] = rate
-            consts[8 + tile : 9 + tile, :] = turning
-            consts[16 + tile : 17 + tile, :] = jnp.concatenate([init[d, 0, 2 * q : 2 * q + 1, :], init[d, 0, 2 * q + 1 : 2 * q + 2, :]], axis=1)
-            consts[24 + tile : 25 + tile, :] = jnp.concatenate([init[d, 1, 2 * q : 2 * q + 1, :], init[d, 1, 2 * q + 1 : 2 * q + 2, :]], axis=1)
-            mine = iota((channels, 128), 0) // wide == 2 * q + iota((channels, 128), 1) // states
-            re_hi, re_lo = halves(jnp.where(mine, scaled_re, 0.0))
-            im_hi, im_lo = halves(jnp.where(mine, scaled_im, 0.0))
-            matrix = jnp.concatenate([jnp.concatenate([re_hi, re_lo], axis=0), jnp.concatenate([im_hi, im_lo], axis=0)], axis=1)
-            driven = dot(state, matrix)
-            damping = -rate * steps
-            s, c = sin_cos((0.5 * turning) * steps)
-            magnitude = jnp.exp(damping)
-            twice = 2.0 * s * s
-            cosine = 1.0 - twice
-            fr = magnitude * cosine
-            fi = magnitude * (2.0 * s * c)
-            lift = exp_less_one(damping) * cosine - twice
-            push_re, push_im = cmul(lift, fi, driven[:, :128], driven[:, 128:])
-            cr = ci = hr = hi = None
-            for i in reversed(range(per)) if backward else range(per):
-                at = slice(i * CHUNKS, i * CHUNKS + CHUNKS)
-                r, m = fr[at], fi[at]
-                if cr is None:
-                    cr, ci, hr, hi = r, m, push_re[at], push_im[at]
+            lanes = lanes_of(tile)
+            some = slice(q * block, q * block + block)
+            matrix = jnp.concatenate([jnp.concatenate(halves(jnp.where(mine, x[some], 0.0)), axis=0) for x in scaled], axis=1)
+            driven = dot(jnp.concatenate([state[:, some], state[:, some]], axis=1), matrix)
+            fr, fi = fr_o[:, lanes], fi_o[:, lanes]
+            push_re, push_im = cmul(lift_s[:, lanes], fi, driven[:, :128], driven[:, 128:])
+            ur_o[:, lanes] = push_re
+            ui_o[:, lanes] = push_im
+            hr = hi = None
+            for at in chunk_rows(tile):
+                if hr is None:
+                    hr, hi = push_re[at], push_im[at]
                 else:
-                    cr, ci = cmul(r, m, cr, ci)
-                    ar, ai = cmul(r, m, hr, hi)
+                    ar, ai = cmul(fr[at], fi[at], hr, hi)
                     hr, hi = ar + push_re[at], ai + push_im[at]
-                pr_o[at, lanes] = cr
-                pi_o[at, lanes] = ci
-                hr_o[at, lanes] = hr
-                hi_o[at, lanes] = hi
-            br, bi, lr, li = scan_chunks(cr, ci, hr, hi, backward)
-            br_o[:, lanes] = one_later(br, backward, 1.0)
-            bi_o[:, lanes] = one_later(bi, backward, 0.0)
+            _, _, lr, li = scan_chunks(er_s[:, lanes], ei_s[:, lanes], hr, hi, backward)
             cr_o[:, lanes] = one_later(lr, backward, 0.0)
             ci_o[:, lanes] = one_later(li, backward, 0.0)
             edge = 0 if backward else CHUNKS - 1
@@ -260,7 +278,7 @@
         message[k] = jnp.where(plane < k, later, earlier).astype(BF16)
 
 
-def finish_kernel(got, inner, consts, hr_i, hi_i, cr_i, ci_i, pr, pi, br, bi, rd_re, rd_im, source, gate, state, proj_conv, proj_state, out):
+def finish_kernel(got, inner, consts, ur, ui, cr_i, ci_i, fr, fi, br, bi, rd_re, rd_im, source, gate, state, proj_conv, proj_state, out):
     size = got.shape[0]
     here, plane = lax.axis_index(SP[1:]), lax.axis_index(SP[0])
     last = lax.axis_size(SP[1:]) - 1
@@ -281,7 +299,7 @@
     ar, ai = cmul(inner[16:24, :], inner[24:32, :], hr, hi)
     inc_re = ar + inner[0:8, :]
     inc_im = ai + inner[8:16, :]
-    n, width = hr_i.shape
+    n, width = ur.shape
     per = n // CHUNKS
     channels = rd_re.shape[0] // 2
     states = rd_re.shape[1]
@@ -296,10 +314,14 @@
             tile = d * pairs + q
             lanes = slice(tile * 128, tile * 128 + 128)
             er, ei = cmul(br[:, lanes], bi[:, lanes], inc_re[tile : tile + 1], inc_im[tile : tile + 1])
-            er = jnp.concatenate([er + cr_i[:, lanes]] * per, axis=0)
-            ei = jnp.concatenate([ei + ci_i[:, lanes]] * per, axis=0)
-            ar, ai = cmul(pr[:, lanes], pi[:, lanes], er, ei)
-            full += [ar + hr_i[:, lanes], ai + hi_i[:, lanes]]
+            hr, hi = er + cr_i[:, lanes], ei + ci_i[:, lanes]
+            history = [None] * per
+            for i in reversed(range(per)) if d == 1 else range(per):
+                at = slice(i * CHUNKS, i * CHUNKS + CHUNKS)
+                ar, ai = cmul(fr[at, lanes], fi[at, lanes], hr, hi)
+                hr, hi = ar + ur[at, lanes], ai + ui[at, lanes]
+                history[i] = (hr, hi)
+            full += [jnp.concatenate([x[part] for x in history], axis=0) for part in range(2)]
             at = slice(d * channels + q * block, d * channels + (q + 1) * block)
             matrix += [jnp.where(mine, doubled(rd_re[at, :]), 0.0), jnp.where(mine, -doubled(rd_im[at, :]), 0.0)]
         high, low = halves(jnp.concatenate(full, axis=1))
@@ -337,13 +359,15 @@
 VMEM = pl.BlockSpec(memory_space=pltpu.VMEM)
 
 
-def call(kernel, shapes, *args, name=None):
+def call(kernel, shapes, *args, scratch=(), bytes_moved=10**6, name=None):
     return pl.pallas_call(
         kernel,
         out_shape=[jax.ShapeDtypeStruct(s, d) for s, d in shapes],
         in_specs=[VMEM] * len(args),
         out_specs=[VMEM] * len(shapes),
+        scratch_shapes=scratch,
         compiler_params=pltpu.CompilerParams(vmem_limit_bytes=24 * 2**20),
+        cost_estimate=pl.CostEstimate(flops=10**9, bytes_accessed=bytes_moved, transcendentals=0),
         name=name,
     )(*args)
 
@@ -375,22 +399,20 @@
     planes = lax.axis_size(SP[0])
     channels = w_value.shape[1]
     width = decay_rate.size
-    packed, notes = pl.pallas_call(
+    (blank,) = call(lead_kernel, [((8, channels), F32)], bytes_moved=3 * 10**8, name="lead")
+    packed, notes = call(
         pack_kernel,
-        out_shape=[jax.ShapeDtypeStruct((parts, n + 8, share), BF16), jax.ShapeDtypeStruct((8, channels), F32)],
-        in_specs=[VMEM] * 5,
-        out_specs=[VMEM] * 2,
-        scratch_shapes=[pltpu.SemaphoreType.DMA((parts,))],
-        compiler_params=pltpu.CompilerParams(vmem_limit_bytes=4 * 2**20),
-        cost_estimate=pl.CostEstimate(flops=10**9, bytes_accessed=3 * 10**8, transcendentals=0),
+        [((parts, n + 8, share), BF16), ((8, channels), F32)],
+        stream, norm_gain.reshape(1, -1), intervals.reshape(1, n), conv_taps, skip_gain.reshape(1, -1), blank,
+        bytes_moved=3 * 10**8,
         name="pack",
-    )(stream, norm_gain.reshape(1, -1), intervals.reshape(1, n), conv_taps, skip_gain.reshape(1, -1))
+    )
     rows = exchange(packed, "tp")
 
     states = ((n, width), F32)
     chunks = ((CHUNKS, width), F32)
     mixed = ((n, channels), F32)
-    hr, hi, cr, ci, pr, pi, br, bi, source, gate, state, consts, message = call(
+    ur, ui, cr, ci, fr, fi, br, bi, source, gate, state, consts, message = call(
         local_kernel,
         [states, states, chunks, chunks, states, states, chunks, chunks, mixed, mixed, mixed]
         + [((40, channels), F32), ((inside, 24, 128), F32)],
@@ -398,6 +420,7 @@
         jnp.swapaxes(input_real, 2, 3).reshape(2 * channels, -1),
         jnp.swapaxes(input_imag, 2, 3).reshape(2 * channels, -1),
         initial_state, notes,
+        scratch=[pltpu.VMEM((n, width), F32)] + [pltpu.VMEM((CHUNKS, width), F32)] * 2,
         name="local",
     )
     inner, message = call(
@@ -410,7 +433,7 @@
     (partial,) = call(
         finish_kernel,
         [((parts, n, share), BF16)],
-        got, inner, consts, hr, hi, cr, ci, pr, pi, br, bi,
+        got, inner, consts, ur, ui, cr, ci, fr, fi, br, bi,
         read_real.reshape(2 * channels, -1), read_imag.reshape(2 * channels, -1), source, gate, state,
         proj_conv, proj_state,
         name="finish",

time: 69.3 us -> 67.5 us (0.974)
  the two profiles are of different devices: /device:TPU:32 before, /device:TPU:2 now
where the time goes in v4:
time: 67.5 us; the launch traced here: 67.2 us
  blocking collectives  61.6 us (91%)
  Pallas kernels  3.67 us (5%)
  local copies, waits for them, and re-layouts  0.96 us (1%)
  other arithmetic  0.75 us (1%)
    all_to_all x4, blocking collectives, exchange(): return lax.all_to_all(x, axis, split_axis=0, concat_axis=0, tiled=True)  61.6 us
    pallas_call x5, Pallas kernels, call(): pl.pallas_call(kernel, out_shape=[jax.ShapeDtypeStruct(s, d) for s, d in...  3.67 us

profile of v4, /device:TPU:2, one launch (start us, length us, event | category | flops | bytes accessed | tf_op | source)
XLA Modules:
  0.0 67.2 jit_solution(14994642847296814727)
XLA Ops:
  0.0 0.0 copy-start.8
  0.0 0.0 copy-start.15
  0.0 0.0 copy-start.14
  0.0 0.0 copy-start.16
  0.0 0.0 copy-start.17
  0.0 0.9 %copy-done.8 = bf16[128,512]{1,0:T(8,128)(2,1)S(1)} copy-done((bf16[128,512]{1,0:T(8,128)(2,1)S(1)}, bf16[128,512]{1,0:T(8,128)(2,1)}, u32[]{:S(2)}) %copy-start.8) | copy-done | bytes 131096
  0.9 0.0 copy-done.15
  0.9 0.0 copy-done.14
  0.9 0.0 copy-done.16
  0.9 0.0 copy-done.17
  0.9 0.0 copy-start.6
  0.9 0.0 copy-start.7
  0.9 0.0 copy-start.9
  1.0 0.0 copy-start.10
  1.0 0.0 copy-start.4
  1.0 0.0 copy-start.5
  1.0 0.0 copy-start.11
  1.1 0.0 copy-start.12
  1.1 0.0 copy-start.13
  1.1 14.2 %all_to_all.20.rows = bf16[4,136,512]{2,1,0:T(8,128)(2,1)S(1)} all-to-all(bf16[4,136,512]{2,1,0:T(8,128)(2,1)S(1)} %get-tuple-element.22), channel_id=1, replica_groups=mesh['sp_0'=16,'sp_1'=4,'sp_2'=2,'tp'=4] {'tp'}, dimensions={0} | all-to-all | bytes 1114112 | tf_op jit(solution)/shard_map/all_to_all | solution.py:356
  15.3 0.0 copy-done.6
  15.3 0.0 copy-done.7
  15.3 0.0 copy-done.9
  15.3 0.0 copy-done.10
  15.3 0.0 copy-done.4
  15.3 0.0 copy-done.5
  15.3 0.0 copy-done.11
  15.4 0.0 copy-done.12
  15.4 0.0 copy-done.13
  15.4 2.1 %local.1 = (f32[128,1024]{1,0:T(8,128)S(1)}, f32[128,1024]{1,0:T(8,128)S(1)}, f32[8,1024]{1,0:T(8,128)S(1)}, f32[8,1024]{1,0:T(8,128)S(1)}, f32[128,1024]{1,0:T(...) custom-call(bf16[4,136,512]{2,1,0:T(8,128)(2,1)S(1)} %all_to_all.20., ...), custom_call_target="tpu_custom_call" | custom-call | flops 1000000000 | bytes 1000000 | tf_op jit(solution)/shard_map/local/pallas_call | solution.py:363
  17.5 9.1 %all_to_all.21.got = f32[8,24,128]{2,1,0:T(8,128)S(1)} all-to-all(f32[8,24,128]{2,1,0:T(8,128)S(1)} %get-tuple-element.24), channel_id=1, replica_groups=mesh['sp_0'=16,'sp_1'=4,'sp_2'=2,'tp'=4] {'sp_1','sp_2'}, dimensions={0} | all-to-all | bytes 196608 | tf_op jit(solution)/shard_map/all_to_all | solution.py:356
  26.6 0.0 copy-start
  26.7 0.0 copy-start.1
  26.7 0.0 copy-start.3
  26.7 0.1 plane.1
  26.7 0.0 copy-start.2
  26.8 27.7 %all_to_all.22.got = bf16[16,16,128]{2,1,0:T(8,128)(2,1)S(1)} all-to-all(bf16[16,16,128]{2,1,0:T(8,128)(2,1)S(1)} %get-tuple-element.26), channel_id=1, replica_groups=mesh['sp_0'=16,'sp_1'=4,'sp_2'=2,'tp'=4] {'sp_0'}, dimensions={0} | all-to-all | bytes 131072 | tf_op jit(solution)/shard_map/all_to_all | solution.py:356
  54.4 0.0 copy-done
  54.4 0.0 copy-done.1
  54.4 0.0 copy-done.3
  54.4 0.0 copy-done.2
  54.5 1.4 %finish.1 = bf16[4,128,512]{2,1,0:T(8,128)(2,1)S(1)} custom-call(bf16[16,16,128]{2,1,0:T(8,128)(2,1)S(1)} %all_to_all.22.got, f32[48,128]{1,0:T(8,128)S(1)} %get-tuple-element.27.inner, f32[40,128]{1,0:T(8,128)S(1)} %get-tuple-element.25.consts, f32[128,1024]{1,0:T(8,128)S(1)} %get-tuple-element.28.ur, f32[128,1024]{1,0:T(8,128)S(1)} %get-tuple-element.29.ui, ...), custom_call_target="tpu_custom_call" | custom-call | flops 1000000000 | bytes 1000000 | tf_op jit(solution)/shard_map/finish/pallas_call | solution.py:363
  55.9 10.6 %all_to_all.23 = bf16[4,128,512]{2,1,0:T(8,128)(2,1)S(1)} all-to-all(bf16[4,128,512]{2,1,0:T(8,128)(2,1)S(1)} %finish.1), channel_id=1, replica_groups=mesh['sp_0'=16,'sp_1'=4,'sp_2'=2,'tp'=4] {'tp'}, dimensions={0} | all-to-all | bytes 1048576 | tf_op jit(solution)/shard_map/all_to_all | solution.py:356
  66.5 0.7 %reduce_sum.12 = bf16[128,512]{1,0:T(8,128)(2,1)} reduce(bf16[4,128,512]{2,1,0:T(8,128)(2,1)S(1)} %all_to_all.23, bf16[]{:T(256)} %constant.2.clone.1), dimensions={0}, to_apply=%region_0.0 | reduce | flops 196608 | bytes 655362 | tf_op jit(solution)/shard_map/reduce_sum | solution.py:442
  (2 shorter events, 0.0 us)
Async XLA Ops:
  0.0 0.9 %copy-start.8 = (bf16[128,512]{1,0:T(8,128)(2,1)S(1)}, bf16[128,512]{1,0:T(8,128)(2,1)}, u32[]{:S(2)}) copy-start(bf16[128,512]{1,0:T(8,128)(2,1)} %stream.1) | copy-start | bytes 393220
  0.0 0.9 %copy-start.15 = (f32[3,128]{1,0:T(4,128)S(1)}, f32[3,128]{1,0:T(4,128)}, u32[]{:S(2)}) copy-start(f32[3,128]{1,0:T(4,128)} %taps.1) | copy-start | bytes 4612
  0.0 0.9 %copy-start.14 = (f32[512]{0:T(512)S(1)}, f32[512]{0:T(512)}, u32[]{:S(2)}) copy-start(f32[512]{0:T(512)} %param.19) | copy-start | bytes 6148
  0.0 0.9 %copy-start.16 = (f32[128]{0:T(128)S(1)}, f32[128]{0:T(128)}, u32[]{:S(2)}) copy-start(f32[128]{0:T(128)} %param.33) | copy-start | bytes 1540
  0.0 0.9 %copy-start.17 = (f32[128]{0:T(128)S(1)}, f32[128]{0:T(128)}, u32[]{:S(2)}) copy-start(f32[128]{0:T(128)} %param.25) | copy-start | bytes 1540
  0.9 14.4 %copy-start.6 = (bf16[2048,128]{1,0:T(8,128)(2,1)S(1)}, bf16[2048,128]{1,0:T(8,128)(2,1)}, u32[]{:S(2)}) copy-start(bf16[2048,128]{1,0:T(8,128)(2,1)} %w_gate.1) | copy-start | bytes 1572868
  0.9 14.4 %copy-start.7 = (bf16[2048,128]{1,0:T(8,128)(2,1)S(1)}, bf16[2048,128]{1,0:T(8,128)(2,1)}, u32[]{:S(2)}) copy-start(bf16[2048,128]{1,0:T(8,128)(2,1)} %w_state.1) | copy-start | bytes 1572868
  0.9 14.4 %copy-start.9 = (f32[2,8,64,16]{2,3,1,0:T(8,128)S(1)}, f32[2,8,64,16]{2,3,1,0:T(8,128)}, u32[]{:S(2)}) copy-start(f32[2,8,64,16]{2,3,1,0:T(8,128)} %param.28) | copy-start | bytes 196612
  1.0 14.4 %copy-start.10 = (f32[2,8,64,16]{2,3,1,0:T(8,128)S(1)}, f32[2,8,64,16]{2,3,1,0:T(8,128)}, u32[]{:S(2)}) copy-start(f32[2,8,64,16]{2,3,1,0:T(8,128)} %param.29) | copy-start | bytes 196612
  1.0 14.3 %copy-start.4 = (bf16[2048,128]{1,0:T(8,128)(2,1)S(1)}, bf16[2048,128]{1,0:T(8,128)(2,1)}, u32[]{:S(2)}) copy-start(bf16[2048,128]{1,0:T(8,128)(2,1)} %w_value.1) | copy-start | bytes 1572868
  1.0 14.3 %copy-start.5 = (bf16[2048,128]{1,0:T(8,128)(2,1)S(1)}, bf16[2048,128]{1,0:T(8,128)(2,1)}, u32[]{:S(2)}) copy-start(bf16[2048,128]{1,0:T(8,128)(2,1)} %w_mix.1) | copy-start | bytes 1572868
  1.0 14.3 %copy-start.11 = (f32[2,2,8,64]{3,2,1,0:T(8,128)S(1)}, f32[2,2,8,64]{3,2,1,0:T(8,128)}, u32[]{:S(2)}) copy-start(f32[2,2,8,64]{3,2,1,0:T(8,128)} %init.1) | copy-start | bytes 24580
  1.1 14.3 %copy-start.12 = (f32[2,8,64]{2,1,0:T(8,128)S(1)}, f32[2,8,64]{2,1,0:T(8,128)}, u32[]{:S(2)}) copy-start(f32[2,8,64]{2,1,0:T(8,128)} %decay.1) | copy-start | bytes 12292
  1.1 14.3 %copy-start.13 = (f32[2,8,64]{2,1,0:T(8,128)S(1)}, f32[2,8,64]{2,1,0:T(8,128)}, u32[]{:S(2)}) copy-start(f32[2,8,64]{2,1,0:T(8,128)} %turn.1) | copy-start | bytes 12292
  26.6 27.8 %copy-start = (bf16[128,2048]{1,0:T(8,128)(2,1)S(1)}, bf16[128,2048]{1,0:T(8,128)(2,1)}, u32[]{:S(2)}) copy-start(bf16[128,2048]{1,0:T(8,128)(2,1)} %proj_conv.1) | copy-start | bytes 1572868
  26.7 27.8 %copy-start.1 = (bf16[128,2048]{1,0:T(8,128)(2,1)S(1)}, bf16[128,2048]{1,0:T(8,128)(2,1)}, u32[]{:S(2)}) copy-start(bf16[128,2048]{1,0:T(8,128)(2,1)} %proj_state.1) | copy-start | bytes 1572868
  26.7 27.8 %copy-start.3 = (f32[2,8,16,64]{3,2,1,0:T(8,128)S(1)}, f32[2,8,16,64]{3,2,1,0:T(8,128)}, u32[]{:S(2)}) copy-start(f32[2,8,16,64]{3,2,1,0:T(8,128)} %param.31) | copy-start | bytes 196612
  26.7 27.7 %copy-start.2 = (f32[2,8,16,64]{3,2,1,0:T(8,128)S(1)}, f32[2,8,16,64]{3,2,1,0:T(8,128)}, u32[]{:S(2)}) copy-start(f32[2,8,16,64]{3,2,1,0:T(8,128)} %param.30) | copy-start | bytes 196612

commit v5 on v4

--- a/solution.py
+++ b/solution.py
@@ -223,18 +223,20 @@
             ci_o[:, lanes] = one_later(li, backward, 0.0)
             edge = 0 if backward else CHUNKS - 1
             edges.append((lr[edge : edge + 1], li[edge : edge + 1]))
+    high = total.astype(BF16).astype(F32)
+    mid = (total - high).astype(BF16).astype(F32)
+    lines = [r for r, m in edges] + [m for r, m in edges]
+    lines += [jnp.broadcast_to(x, (1, 128)) for x in (high, mid, total - high - mid)]
+    lines += [source[0:1], source[n - 1 : n], jnp.zeros((3, 128), F32)]
+    lines = jnp.concatenate(lines, axis=0).astype(BF16)
     for k in range(message.shape[0]):
-        for tile, (r, m) in enumerate(edges):
-            message[k, tile : tile + 1, :] = r
-            message[k, 8 + tile : 9 + tile, :] = m
-        message[k, 16:17, :] = jnp.broadcast_to(total, (1, 128))
-        message[k, 17:18, :] = source[0:1]
-        message[k, 18:19, :] = source[n - 1 : n]
-        message[k, 19:24, :] = jnp.zeros((5, 128), F32)
+        message[k] = lines
 
 
 def plane_kernel(got, consts, inner, message):
     size = got.shape[0]
+    came = [got[k].astype(F32) for k in range(size)]
+    times = [(x[16:17] + x[17:18]) + x[18:19] for x in came]
     here, plane = lax.axis_index(SP[1:]), lax.axis_index(SP[0])
     rate, turning = consts[0:8, :], consts[8:16, :]
     forward = iota((8, 128), 0) < 4
@@ -246,11 +248,11 @@
         ir = jnp.where(mine, hr, ir)
         ii = jnp.where(mine, hi, ii)
         before = jnp.where(mine, spent, before)
-        elapsed = jnp.where(forward, got[k, 16:17, :], got[m, 16:17, :])
+        elapsed = jnp.where(forward, times[k], times[m])
         ar, ai = moved(elapsed, rate, turning)
         ar, ai = cmul(ar, ai, hr, hi)
-        hr = ar + jnp.where(forward, got[k, 0:8, :], got[m, 0:8, :])
-        hi = ai + jnp.where(forward, got[k, 8:16, :], got[m, 8:16, :])
+        hr = ar + jnp.where(forward, came[k][0:8], came[m][0:8])
+        hi = ai + jnp.where(forward, came[k][8:16], came[m][8:16])
         spent = spent + elapsed
     wr, wi = moved(before, rate, turning)
     inner[0:8, :] = ir
@@ -259,21 +261,17 @@
     inner[24:32, :] = wi
     previous = following = jnp.zeros((1, 128), F32)
     for k in range(size):
-        previous = jnp.where(here - 1 == k, got[k, 18:19, :], previous)
-        following = jnp.where(here + 1 == k, got[k, 17:18, :], following)
+        previous = jnp.where(here - 1 == k, came[k][20:21], previous)
+        following = jnp.where(here + 1 == k, came[k][19:20], following)
     inner[32:40, :] = jnp.broadcast_to(previous, (8, 128))
     inner[40:48, :] = jnp.broadcast_to(following, (8, 128))
-    swapped = pltpu.roll(hi, 4, 0)
-    later = jnp.where(forward, hr, swapped)
-    earlier = jnp.where(forward, swapped, hr)
-    row = iota((8, 128), 0)
-    high = spent.astype(BF16).astype(F32)
-    mid = (spent - high).astype(BF16).astype(F32)
-    note = jnp.where(row == 0, high, jnp.where(row == 1, mid, jnp.where(row == 2, spent - high - mid, 0.0)))
-    note_later = jnp.where(row == 3, got[size - 1, 18:19, :], note)
-    note_earlier = jnp.where(row == 3, got[0, 17:18, :], note)
-    later = jnp.concatenate([later, note_later], axis=0)
-    earlier = jnp.concatenate([earlier, note_earlier], axis=0)
+    high = spent[0:1].astype(BF16).astype(F32)
+    mid = (spent[0:1] - high).astype(BF16).astype(F32)
+    note = [high, mid, spent[0:1] - high - mid]
+    note_later = jnp.concatenate(note + [came[size - 1][20:21]], axis=0)
+    note_earlier = jnp.concatenate(note + [came[0][19:20]], axis=0)
+    later = jnp.concatenate([hr[0:4], hi[0:4], note_later], axis=1)
+    earlier = jnp.concatenate([hr[4:8], hi[4:8], note_earlier], axis=1)
     for k in range(message.shape[0]):
         message[k] = jnp.where(plane < k, later, earlier).astype(BF16)
 
@@ -286,16 +284,15 @@
     forward = iota((8, 128), 0) < 4
     hr, hi = consts[16:24, :], consts[24:32, :]
     arrived = [got[k].astype(F32) for k in range(size)]
-    times = [(x[8:9] + x[9:10]) + x[10:11] for x in arrived]
+    times = [(x[0:1, 256:] + x[1:2, 256:]) + x[2:3, 256:] for x in arrived]
     for k in range(size):
         m = size - 1 - k
         active = (forward & (plane > k)) | (jnp.logical_not(forward) & (plane < m))
         elapsed = jnp.where(forward, times[k], times[m])
         ar, ai = moved(elapsed, rate, turning)
         ar, ai = cmul(ar, ai, hr, hi)
-        a, b = arrived[k][0:8], arrived[m][0:8]
-        hr = jnp.where(active, ar + jnp.where(forward, a, b), hr)
-        hi = jnp.where(active, ai + pltpu.roll(jnp.where(forward, b, a), 4, 0), hi)
+        hr = jnp.where(active, ar + jnp.concatenate([arrived[k][:, :128], arrived[m][:, :128]], axis=0), hr)
+        hi = jnp.where(active, ai + jnp.concatenate([arrived[k][:, 128:256], arrived[m][:, 128:256]], axis=0), hi)
     ar, ai = cmul(inner[16:24, :], inner[24:32, :], hr, hi)
     inc_re = ar + inner[0:8, :]
     inc_im = ai + inner[8:16, :]
@@ -332,8 +329,8 @@
     state_out = jax.nn.gelu(response).astype(BF16)
     previous, following = inner[32:33, :], inner[40:41, :]
     for k in range(size):
-        previous = jnp.where((here == 0) & (plane - 1 == k), arrived[k][11:12], previous)
-        following = jnp.where((here == last) & (plane + 1 == k), arrived[k][11:12], following)
+        previous = jnp.where((here == 0) & (plane - 1 == k), arrived[k][3:4, 256:], previous)
+        following = jnp.where((here == last) & (plane + 1 == k), arrived[k][3:4, 256:], following)
     x = source[...]
     row = iota((CHUNKS, x.shape[1]), 0)
     head = jnp.where(row == 0, previous, pltpu.roll(x[n - CHUNKS :], 1, 0))
@@ -415,7 +412,7 @@
     ur, ui, cr, ci, fr, fi, br, bi, source, gate, state, consts, message = call(
         local_kernel,
         [states, states, chunks, chunks, states, states, chunks, chunks, mixed, mixed, mixed]
-        + [((40, channels), F32), ((inside, 24, 128), F32)],
+        + [((40, channels), F32), ((inside, 24, 128), BF16)],
         rows, w_value, w_mix, w_gate, w_state, decay_rate, turn_rate,
         jnp.swapaxes(input_real, 2, 3).reshape(2 * channels, -1),
         jnp.swapaxes(input_imag, 2, 3).reshape(2 * channels, -1),
@@ -425,7 +422,7 @@
     )
     inner, message = call(
         plane_kernel,
-        [((48, 128), F32), ((planes, 16, 128), BF16)],
+        [((48, 128), F32), ((planes, 4, 384), BF16)],
         exchange(message, inner_axes), consts,
         name="plane",
     )

time: 67.5 us -> 67.3 us (level)
  no operation moved by 1% of the time
where the time goes in v5:
time: 67.3 us; the launch traced here: 67 us
  blocking collectives  61.4 us (91%)
  Pallas kernels  3.7 us (5%)
  local copies, waits for them, and re-layouts  0.95 us (1%)
  other arithmetic  0.75 us (1%)
    all_to_all x4, blocking collectives, exchange(): return lax.all_to_all(x, axis, split_axis=0, concat_axis=0, tiled=True)  61.4 us
    pallas_call x5, Pallas kernels, call(): pl.pallas_call(kernel, out_shape=[jax.ShapeDtypeStruct(s, d) for s, d in...  3.7 us

profile of v5, /device:TPU:2, one launch (start us, length us, event | category | flops | bytes accessed | tf_op | source)
XLA Modules:
  0.0 67.0 jit_solution(9560382836057291497)
XLA Ops:
  0.0 0.0 copy-start.8
  0.0 0.0 copy-start.15
  0.0 0.0 copy-start.14
  0.0 0.0 copy-start.16
  0.0 0.0 copy-start.17
  0.0 0.9 %copy-done.8 = bf16[128,512]{1,0:T(8,128)(2,1)S(1)} copy-done((bf16[128,512]{1,0:T(8,128)(2,1)S(1)}, bf16[128,512]{1,0:T(8,128)(2,1)}, u32[]{:S(2)}) %copy-start.8) | copy-done | bytes 131096
  0.9 0.0 copy-done.15
  0.9 0.0 copy-done.14
  0.9 0.0 copy-done.16
  0.9 0.0 copy-done.17
  0.9 0.0 copy-start.6
  0.9 0.0 copy-start.7
  0.9 0.0 copy-start.9
  1.0 0.0 copy-start.10
  1.0 0.0 copy-start.4
  1.0 0.0 copy-start.5
  1.0 0.0 copy-start.11
  1.1 0.0 copy-start.12
  1.1 0.0 copy-start.13
  1.1 14.2 %all_to_all.20.rows = bf16[4,136,512]{2,1,0:T(8,128)(2,1)S(1)} all-to-all(bf16[4,136,512]{2,1,0:T(8,128)(2,1)S(1)} %get-tuple-element.22), channel_id=1, replica_groups=mesh['sp_0'=16,'sp_1'=4,'sp_2'=2,'tp'=4] {'tp'}, dimensions={0} | all-to-all | bytes 1114112 | tf_op jit(solution)/shard_map/all_to_all | solution.py:353
  15.3 0.0 copy-done.6
  15.3 0.0 copy-done.7
  15.3 0.0 copy-done.9
  15.3 0.0 copy-done.10
  15.3 0.0 copy-done.4
  15.3 0.0 copy-done.5
  15.3 0.0 copy-done.11
  15.4 0.0 copy-done.12
  15.4 0.0 copy-done.13
  15.4 2.1 %local.1 = (f32[128,1024]{1,0:T(8,128)S(1)}, f32[128,1024]{1,0:T(8,128)S(1)}, f32[8,1024]{1,0:T(8,128)S(1)}, f32[8,1024]{1,0:T(8,128)S(1)}, f32[128,1024]{1,0:T(...) custom-call(bf16[4,136,512]{2,1,0:T(8,128)(2,1)S(1)} %all_to_all.20., ...), custom_call_target="tpu_custom_call" | custom-call | flops 1000000000 | bytes 1000000 | tf_op jit(solution)/shard_map/local/pallas_call | solution.py:360
  17.5 8.9 %all_to_all.21.got = bf16[8,24,128]{2,1,0:T(8,128)(2,1)S(1)} all-to-all(bf16[8,24,128]{2,1,0:T(8,128)(2,1)S(1)} %get-tuple-element.24), channel_id=1, replica_groups=mesh['sp_0'=16,'sp_1'=4,'sp_2'=2,'tp'=4] {'sp_1','sp_2'}, dimensions={0} | all-to-all | bytes 98304 | tf_op jit(solution)/shard_map/all_to_all | solution.py:353
  26.4 0.0 copy-start
  26.4 0.0 copy-start.1
  26.4 0.0 copy-start.2
  26.4 0.0 copy-start.3
  26.4 0.1 plane.1
  26.5 27.6 %all_to_all.22.got = bf16[16,4,384]{2,1,0:T(4,128)(2,1)S(1)} all-to-all(bf16[16,4,384]{2,1,0:T(4,128)(2,1)S(1)} %get-tuple-element.26), channel_id=1, replica_groups=mesh['sp_0'=16,'sp_1'=4,'sp_2'=2,'tp'=4] {'sp_0'}, dimensions={0} | all-to-all | bytes 98304 | tf_op jit(solution)/shard_map/all_to_all | solution.py:353
  54.1 0.0 copy-done
  54.1 0.0 copy-done.1
  54.1 0.0 copy-done.2
  54.1 0.0 copy-done.3
  54.1 1.4 %finish.1 = bf16[4,128,512]{2,1,0:T(8,128)(2,1)S(1)} custom-call(bf16[16,4,384]{2,1,0:T(4,128)(2,1)S(1)} %all_to_all.22.got, f32[48,128]{1,0:T(8,128)S(1)} %get-tuple-element.27.inner, f32[40,128]{1,0:T(8,128)S(1)} %get-tuple-element.25.consts, f32[128,1024]{1,0:T(8,128)S(1)} %get-tuple-element.28.ur, f32[128,1024]{1,0:T(8,128)S(1)} %get-tuple-element.29.ui, ...), custom_call_target="tpu_custom_call" | custom-call | flops 1000000000 | bytes 1000000 | tf_op jit(solution)/shard_map/finish/pallas_call | solution.py:360
  55.6 10.7 %all_to_all.23 = bf16[4,128,512]{2,1,0:T(8,128)(2,1)S(1)} all-to-all(bf16[4,128,512]{2,1,0:T(8,128)(2,1)S(1)} %finish.1), channel_id=1, replica_groups=mesh['sp_0'=16,'sp_1'=4,'sp_2'=2,'tp'=4] {'tp'}, dimensions={0} | all-to-all | bytes 1048576 | tf_op jit(solution)/shard_map/all_to_all | solution.py:353
  66.3 0.7 %reduce_sum.12 = bf16[128,512]{1,0:T(8,128)(2,1)} reduce(bf16[4,128,512]{2,1,0:T(8,128)(2,1)S(1)} %all_to_all.23, bf16[]{:T(256)} %constant.2.clone.1), dimensions={0}, to_apply=%region_0.0 | reduce | flops 196608 | bytes 655362 | tf_op jit(solution)/shard_map/reduce_sum | solution.py:439
  (2 shorter events, 0.0 us)
Async XLA Ops:
  0.0 0.9 %copy-start.8 = (bf16[128,512]{1,0:T(8,128)(2,1)S(1)}, bf16[128,512]{1,0:T(8,128)(2,1)}, u32[]{:S(2)}) copy-start(bf16[128,512]{1,0:T(8,128)(2,1)} %stream.1) | copy-start | bytes 393220
  0.0 0.9 %copy-start.15 = (f32[3,128]{1,0:T(4,128)S(1)}, f32[3,128]{1,0:T(4,128)}, u32[]{:S(2)}) copy-start(f32[3,128]{1,0:T(4,128)} %taps.1) | copy-start | bytes 4612
  0.0 0.9 %copy-start.14 = (f32[512]{0:T(512)S(1)}, f32[512]{0:T(512)}, u32[]{:S(2)}) copy-start(f32[512]{0:T(512)} %param.19) | copy-start | bytes 6148
  0.0 0.9 %copy-start.16 = (f32[128]{0:T(128)S(1)}, f32[128]{0:T(128)}, u32[]{:S(2)}) copy-start(f32[128]{0:T(128)} %param.33) | copy-start | bytes 1540
  0.0 0.9 %copy-start.17 = (f32[128]{0:T(128)S(1)}, f32[128]{0:T(128)}, u32[]{:S(2)}) copy-start(f32[128]{0:T(128)} %param.25) | copy-start | bytes 1540
  0.9 14.4 %copy-start.6 = (bf16[2048,128]{1,0:T(8,128)(2,1)S(1)}, bf16[2048,128]{1,0:T(8,128)(2,1)}, u32[]{:S(2)}) copy-start(bf16[2048,128]{1,0:T(8,128)(2,1)} %w_gate.1) | copy-start | bytes 1572868
  0.9 14.4 %copy-start.7 = (bf16[2048,128]{1,0:T(8,128)(2,1)S(1)}, bf16[2048,128]{1,0:T(8,128)(2,1)}, u32[]{:S(2)}) copy-start(bf16[2048,128]{1,0:T(8,128)(2,1)} %w_state.1) | copy-start | bytes 1572868
  0.9 14.4 %copy-start.9 = (f32[2,8,64,16]{2,3,1,0:T(8,128)S(1)}, f32[2,8,64,16]{2,3,1,0:T(8,128)}, u32[]{:S(2)}) copy-start(f32[2,8,64,16]{2,3,1,0:T(8,128)} %param.28) | copy-start | bytes 196612
  1.0 14.4 %copy-start.10 = (f32[2,8,64,16]{2,3,1,0:T(8,128)S(1)}, f32[2,8,64,16]{2,3,1,0:T(8,128)}, u32[]{:S(2)}) copy-start(f32[2,8,64,16]{2,3,1,0:T(8,128)} %param.29) | copy-start | bytes 196612
  1.0 14.3 %copy-start.4 = (bf16[2048,128]{1,0:T(8,128)(2,1)S(1)}, bf16[2048,128]{1,0:T(8,128)(2,1)}, u32[]{:S(2)}) copy-start(bf16[2048,128]{1,0:T(8,128)(2,1)} %w_value.1) | copy-start | bytes 1572868
  1.0 14.3 %copy-start.5 = (bf16[2048,128]{1,0:T(8,128)(2,1)S(1)}, bf16[2048,128]{1,0:T(8,128)(2,1)}, u32[]{:S(2)}) copy-start(bf16[2048,128]{1,0:T(8,128)(2,1)} %w_mix.1) | copy-start | bytes 1572868
  1.0 14.3 %copy-start.11 = (f32[2,2,8,64]{3,2,1,0:T(8,128)S(1)}, f32[2,2,8,64]{3,2,1,0:T(8,128)}, u32[]{:S(2)}) copy-start(f32[2,2,8,64]{3,2,1,0:T(8,128)} %init.1) | copy-start | bytes 24580
  1.1 14.3 %copy-start.12 = (f32[2,8,64]{2,1,0:T(8,128)S(1)}, f32[2,8,64]{2,1,0:T(8,128)}, u32[]{:S(2)}) copy-start(f32[2,8,64]{2,1,0:T(8,128)} %decay.1) | copy-start | bytes 12292
  1.1 14.3 %copy-start.13 = (f32[2,8,64]{2,1,0:T(8,128)S(1)}, f32[2,8,64]{2,1,0:T(8,128)}, u32[]{:S(2)}) copy-start(f32[2,8,64]{2,1,0:T(8,128)} %turn.1) | copy-start | bytes 12292
  26.4 27.7 %copy-start = (bf16[128,2048]{1,0:T(8,128)(2,1)S(1)}, bf16[128,2048]{1,0:T(8,128)(2,1)}, u32[]{:S(2)}) copy-start(bf16[128,2048]{1,0:T(8,128)(2,1)} %proj_conv.1) | copy-start | bytes 1572868
  26.4 27.7 %copy-start.1 = (bf16[128,2048]{1,0:T(8,128)(2,1)S(1)}, bf16[128,2048]{1,0:T(8,128)(2,1)}, u32[]{:S(2)}) copy-start(bf16[128,2048]{1,0:T(8,128)(2,1)} %proj_state.1) | copy-start | bytes 1572868
  26.4 27.7 %copy-start.2 = (f32[2,8,16,64]{3,2,1,0:T(8,128)S(1)}, f32[2,8,16,64]{3,2,1,0:T(8,128)}, u32[]{:S(2)}) copy-start(f32[2,8,16,64]{3,2,1,0:T(8,128)} %param.30) | copy-start | bytes 196612
  26.4 27.7 %copy-start.3 = (f32[2,8,16,64]{3,2,1,0:T(8,128)S(1)}, f32[2,8,16,64]{3,2,1,0:T(8,128)}, u32[]{:S(2)}) copy-start(f32[2,8,16,64]{3,2,1,0:T(8,128)} %param.31) | copy-start | bytes 196612

commit v6 on v5

--- a/solution.py
+++ b/solution.py
@@ -12,6 +12,7 @@
 F32 = jnp.float32
 BF16 = jnp.bfloat16
 CHUNKS = 8
+LONGEST = 1e30
 
 
 def turned(half_turn, elapsed):
@@ -134,8 +135,8 @@
     tail = rows[0, n : n + 8, 0:n].astype(F32)
     intervals = (tail[3:4] + tail[4:5]) + tail[5:6]
     steps = jnp.sum(jnp.where(ordered, intervals, 0.0), axis=1, keepdims=True)
-    total = jnp.sum(intervals, axis=1, keepdims=True)
-    elapsed = sum(steps[i * CHUNKS : i * CHUNKS + CHUNKS] for i in range(per))
+    total = jnp.minimum(jnp.sum(intervals, axis=1, keepdims=True), LONGEST)
+    elapsed = jnp.minimum(sum(steps[i * CHUNKS : i * CHUNKS + CHUNKS] for i in range(per)), LONGEST)
     order = jnp.where(ordered, 1.0, 0.0).astype(BF16)
     consts[32:40, :] = notes[...]
 
@@ -324,7 +325,8 @@
         high, low = halves(jnp.concatenate(full, axis=1))
         r_hi, r_lo = halves(jnp.concatenate(matrix, axis=1))
         across = ((1,), (1,))
-        responses.append((dot(low, r_hi, across) + dot(high, r_lo, across)) + dot(high, r_hi, across))
+        stacked = dot(jnp.concatenate([high, low], axis=0), r_hi, across)
+        responses.append((stacked[n:] + dot(high, r_lo, across)) + stacked[:n])
     response = state[...] * consts[35:36, :] + jnp.concatenate(responses, axis=1)
     state_out = jax.nn.gelu(response).astype(BF16)
     previous, following = inner[32:33, :], inner[40:41, :]

time: 67.3 us -> 67.3 us (level)
  no operation moved by 1% of the time
where the time goes in v6:
time: 67.3 us; the launch traced here: 67 us
  blocking collectives  61.4 us (91%)
  Pallas kernels  3.69 us (5%)
  local copies, waits for them, and re-layouts  0.95 us (1%)
  other arithmetic  0.75 us (1%)
    all_to_all x4, blocking collectives, exchange(): return lax.all_to_all(x, axis, split_axis=0, concat_axis=0, tiled=True)  61.4 us
    pallas_call x5, Pallas kernels, call(): pl.pallas_call(kernel, out_shape=[jax.ShapeDtypeStruct(s, d) for s, d in...  3.69 us

profile of v6, /device:TPU:2, one launch (start us, length us, event | category | flops | bytes accessed | tf_op | source)
XLA Modules:
  0.0 67.0 jit_solution(13414832570036942627)
XLA Ops:
  0.0 0.0 copy-start.8
  0.0 0.0 copy-start.15
  0.0 0.0 copy-start.14
  0.0 0.0 copy-start.16
  0.0 0.0 copy-start.17
  0.0 0.9 %copy-done.8 = bf16[128,512]{1,0:T(8,128)(2,1)S(1)} copy-done((bf16[128,512]{1,0:T(8,128)(2,1)S(1)}, bf16[128,512]{1,0:T(8,128)(2,1)}, u32[]{:S(2)}) %copy-start.8) | copy-done | bytes 131096
  0.9 0.0 copy-done.15
  0.9 0.0 copy-done.14
  0.9 0.0 copy-done.16
  0.9 0.0 copy-done.17
  0.9 0.0 copy-start.6
  0.9 0.0 copy-start.7
  0.9 0.0 copy-start.9
  1.0 0.0 copy-start.10
  1.0 0.0 copy-start.4
  1.0 0.0 copy-start.5
  1.0 0.0 copy-start.11
  1.1 0.0 copy-start.12
  1.1 0.0 copy-start.13
  1.1 14.2 %all_to_all.20.rows = bf16[4,136,512]{2,1,0:T(8,128)(2,1)S(1)} all-to-all(bf16[4,136,512]{2,1,0:T(8,128)(2,1)S(1)} %get-tuple-element.22), channel_id=1, replica_groups=mesh['sp_0'=16,'sp_1'=4,'sp_2'=2,'tp'=4] {'tp'}, dimensions={0} | all-to-all | bytes 1114112 | tf_op jit(solution)/shard_map/all_to_all | solution.py:355
  15.3 0.0 copy-done.6
  15.3 0.0 copy-done.7
  15.3 0.0 copy-done.9
  15.3 0.0 copy-done.10
  15.3 0.0 copy-done.4
  15.3 0.0 copy-done.5
  15.3 0.0 copy-done.11
  15.4 0.0 copy-done.12
  15.4 0.0 copy-done.13
  15.4 2.1 %local.1 = (f32[128,1024]{1,0:T(8,128)S(1)}, f32[128,1024]{1,0:T(8,128)S(1)}, f32[8,1024]{1,0:T(8,128)S(1)}, f32[8,1024]{1,0:T(8,128)S(1)}, f32[128,1024]{1,0:T(...) custom-call(bf16[4,136,512]{2,1,0:T(8,128)(2,1)S(1)} %all_to_all.20., ...), custom_call_target="tpu_custom_call" | custom-call | flops 1000000000 | bytes 1000000 | tf_op jit(solution)/shard_map/local/pallas_call | solution.py:362
  17.5 8.9 %all_to_all.21.got = bf16[8,24,128]{2,1,0:T(8,128)(2,1)S(1)} all-to-all(bf16[8,24,128]{2,1,0:T(8,128)(2,1)S(1)} %get-tuple-element.24), channel_id=1, replica_groups=mesh['sp_0'=16,'sp_1'=4,'sp_2'=2,'tp'=4] {'sp_1','sp_2'}, dimensions={0} | all-to-all | bytes 98304 | tf_op jit(solution)/shard_map/all_to_all | solution.py:355
  26.4 0.0 copy-start
  26.4 0.0 copy-start.1
  26.4 0.0 copy-start.2
  26.4 0.0 copy-start.3
  26.4 0.1 plane.1
  26.5 27.6 %all_to_all.22.got = bf16[16,4,384]{2,1,0:T(4,128)(2,1)S(1)} all-to-all(bf16[16,4,384]{2,1,0:T(4,128)(2,1)S(1)} %get-tuple-element.26), channel_id=1, replica_groups=mesh['sp_0'=16,'sp_1'=4,'sp_2'=2,'tp'=4] {'sp_0'}, dimensions={0} | all-to-all | bytes 98304 | tf_op jit(solution)/shard_map/all_to_all | solution.py:355
  54.1 0.0 copy-done
  54.1 0.0 copy-done.1
  54.1 0.0 copy-done.2
  54.1 0.0 copy-done.3
  54.1 1.4 %finish.1 = bf16[4,128,512]{2,1,0:T(8,128)(2,1)S(1)} custom-call(bf16[16,4,384]{2,1,0:T(4,128)(2,1)S(1)} %all_to_all.22.got, f32[48,128]{1,0:T(8,128)S(1)} %get-tuple-element.27.inner, f32[40,128]{1,0:T(8,128)S(1)} %get-tuple-element.25.consts, f32[128,1024]{1,0:T(8,128)S(1)} %get-tuple-element.28.ur, f32[128,1024]{1,0:T(8,128)S(1)} %get-tuple-element.29.ui, ...), custom_call_target="tpu_custom_call" | custom-call | flops 1000000000 | bytes 1000000 | tf_op jit(solution)/shard_map/finish/pallas_call | solution.py:362
  55.6 10.7 %all_to_all.23 = bf16[4,128,512]{2,1,0:T(8,128)(2,1)S(1)} all-to-all(bf16[4,128,512]{2,1,0:T(8,128)(2,1)S(1)} %finish.1), channel_id=1, replica_groups=mesh['sp_0'=16,'sp_1'=4,'sp_2'=2,'tp'=4] {'tp'}, dimensions={0} | all-to-all | bytes 1048576 | tf_op jit(solution)/shard_map/all_to_all | solution.py:355
  66.2 0.7 %reduce_sum.12 = bf16[128,512]{1,0:T(8,128)(2,1)} reduce(bf16[4,128,512]{2,1,0:T(8,128)(2,1)S(1)} %all_to_all.23, bf16[]{:T(256)} %constant.2.clone.1), dimensions={0}, to_apply=%region_0.0 | reduce | flops 196608 | bytes 655362 | tf_op jit(solution)/shard_map/reduce_sum | solution.py:441
  (2 shorter events, 0.0 us)
Async XLA Ops:
  0.0 0.9 %copy-start.8 = (bf16[128,512]{1,0:T(8,128)(2,1)S(1)}, bf16[128,512]{1,0:T(8,128)(2,1)}, u32[]{:S(2)}) copy-start(bf16[128,512]{1,0:T(8,128)(2,1)} %stream.1) | copy-start | bytes 393220
  0.0 0.9 %copy-start.15 = (f32[3,128]{1,0:T(4,128)S(1)}, f32[3,128]{1,0:T(4,128)}, u32[]{:S(2)}) copy-start(f32[3,128]{1,0:T(4,128)} %taps.1) | copy-start | bytes 4612
  0.0 0.9 %copy-start.14 = (f32[512]{0:T(512)S(1)}, f32[512]{0:T(512)}, u32[]{:S(2)}) copy-start(f32[512]{0:T(512)} %param.19) | copy-start | bytes 6148
  0.0 0.9 %copy-start.16 = (f32[128]{0:T(128)S(1)}, f32[128]{0:T(128)}, u32[]{:S(2)}) copy-start(f32[128]{0:T(128)} %param.33) | copy-start | bytes 1540
  0.0 0.9 %copy-start.17 = (f32[128]{0:T(128)S(1)}, f32[128]{0:T(128)}, u32[]{:S(2)}) copy-start(f32[128]{0:T(128)} %param.25) | copy-start | bytes 1540
  0.9 14.4 %copy-start.6 = (bf16[2048,128]{1,0:T(8,128)(2,1)S(1)}, bf16[2048,128]{1,0:T(8,128)(2,1)}, u32[]{:S(2)}) copy-start(bf16[2048,128]{1,0:T(8,128)(2,1)} %w_gate.1) | copy-start | bytes 1572868
  0.9 14.4 %copy-start.7 = (bf16[2048,128]{1,0:T(8,128)(2,1)S(1)}, bf16[2048,128]{1,0:T(8,128)(2,1)}, u32[]{:S(2)}) copy-start(bf16[2048,128]{1,0:T(8,128)(2,1)} %w_state.1) | copy-start | bytes 1572868
  0.9 14.4 %copy-start.9 = (f32[2,8,64,16]{2,3,1,0:T(8,128)S(1)}, f32[2,8,64,16]{2,3,1,0:T(8,128)}, u32[]{:S(2)}) copy-start(f32[2,8,64,16]{2,3,1,0:T(8,128)} %param.28) | copy-start | bytes 196612
  1.0 14.4 %copy-start.10 = (f32[2,8,64,16]{2,3,1,0:T(8,128)S(1)}, f32[2,8,64,16]{2,3,1,0:T(8,128)}, u32[]{:S(2)}) copy-start(f32[2,8,64,16]{2,3,1,0:T(8,128)} %param.29) | copy-start | bytes 196612
  1.0 14.3 %copy-start.4 = (bf16[2048,128]{1,0:T(8,128)(2,1)S(1)}, bf16[2048,128]{1,0:T(8,128)(2,1)}, u32[]{:S(2)}) copy-start(bf16[2048,128]{1,0:T(8,128)(2,1)} %w_value.1) | copy-start | bytes 1572868
  1.0 14.3 %copy-start.5 = (bf16[2048,128]{1,0:T(8,128)(2,1)S(1)}, bf16[2048,128]{1,0:T(8,128)(2,1)}, u32[]{:S(2)}) copy-start(bf16[2048,128]{1,0:T(8,128)(2,1)} %w_mix.1) | copy-start | bytes 1572868
  1.0 14.3 %copy-start.11 = (f32[2,2,8,64]{3,2,1,0:T(8,128)S(1)}, f32[2,2,8,64]{3,2,1,0:T(8,128)}, u32[]{:S(2)}) copy-start(f32[2,2,8,64]{3,2,1,0:T(8,128)} %init.1) | copy-start | bytes 24580
  1.1 14.3 %copy-start.12 = (f32[2,8,64]{2,1,0:T(8,128)S(1)}, f32[2,8,64]{2,1,0:T(8,128)}, u32[]{:S(2)}) copy-start(f32[2,8,64]{2,1,0:T(8,128)} %decay.1) | copy-start | bytes 12292
  1.1 14.3 %copy-start.13 = (f32[2,8,64]{2,1,0:T(8,128)S(1)}, f32[2,8,64]{2,1,0:T(8,128)}, u32[]{:S(2)}) copy-start(f32[2,8,64]{2,1,0:T(8,128)} %turn.1) | copy-start | bytes 12292
  26.4 27.7 %copy-start = (bf16[128,2048]{1,0:T(8,128)(2,1)S(1)}, bf16[128,2048]{1,0:T(8,128)(2,1)}, u32[]{:S(2)}) copy-start(bf16[128,2048]{1,0:T(8,128)(2,1)} %proj_conv.1) | copy-start | bytes 1572868
  26.4 27.7 %copy-start.1 = (bf16[128,2048]{1,0:T(8,128)(2,1)S(1)}, bf16[128,2048]{1,0:T(8,128)(2,1)}, u32[]{:S(2)}) copy-start(bf16[128,2048]{1,0:T(8,128)(2,1)} %proj_state.1) | copy-start | bytes 1572868
  26.4 27.7 %copy-start.2 = (f32[2,8,16,64]{3,2,1,0:T(8,128)S(1)}, f32[2,8,16,64]{3,2,1,0:T(8,128)}, u32[]{:S(2)}) copy-start(f32[2,8,16,64]{3,2,1,0:T(8,128)} %param.30) | copy-start | bytes 196612
  26.4 27.7 %copy-start.3 = (f32[2,8,16,64]{3,2,1,0:T(8,128)S(1)}, f32[2,8,16,64]{3,2,1,0:T(8,128)}, u32[]{:S(2)}) copy-start(f32[2,8,16,64]{3,2,1,0:T(8,128)} %param.31) | copy-start | bytes 196612

commit v7 on v6

--- a/solution.py
+++ b/solution.py
@@ -13,6 +13,7 @@
 BF16 = jnp.bfloat16
 CHUNKS = 8
 LONGEST = 1e30
+LOG2E = 1.4426950408889634
 
 
 def turned(half_turn, elapsed):
@@ -39,7 +40,7 @@
 
 def damped(half_rate, elapsed):
     x = half_rate * elapsed
-    root = jnp.exp(-x)
+    root = jnp.exp2(x * -LOG2E)
     magnitude = root * root
     square = x * x
     series = root * (x * (-2.0 - square * (1 / 3 + square * (1 / 60))))
@@ -47,7 +48,7 @@
 
 
 def moved(elapsed, rate, half_turn):
-    magnitude = jnp.exp(-rate * elapsed)
+    magnitude = jnp.exp2((rate * -LOG2E) * elapsed)
     sine, cosine, _ = turned(half_turn, elapsed)
     return magnitude * cosine, magnitude * sine
 
@@ -345,10 +346,11 @@
     order = jnp.where(row == (col % CHUNKS) * per + col // CHUNKS, 1.0, 0.0).astype(BF16)
     conv_out = dot(order, conv_out).astype(BF16)
     state_out = dot(order, state_out).astype(BF16)
+    both = jnp.concatenate([conv_out, state_out], axis=1)
     share = out.shape[2]
     for k in range(out.shape[0]):
         at = slice(k * share, k * share + share)
-        out[k] = (dot(conv_out, proj_conv[:, at]) + dot(state_out, proj_state[:, at])).astype(BF16)
+        out[k] = dot(both, jnp.concatenate([proj_conv[:, at], proj_state[:, at]], axis=0)).astype(BF16)
 
 
 def exchange(x, axis):

time: 67.3 us -> 67.1 us (level)
  no operation moved by 1% of the time
where the time goes in v7:
time: 67.1 us; the launch traced here: 66.8 us
  blocking collectives  61.4 us (92%)
  Pallas kernels  3.53 us (5%)
  local copies, waits for them, and re-layouts  0.95 us (1%)
  other arithmetic  0.75 us (1%)
    all_to_all x4, blocking collectives, exchange(): return lax.all_to_all(x, axis, split_axis=0, concat_axis=0, tiled=True)  61.4 us
    pallas_call x5, Pallas kernels, call(): pl.pallas_call(kernel, out_shape=[jax.ShapeDtypeStruct(s, d) for s, d in...  3.53 us

profile of v7, /device:TPU:2, one launch (start us, length us, event | category | flops | bytes accessed | tf_op | source)
XLA Modules:
  0.0 66.8 jit_solution(118154352551703975)
XLA Ops:
  0.0 0.0 copy-start.8
  0.0 0.0 copy-start.15
  0.0 0.0 copy-start.14
  0.0 0.0 copy-start.16
  0.0 0.0 copy-start.17
  0.0 0.9 %copy-done.8 = bf16[128,512]{1,0:T(8,128)(2,1)S(1)} copy-done((bf16[128,512]{1,0:T(8,128)(2,1)S(1)}, bf16[128,512]{1,0:T(8,128)(2,1)}, u32[]{:S(2)}) %copy-start.8) | copy-done | bytes 131096
  0.9 0.0 copy-done.15
  0.9 0.0 copy-done.14
  0.9 0.0 copy-done.16
  0.9 0.0 copy-done.17
  0.9 0.0 copy-start.6
  0.9 0.0 copy-start.7
  0.9 0.0 copy-start.9
  1.0 0.0 copy-start.10
  1.0 0.0 copy-start.4
  1.0 0.0 copy-start.5
  1.0 0.0 copy-start.11
  1.1 0.0 copy-start.12
  1.1 0.0 copy-start.13
  1.1 14.2 %all_to_all.20.rows = bf16[4,136,512]{2,1,0:T(8,128)(2,1)S(1)} all-to-all(bf16[4,136,512]{2,1,0:T(8,128)(2,1)S(1)} %get-tuple-element.22), channel_id=1, replica_groups=mesh['sp_0'=16,'sp_1'=4,'sp_2'=2,'tp'=4] {'tp'}, dimensions={0} | all-to-all | bytes 1114112 | tf_op jit(solution)/shard_map/all_to_all | solution.py:357
  15.3 0.0 copy-done.6
  15.3 0.0 copy-done.7
  15.3 0.0 copy-done.9
  15.3 0.0 copy-done.10
  15.3 0.0 copy-done.4
  15.3 0.0 copy-done.5
  15.3 0.0 copy-done.11
  15.4 0.0 copy-done.12
  15.4 0.0 copy-done.13
  15.4 2.1 %local.1 = (f32[128,1024]{1,0:T(8,128)S(1)}, f32[128,1024]{1,0:T(8,128)S(1)}, f32[8,1024]{1,0:T(8,128)S(1)}, f32[8,1024]{1,0:T(8,128)S(1)}, f32[128,1024]{1,0:T(...) custom-call(bf16[4,136,512]{2,1,0:T(8,128)(2,1)S(1)} %all_to_all.20., ...), custom_call_target="tpu_custom_call" | custom-call | flops 1000000000 | bytes 1000000 | tf_op jit(solution)/shard_map/local/pallas_call | solution.py:364
  17.5 8.9 %all_to_all.21.got = bf16[8,24,128]{2,1,0:T(8,128)(2,1)S(1)} all-to-all(bf16[8,24,128]{2,1,0:T(8,128)(2,1)S(1)} %get-tuple-element.24), channel_id=1, replica_groups=mesh['sp_0'=16,'sp_1'=4,'sp_2'=2,'tp'=4] {'sp_1','sp_2'}, dimensions={0} | all-to-all | bytes 98304 | tf_op jit(solution)/shard_map/all_to_all | solution.py:357
  26.3 0.0 copy-start
  26.3 0.0 copy-start.1
  26.3 0.0 copy-start.2
  26.3 0.0 copy-start.3
  26.4 0.1 plane.1
  26.5 27.6 %all_to_all.22.got = bf16[16,4,384]{2,1,0:T(4,128)(2,1)S(1)} all-to-all(bf16[16,4,384]{2,1,0:T(4,128)(2,1)S(1)} %get-tuple-element.26), channel_id=1, replica_groups=mesh['sp_0'=16,'sp_1'=4,'sp_2'=2,'tp'=4] {'sp_0'}, dimensions={0} | all-to-all | bytes 98304 | tf_op jit(solution)/shard_map/all_to_all | solution.py:357
  54.1 0.0 copy-done
  54.1 0.0 copy-done.1
  54.1 0.0 copy-done.2
  54.1 0.0 copy-done.3
  54.1 1.3 %finish.1 = bf16[4,128,512]{2,1,0:T(8,128)(2,1)S(1)} custom-call(bf16[16,4,384]{2,1,0:T(4,128)(2,1)S(1)} %all_to_all.22.got, f32[48,128]{1,0:T(8,128)S(1)} %get-tuple-element.27.inner, f32[40,128]{1,0:T(8,128)S(1)} %get-tuple-element.25.consts, f32[128,1024]{1,0:T(8,128)S(1)} %get-tuple-element.28.ur, f32[128,1024]{1,0:T(8,128)S(1)} %get-tuple-element.29.ui, ...), custom_call_target="tpu_custom_call" | custom-call | flops 1000000000 | bytes 1000000 | tf_op jit(solution)/shard_map/finish/pallas_call | solution.py:364
  55.4 10.7 %all_to_all.23 = bf16[4,128,512]{2,1,0:T(8,128)(2,1)S(1)} all-to-all(bf16[4,128,512]{2,1,0:T(8,128)(2,1)S(1)} %finish.1), channel_id=1, replica_groups=mesh['sp_0'=16,'sp_1'=4,'sp_2'=2,'tp'=4] {'tp'}, dimensions={0} | all-to-all | bytes 1048576 | tf_op jit(solution)/shard_map/all_to_all | solution.py:357
  66.1 0.7 %reduce_sum.12 = bf16[128,512]{1,0:T(8,128)(2,1)} reduce(bf16[4,128,512]{2,1,0:T(8,128)(2,1)S(1)} %all_to_all.23, bf16[]{:T(256)} %constant.2.clone.1), dimensions={0}, to_apply=%region_0.0 | reduce | flops 196608 | bytes 655362 | tf_op jit(solution)/shard_map/reduce_sum | solution.py:443
  (2 shorter events, 0.0 us)
Async XLA Ops:
  0.0 0.9 %copy-start.8 = (bf16[128,512]{1,0:T(8,128)(2,1)S(1)}, bf16[128,512]{1,0:T(8,128)(2,1)}, u32[]{:S(2)}) copy-start(bf16[128,512]{1,0:T(8,128)(2,1)} %stream.1) | copy-start | bytes 393220
  0.0 0.9 %copy-start.15 = (f32[3,128]{1,0:T(4,128)S(1)}, f32[3,128]{1,0:T(4,128)}, u32[]{:S(2)}) copy-start(f32[3,128]{1,0:T(4,128)} %taps.1) | copy-start | bytes 4612
  0.0 0.9 %copy-start.14 = (f32[512]{0:T(512)S(1)}, f32[512]{0:T(512)}, u32[]{:S(2)}) copy-start(f32[512]{0:T(512)} %param.19) | copy-start | bytes 6148
  0.0 0.9 %copy-start.16 = (f32[128]{0:T(128)S(1)}, f32[128]{0:T(128)}, u32[]{:S(2)}) copy-start(f32[128]{0:T(128)} %param.33) | copy-start | bytes 1540
  0.0 0.9 %copy-start.17 = (f32[128]{0:T(128)S(1)}, f32[128]{0:T(128)}, u32[]{:S(2)}) copy-start(f32[128]{0:T(128)} %param.25) | copy-start | bytes 1540
  0.9 14.4 %copy-start.6 = (bf16[2048,128]{1,0:T(8,128)(2,1)S(1)}, bf16[2048,128]{1,0:T(8,128)(2,1)}, u32[]{:S(2)}) copy-start(bf16[2048,128]{1,0:T(8,128)(2,1)} %w_gate.1) | copy-start | bytes 1572868
  0.9 14.4 %copy-start.7 = (bf16[2048,128]{1,0:T(8,128)(2,1)S(1)}, bf16[2048,128]{1,0:T(8,128)(2,1)}, u32[]{:S(2)}) copy-start(bf16[2048,128]{1,0:T(8,128)(2,1)} %w_state.1) | copy-start | bytes 1572868
  0.9 14.4 %copy-start.9 = (f32[2,8,64,16]{2,3,1,0:T(8,128)S(1)}, f32[2,8,64,16]{2,3,1,0:T(8,128)}, u32[]{:S(2)}) copy-start(f32[2,8,64,16]{2,3,1,0:T(8,128)} %param.28) | copy-start | bytes 196612
  1.0 14.4 %copy-start.10 = (f32[2,8,64,16]{2,3,1,0:T(8,128)S(1)}, f32[2,8,64,16]{2,3,1,0:T(8,128)}, u32[]{:S(2)}) copy-start(f32[2,8,64,16]{2,3,1,0:T(8,128)} %param.29) | copy-start | bytes 196612
  1.0 14.3 %copy-start.4 = (bf16[2048,128]{1,0:T(8,128)(2,1)S(1)}, bf16[2048,128]{1,0:T(8,128)(2,1)}, u32[]{:S(2)}) copy-start(bf16[2048,128]{1,0:T(8,128)(2,1)} %w_value.1) | copy-start | bytes 1572868
  1.0 14.3 %copy-start.5 = (bf16[2048,128]{1,0:T(8,128)(2,1)S(1)}, bf16[2048,128]{1,0:T(8,128)(2,1)}, u32[]{:S(2)}) copy-start(bf16[2048,128]{1,0:T(8,128)(2,1)} %w_mix.1) | copy-start | bytes 1572868
  1.0 14.3 %copy-start.11 = (f32[2,2,8,64]{3,2,1,0:T(8,128)S(1)}, f32[2,2,8,64]{3,2,1,0:T(8,128)}, u32[]{:S(2)}) copy-start(f32[2,2,8,64]{3,2,1,0:T(8,128)} %init.1) | copy-start | bytes 24580
  1.1 14.3 %copy-start.12 = (f32[2,8,64]{2,1,0:T(8,128)S(1)}, f32[2,8,64]{2,1,0:T(8,128)}, u32[]{:S(2)}) copy-start(f32[2,8,64]{2,1,0:T(8,128)} %decay.1) | copy-start | bytes 12292
  1.1 14.3 %copy-start.13 = (f32[2,8,64]{2,1,0:T(8,128)S(1)}, f32[2,8,64]{2,1,0:T(8,128)}, u32[]{:S(2)}) copy-start(f32[2,8,64]{2,1,0:T(8,128)} %turn.1) | copy-start | bytes 12292
  26.3 27.7 %copy-start = (bf16[128,2048]{1,0:T(8,128)(2,1)S(1)}, bf16[128,2048]{1,0:T(8,128)(2,1)}, u32[]{:S(2)}) copy-start(bf16[128,2048]{1,0:T(8,128)(2,1)} %proj_conv.1) | copy-start | bytes 1572868
  26.3 27.7 %copy-start.1 = (bf16[128,2048]{1,0:T(8,128)(2,1)S(1)}, bf16[128,2048]{1,0:T(8,128)(2,1)}, u32[]{:S(2)}) copy-start(bf16[128,2048]{1,0:T(8,128)(2,1)} %proj_state.1) | copy-start | bytes 1572868
  26.3 27.7 %copy-start.2 = (f32[2,8,16,64]{3,2,1,0:T(8,128)S(1)}, f32[2,8,16,64]{3,2,1,0:T(8,128)}, u32[]{:S(2)}) copy-start(f32[2,8,16,64]{3,2,1,0:T(8,128)} %param.30) | copy-start | bytes 196612
  26.3 27.7 %copy-start.3 = (f32[2,8,16,64]{3,2,1,0:T(8,128)S(1)}, f32[2,8,16,64]{3,2,1,0:T(8,128)}, u32[]{:S(2)}) copy-start(f32[2,8,16,64]{3,2,1,0:T(8,128)} %param.31) | copy-start | bytes 196612

commit v8 on v7

--- a/solution.py
+++ b/solution.py
@@ -171,7 +171,8 @@
     squares = 0.0
     for k in range(parts):
         x = rows[k, 0:n, :].astype(F32)
-        squares = squares + jnp.sum(x * x, axis=1, keepdims=True)
+        squares = squares + x * x
+    squares = jnp.sum(squares, axis=1, keepdims=True)
     inv_rms = lax.rsqrt(squares / D + EPSILON)
     first = second = 0.0
     for k in range(parts):

time: 67.1 us -> 67.1 us (level)
  no operation moved by 1% of the time
where the time goes in v8:
time: 67.1 us; the launch traced here: 66.8 us
  blocking collectives  61.4 us (92%)
  Pallas kernels  3.53 us (5%)
  local copies, waits for them, and re-layouts  0.95 us (1%)
  other arithmetic  0.75 us (1%)
    all_to_all x4, blocking collectives, exchange(): return lax.all_to_all(x, axis, split_axis=0, concat_axis=0, tiled=True)  61.4 us
    pallas_call x5, Pallas kernels, call(): pl.pallas_call(kernel, out_shape=[jax.ShapeDtypeStruct(s, d) for s, d in...  3.53 us

profile of v8, /device:TPU:2, one launch (start us, length us, event | category | flops | bytes accessed | tf_op | source)
XLA Modules:
  0.0 66.8 jit_solution(17842788726994846251)
XLA Ops:
  0.0 0.0 copy-start.8
  0.0 0.0 copy-start.15
  0.0 0.0 copy-start.14
  0.0 0.0 copy-start.16
  0.0 0.0 copy-start.17
  0.0 0.9 %copy-done.8 = bf16[128,512]{1,0:T(8,128)(2,1)S(1)} copy-done((bf16[128,512]{1,0:T(8,128)(2,1)S(1)}, bf16[128,512]{1,0:T(8,128)(2,1)}, u32[]{:S(2)}) %copy-start.8) | copy-done | bytes 131096
  0.9 0.0 copy-done.15
  0.9 0.0 copy-done.14
  0.9 0.0 copy-done.16
  0.9 0.0 copy-done.17
  0.9 0.0 copy-start.6
  0.9 0.0 copy-start.7
  0.9 0.0 copy-start.9
  1.0 0.0 copy-start.10
  1.0 0.0 copy-start.4
  1.0 0.0 copy-start.5
  1.0 0.0 copy-start.11
  1.1 0.0 copy-start.12
  1.1 0.0 copy-start.13
  1.1 14.2 %all_to_all.20.rows = bf16[4,136,512]{2,1,0:T(8,128)(2,1)S(1)} all-to-all(bf16[4,136,512]{2,1,0:T(8,128)(2,1)S(1)} %get-tuple-element.22), channel_id=1, replica_groups=mesh['sp_0'=16,'sp_1'=4,'sp_2'=2,'tp'=4] {'tp'}, dimensions={0} | all-to-all | bytes 1114112 | tf_op jit(solution)/shard_map/all_to_all | solution.py:358
  15.3 0.0 copy-done.6
  15.3 0.0 copy-done.7
  15.3 0.0 copy-done.9
  15.3 0.0 copy-done.10
  15.3 0.0 copy-done.4
  15.3 0.0 copy-done.5
  15.3 0.0 copy-done.11
  15.4 0.0 copy-done.12
  15.4 0.0 copy-done.13
  15.4 2.1 %local.1 = (f32[128,1024]{1,0:T(8,128)S(1)}, f32[128,1024]{1,0:T(8,128)S(1)}, f32[8,1024]{1,0:T(8,128)S(1)}, f32[8,1024]{1,0:T(8,128)S(1)}, f32[128,1024]{1,0:T(...) custom-call(bf16[4,136,512]{2,1,0:T(8,128)(2,1)S(1)} %all_to_all.20., ...), custom_call_target="tpu_custom_call" | custom-call | flops 1000000000 | bytes 1000000 | tf_op jit(solution)/shard_map/local/pallas_call | solution.py:365
  17.5 8.9 %all_to_all.21.got = bf16[8,24,128]{2,1,0:T(8,128)(2,1)S(1)} all-to-all(bf16[8,24,128]{2,1,0:T(8,128)(2,1)S(1)} %get-tuple-element.24), channel_id=1, replica_groups=mesh['sp_0'=16,'sp_1'=4,'sp_2'=2,'tp'=4] {'sp_1','sp_2'}, dimensions={0} | all-to-all | bytes 98304 | tf_op jit(solution)/shard_map/all_to_all | solution.py:358
  26.3 0.0 copy-start
  26.3 0.0 copy-start.1
  26.3 0.0 copy-start.2
  26.3 0.0 copy-start.3
  26.4 0.1 plane.1
  26.5 27.6 %all_to_all.22.got = bf16[16,4,384]{2,1,0:T(4,128)(2,1)S(1)} all-to-all(bf16[16,4,384]{2,1,0:T(4,128)(2,1)S(1)} %get-tuple-element.26), channel_id=1, replica_groups=mesh['sp_0'=16,'sp_1'=4,'sp_2'=2,'tp'=4] {'sp_0'}, dimensions={0} | all-to-all | bytes 98304 | tf_op jit(solution)/shard_map/all_to_all | solution.py:358
  54.1 0.0 copy-done
  54.1 0.0 copy-done.1
  54.1 0.0 copy-done.2
  54.1 0.0 copy-done.3
  54.1 1.3 %finish.1 = bf16[4,128,512]{2,1,0:T(8,128)(2,1)S(1)} custom-call(bf16[16,4,384]{2,1,0:T(4,128)(2,1)S(1)} %all_to_all.22.got, f32[48,128]{1,0:T(8,128)S(1)} %get-tuple-element.27.inner, f32[40,128]{1,0:T(8,128)S(1)} %get-tuple-element.25.consts, f32[128,1024]{1,0:T(8,128)S(1)} %get-tuple-element.28.ur, f32[128,1024]{1,0:T(8,128)S(1)} %get-tuple-element.29.ui, ...), custom_call_target="tpu_custom_call" | custom-call | flops 1000000000 | bytes 1000000 | tf_op jit(solution)/shard_map/finish/pallas_call | solution.py:365
  55.4 10.7 %all_to_all.23 = bf16[4,128,512]{2,1,0:T(8,128)(2,1)S(1)} all-to-all(bf16[4,128,512]{2,1,0:T(8,128)(2,1)S(1)} %finish.1), channel_id=1, replica_groups=mesh['sp_0'=16,'sp_1'=4,'sp_2'=2,'tp'=4] {'tp'}, dimensions={0} | all-to-all | bytes 1048576 | tf_op jit(solution)/shard_map/all_to_all | solution.py:358
  66.1 0.7 %reduce_sum.12 = bf16[128,512]{1,0:T(8,128)(2,1)} reduce(bf16[4,128,512]{2,1,0:T(8,128)(2,1)S(1)} %all_to_all.23, bf16[]{:T(256)} %constant.2.clone.1), dimensions={0}, to_apply=%region_0.0 | reduce | flops 196608 | bytes 655362 | tf_op jit(solution)/shard_map/reduce_sum | solution.py:444
  (2 shorter events, 0.0 us)
Async XLA Ops:
  0.0 0.9 %copy-start.8 = (bf16[128,512]{1,0:T(8,128)(2,1)S(1)}, bf16[128,512]{1,0:T(8,128)(2,1)}, u32[]{:S(2)}) copy-start(bf16[128,512]{1,0:T(8,128)(2,1)} %stream.1) | copy-start | bytes 393220
  0.0 0.9 %copy-start.15 = (f32[3,128]{1,0:T(4,128)S(1)}, f32[3,128]{1,0:T(4,128)}, u32[]{:S(2)}) copy-start(f32[3,128]{1,0:T(4,128)} %taps.1) | copy-start | bytes 4612
  0.0 0.9 %copy-start.14 = (f32[512]{0:T(512)S(1)}, f32[512]{0:T(512)}, u32[]{:S(2)}) copy-start(f32[512]{0:T(512)} %param.19) | copy-start | bytes 6148
  0.0 0.9 %copy-start.16 = (f32[128]{0:T(128)S(1)}, f32[128]{0:T(128)}, u32[]{:S(2)}) copy-start(f32[128]{0:T(128)} %param.33) | copy-start | bytes 1540
  0.0 0.9 %copy-start.17 = (f32[128]{0:T(128)S(1)}, f32[128]{0:T(128)}, u32[]{:S(2)}) copy-start(f32[128]{0:T(128)} %param.25) | copy-start | bytes 1540
  0.9 14.4 %copy-start.6 = (bf16[2048,128]{1,0:T(8,128)(2,1)S(1)}, bf16[2048,128]{1,0:T(8,128)(2,1)}, u32[]{:S(2)}) copy-start(bf16[2048,128]{1,0:T(8,128)(2,1)} %w_gate.1) | copy-start | bytes 1572868
  0.9 14.4 %copy-start.7 = (bf16[2048,128]{1,0:T(8,128)(2,1)S(1)}, bf16[2048,128]{1,0:T(8,128)(2,1)}, u32[]{:S(2)}) copy-start(bf16[2048,128]{1,0:T(8,128)(2,1)} %w_state.1) | copy-start | bytes 1572868
  0.9 14.4 %copy-start.9 = (f32[2,8,64,16]{2,3,1,0:T(8,128)S(1)}, f32[2,8,64,16]{2,3,1,0:T(8,128)}, u32[]{:S(2)}) copy-start(f32[2,8,64,16]{2,3,1,0:T(8,128)} %param.28) | copy-start | bytes 196612
  1.0 14.4 %copy-start.10 = (f32[2,8,64,16]{2,3,1,0:T(8,128)S(1)}, f32[2,8,64,16]{2,3,1,0:T(8,128)}, u32[]{:S(2)}) copy-start(f32[2,8,64,16]{2,3,1,0:T(8,128)} %param.29) | copy-start | bytes 196612
  1.0 14.3 %copy-start.4 = (bf16[2048,128]{1,0:T(8,128)(2,1)S(1)}, bf16[2048,128]{1,0:T(8,128)(2,1)}, u32[]{:S(2)}) copy-start(bf16[2048,128]{1,0:T(8,128)(2,1)} %w_value.1) | copy-start | bytes 1572868
  1.0 14.3 %copy-start.5 = (bf16[2048,128]{1,0:T(8,128)(2,1)S(1)}, bf16[2048,128]{1,0:T(8,128)(2,1)}, u32[]{:S(2)}) copy-start(bf16[2048,128]{1,0:T(8,128)(2,1)} %w_mix.1) | copy-start | bytes 1572868
  1.0 14.3 %copy-start.11 = (f32[2,2,8,64]{3,2,1,0:T(8,128)S(1)}, f32[2,2,8,64]{3,2,1,0:T(8,128)}, u32[]{:S(2)}) copy-start(f32[2,2,8,64]{3,2,1,0:T(8,128)} %init.1) | copy-start | bytes 24580
  1.1 14.3 %copy-start.12 = (f32[2,8,64]{2,1,0:T(8,128)S(1)}, f32[2,8,64]{2,1,0:T(8,128)}, u32[]{:S(2)}) copy-start(f32[2,8,64]{2,1,0:T(8,128)} %decay.1) | copy-start | bytes 12292
  1.1 14.3 %copy-start.13 = (f32[2,8,64]{2,1,0:T(8,128)S(1)}, f32[2,8,64]{2,1,0:T(8,128)}, u32[]{:S(2)}) copy-start(f32[2,8,64]{2,1,0:T(8,128)} %turn.1) | copy-start | bytes 12292
  26.3 27.7 %copy-start = (bf16[128,2048]{1,0:T(8,128)(2,1)S(1)}, bf16[128,2048]{1,0:T(8,128)(2,1)}, u32[]{:S(2)}) copy-start(bf16[128,2048]{1,0:T(8,128)(2,1)} %proj_conv.1) | copy-start | bytes 1572868
  26.3 27.7 %copy-start.1 = (bf16[128,2048]{1,0:T(8,128)(2,1)S(1)}, bf16[128,2048]{1,0:T(8,128)(2,1)}, u32[]{:S(2)}) copy-start(bf16[128,2048]{1,0:T(8,128)(2,1)} %proj_state.1) | copy-start | bytes 1572868
  26.3 27.7 %copy-start.2 = (f32[2,8,16,64]{3,2,1,0:T(8,128)S(1)}, f32[2,8,16,64]{3,2,1,0:T(8,128)}, u32[]{:S(2)}) copy-start(f32[2,8,16,64]{3,2,1,0:T(8,128)} %param.30) | copy-start | bytes 196612
  26.3 27.7 %copy-start.3 = (f32[2,8,16,64]{3,2,1,0:T(8,128)S(1)}, f32[2,8,16,64]{3,2,1,0:T(8,128)}, u32[]{:S(2)}) copy-start(f32[2,8,16,64]{3,2,1,0:T(8,128)} %param.31) | copy-start | bytes 196612

commit v9 on v8

--- a/solution.py
+++ b/solution.py
@@ -39,12 +39,12 @@
 
 
 def damped(half_rate, elapsed):
-    x = half_rate * elapsed
-    root = jnp.exp2(x * -LOG2E)
+    x = (half_rate * -LOG2E) * elapsed
+    root = jnp.exp2(x)
     magnitude = root * root
     square = x * x
-    series = root * (x * (-2.0 - square * (1 / 3 + square * (1 / 60))))
-    return magnitude, jnp.where(x < 0.25, series, magnitude - 1.0)
+    series = root * (x * (1.3862943611198906 + square * (0.11100821732964315 + square * 0.002666711628)))
+    return magnitude, jnp.where(x > -0.36, series, magnitude - 1.0)
 
 
 def moved(elapsed, rate, half_turn):

time: 67.1 us -> 67.1 us (level)
  no operation moved by 1% of the time
where the time goes in v9:
time: 67.1 us; the launch traced here: 66.8 us
  blocking collectives  61.4 us (92%)
  Pallas kernels  3.53 us (5%)
  local copies, waits for them, and re-layouts  0.95 us (1%)
  other arithmetic  0.75 us (1%)
    all_to_all x4, blocking collectives, exchange(): return lax.all_to_all(x, axis, split_axis=0, concat_axis=0, tiled=True)  61.4 us
    pallas_call x5, Pallas kernels, call(): pl.pallas_call(kernel, out_shape=[jax.ShapeDtypeStruct(s, d) for s, d in...  3.53 us

profile of v9, /device:TPU:2, one launch (start us, length us, event | category | flops | bytes accessed | tf_op | source)
XLA Modules:
  0.0 66.8 jit_solution(9439997017595780544)
XLA Ops:
  0.0 0.0 copy-start.8
  0.0 0.0 copy-start.15
  0.0 0.0 copy-start.14
  0.0 0.0 copy-start.16
  0.0 0.0 copy-start.17
  0.0 0.9 %copy-done.8 = bf16[128,512]{1,0:T(8,128)(2,1)S(1)} copy-done((bf16[128,512]{1,0:T(8,128)(2,1)S(1)}, bf16[128,512]{1,0:T(8,128)(2,1)}, u32[]{:S(2)}) %copy-start.8) | copy-done | bytes 131096
  0.9 0.0 copy-done.15
  0.9 0.0 copy-done.14
  0.9 0.0 copy-done.16
  0.9 0.0 copy-done.17
  0.9 0.0 copy-start.6
  0.9 0.0 copy-start.7
  0.9 0.0 copy-start.9
  1.0 0.0 copy-start.10
  1.0 0.0 copy-start.4
  1.0 0.0 copy-start.5
  1.0 0.0 copy-start.11
  1.1 0.0 copy-start.12
  1.1 0.0 copy-start.13
  1.1 14.2 %all_to_all.20.rows = bf16[4,136,512]{2,1,0:T(8,128)(2,1)S(1)} all-to-all(bf16[4,136,512]{2,1,0:T(8,128)(2,1)S(1)} %get-tuple-element.22), channel_id=1, replica_groups=mesh['sp_0'=16,'sp_1'=4,'sp_2'=2,'tp'=4] {'tp'}, dimensions={0} | all-to-all | bytes 1114112 | tf_op jit(solution)/shard_map/all_to_all | solution.py:358
  15.3 0.0 copy-done.6
  15.3 0.0 copy-done.7
  15.3 0.0 copy-done.9
  15.3 0.0 copy-done.10
  15.3 0.0 copy-done.4
  15.3 0.0 copy-done.5
  15.3 0.0 copy-done.11
  15.4 0.0 copy-done.12
  15.4 0.0 copy-done.13
  15.4 2.1 %local.1 = (f32[128,1024]{1,0:T(8,128)S(1)}, f32[128,1024]{1,0:T(8,128)S(1)}, f32[8,1024]{1,0:T(8,128)S(1)}, f32[8,1024]{1,0:T(8,128)S(1)}, f32[128,1024]{1,0:T(...) custom-call(bf16[4,136,512]{2,1,0:T(8,128)(2,1)S(1)} %all_to_all.20., ...), custom_call_target="tpu_custom_call" | custom-call | flops 1000000000 | bytes 1000000 | tf_op jit(solution)/shard_map/local/pallas_call | solution.py:365
  17.5 8.9 %all_to_all.21.got = bf16[8,24,128]{2,1,0:T(8,128)(2,1)S(1)} all-to-all(bf16[8,24,128]{2,1,0:T(8,128)(2,1)S(1)} %get-tuple-element.24), channel_id=1, replica_groups=mesh['sp_0'=16,'sp_1'=4,'sp_2'=2,'tp'=4] {'sp_1','sp_2'}, dimensions={0} | all-to-all | bytes 98304 | tf_op jit(solution)/shard_map/all_to_all | solution.py:358
  26.3 0.0 copy-start
  26.3 0.0 copy-start.1
  26.3 0.0 copy-start.2
  26.3 0.0 copy-start.3
  26.3 0.1 plane.1
  26.5 27.6 %all_to_all.22.got = bf16[16,4,384]{2,1,0:T(4,128)(2,1)S(1)} all-to-all(bf16[16,4,384]{2,1,0:T(4,128)(2,1)S(1)} %get-tuple-element.26), channel_id=1, replica_groups=mesh['sp_0'=16,'sp_1'=4,'sp_2'=2,'tp'=4] {'sp_0'}, dimensions={0} | all-to-all | bytes 98304 | tf_op jit(solution)/shard_map/all_to_all | solution.py:358
  54.1 0.0 copy-done
  54.1 0.0 copy-done.1
  54.1 0.0 copy-done.2
  54.1 0.0 copy-done.3
  54.1 1.3 %finish.1 = bf16[4,128,512]{2,1,0:T(8,128)(2,1)S(1)} custom-call(bf16[16,4,384]{2,1,0:T(4,128)(2,1)S(1)} %all_to_all.22.got, f32[48,128]{1,0:T(8,128)S(1)} %get-tuple-element.27.inner, f32[40,128]{1,0:T(8,128)S(1)} %get-tuple-element.25.consts, f32[128,1024]{1,0:T(8,128)S(1)} %get-tuple-element.28.ur, f32[128,1024]{1,0:T(8,128)S(1)} %get-tuple-element.29.ui, ...), custom_call_target="tpu_custom_call" | custom-call | flops 1000000000 | bytes 1000000 | tf_op jit(solution)/shard_map/finish/pallas_call | solution.py:365
  55.4 10.7 %all_to_all.23 = bf16[4,128,512]{2,1,0:T(8,128)(2,1)S(1)} all-to-all(bf16[4,128,512]{2,1,0:T(8,128)(2,1)S(1)} %finish.1), channel_id=1, replica_groups=mesh['sp_0'=16,'sp_1'=4,'sp_2'=2,'tp'=4] {'tp'}, dimensions={0} | all-to-all | bytes 1048576 | tf_op jit(solution)/shard_map/all_to_all | solution.py:358
  66.1 0.7 %reduce_sum.12 = bf16[128,512]{1,0:T(8,128)(2,1)} reduce(bf16[4,128,512]{2,1,0:T(8,128)(2,1)S(1)} %all_to_all.23, bf16[]{:T(256)} %constant.2.clone.1), dimensions={0}, to_apply=%region_0.0 | reduce | flops 196608 | bytes 655362 | tf_op jit(solution)/shard_map/reduce_sum | solution.py:444
  (2 shorter events, 0.0 us)
Async XLA Ops:
  0.0 0.9 %copy-start.8 = (bf16[128,512]{1,0:T(8,128)(2,1)S(1)}, bf16[128,512]{1,0:T(8,128)(2,1)}, u32[]{:S(2)}) copy-start(bf16[128,512]{1,0:T(8,128)(2,1)} %stream.1) | copy-start | bytes 393220
  0.0 0.9 %copy-start.15 = (f32[3,128]{1,0:T(4,128)S(1)}, f32[3,128]{1,0:T(4,128)}, u32[]{:S(2)}) copy-start(f32[3,128]{1,0:T(4,128)} %taps.1) | copy-start | bytes 4612
  0.0 0.9 %copy-start.14 = (f32[512]{0:T(512)S(1)}, f32[512]{0:T(512)}, u32[]{:S(2)}) copy-start(f32[512]{0:T(512)} %param.19) | copy-start | bytes 6148
  0.0 0.9 %copy-start.16 = (f32[128]{0:T(128)S(1)}, f32[128]{0:T(128)}, u32[]{:S(2)}) copy-start(f32[128]{0:T(128)} %param.33) | copy-start | bytes 1540
  0.0 0.9 %copy-start.17 = (f32[128]{0:T(128)S(1)}, f32[128]{0:T(128)}, u32[]{:S(2)}) copy-start(f32[128]{0:T(128)} %param.25) | copy-start | bytes 1540
  0.9 14.4 %copy-start.6 = (bf16[2048,128]{1,0:T(8,128)(2,1)S(1)}, bf16[2048,128]{1,0:T(8,128)(2,1)}, u32[]{:S(2)}) copy-start(bf16[2048,128]{1,0:T(8,128)(2,1)} %w_gate.1) | copy-start | bytes 1572868
  0.9 14.4 %copy-start.7 = (bf16[2048,128]{1,0:T(8,128)(2,1)S(1)}, bf16[2048,128]{1,0:T(8,128)(2,1)}, u32[]{:S(2)}) copy-start(bf16[2048,128]{1,0:T(8,128)(2,1)} %w_state.1) | copy-start | bytes 1572868
  0.9 14.4 %copy-start.9 = (f32[2,8,64,16]{2,3,1,0:T(8,128)S(1)}, f32[2,8,64,16]{2,3,1,0:T(8,128)}, u32[]{:S(2)}) copy-start(f32[2,8,64,16]{2,3,1,0:T(8,128)} %param.28) | copy-start | bytes 196612
  1.0 14.4 %copy-start.10 = (f32[2,8,64,16]{2,3,1,0:T(8,128)S(1)}, f32[2,8,64,16]{2,3,1,0:T(8,128)}, u32[]{:S(2)}) copy-start(f32[2,8,64,16]{2,3,1,0:T(8,128)} %param.29) | copy-start | bytes 196612
  1.0 14.3 %copy-start.4 = (bf16[2048,128]{1,0:T(8,128)(2,1)S(1)}, bf16[2048,128]{1,0:T(8,128)(2,1)}, u32[]{:S(2)}) copy-start(bf16[2048,128]{1,0:T(8,128)(2,1)} %w_value.1) | copy-start | bytes 1572868
  1.0 14.3 %copy-start.5 = (bf16[2048,128]{1,0:T(8,128)(2,1)S(1)}, bf16[2048,128]{1,0:T(8,128)(2,1)}, u32[]{:S(2)}) copy-start(bf16[2048,128]{1,0:T(8,128)(2,1)} %w_mix.1) | copy-start | bytes 1572868
  1.0 14.3 %copy-start.11 = (f32[2,2,8,64]{3,2,1,0:T(8,128)S(1)}, f32[2,2,8,64]{3,2,1,0:T(8,128)}, u32[]{:S(2)}) copy-start(f32[2,2,8,64]{3,2,1,0:T(8,128)} %init.1) | copy-start | bytes 24580
  1.1 14.3 %copy-start.12 = (f32[2,8,64]{2,1,0:T(8,128)S(1)}, f32[2,8,64]{2,1,0:T(8,128)}, u32[]{:S(2)}) copy-start(f32[2,8,64]{2,1,0:T(8,128)} %decay.1) | copy-start | bytes 12292
  1.1 14.3 %copy-start.13 = (f32[2,8,64]{2,1,0:T(8,128)S(1)}, f32[2,8,64]{2,1,0:T(8,128)}, u32[]{:S(2)}) copy-start(f32[2,8,64]{2,1,0:T(8,128)} %turn.1) | copy-start | bytes 12292
  26.3 27.7 %copy-start = (bf16[128,2048]{1,0:T(8,128)(2,1)S(1)}, bf16[128,2048]{1,0:T(8,128)(2,1)}, u32[]{:S(2)}) copy-start(bf16[128,2048]{1,0:T(8,128)(2,1)} %proj_conv.1) | copy-start | bytes 1572868
  26.3 27.7 %copy-start.1 = (bf16[128,2048]{1,0:T(8,128)(2,1)S(1)}, bf16[128,2048]{1,0:T(8,128)(2,1)}, u32[]{:S(2)}) copy-start(bf16[128,2048]{1,0:T(8,128)(2,1)} %proj_state.1) | copy-start | bytes 1572868
  26.3 27.7 %copy-start.2 = (f32[2,8,16,64]{3,2,1,0:T(8,128)S(1)}, f32[2,8,16,64]{3,2,1,0:T(8,128)}, u32[]{:S(2)}) copy-start(f32[2,8,16,64]{3,2,1,0:T(8,128)} %param.30) | copy-start | bytes 196612
  26.3 27.7 %copy-start.3 = (f32[2,8,16,64]{3,2,1,0:T(8,128)S(1)}, f32[2,8,16,64]{3,2,1,0:T(8,128)}, u32[]{:S(2)}) copy-start(f32[2,8,16,64]{3,2,1,0:T(8,128)} %param.31) | copy-start | bytes 196612
